TPU v7x, 512 devices: a whole 4x4x16 slice. The times are simulated.
512 devices in a mesh: sp: 16 (over z), fs: 4 (over y), tp: 8 (over x, core).
Axes of the slice: x: 4, y: 4, z: 16, core: 2. Of those that a mesh axis runs over, the one named last changes fastest.
Arguments:
- tokens: bfloat16 [4, 8192, 2048], P('fs', ('sp', 'tp')), may hold values from -6 to 6
- input_gain: float32 [2048], replicated, may hold values from 0.1 to 1.9
- query_weight: bfloat16 [2048, 768], P(None, 'tp'), may hold values from -0.125 to 0.125
- latent_down: bfloat16 [2048, 256], replicated, may hold values from -0.125 to 0.125
- rotary_down: bfloat16 [2048, 32], replicated, may hold values from -0.125 to 0.125
- pool_down: bfloat16 [2048, 1024], P(None, 'tp'), may hold values from -0.125 to 0.125
- key_up: bfloat16 [256, 512], replicated, may hold values from -0.375 to 0.375
- value_up: bfloat16 [256, 1024], replicated, may hold values from -1.125 to 1.125, as said below
- query_gain: float32 [96], replicated, may hold values from 0.1 to 1.9
- key_gain: float32 [96], replicated, may hold values from 0.1 to 1.9
- pool_weight: bfloat16 [16, 64, 64], replicated, may hold values from -2.25 to 2.25, as said below
- pool_scale: float32 [1024], P('tp'), may hold values from 0.1 to 1.9
- attention_gain: float32 [1024], P('tp'), may hold values from 0.1 to 1.9
- pool_gain: float32 [1024], P('tp'), may hold values from 0.1 to 1.9
- attention_out: bfloat16 [1024, 2048], P('tp'), may hold values from -0.125 to 0.125
- pool_out: bfloat16 [1024, 2048], P('tp'), may hold values from -0.125 to 0.125
Outputs:
- mixed: bfloat16 [4, 8192, 2048], P('fs', ('sp', 'tp'))
Inputs may be any that keep to these rules, and one draw needn't show every extreme that they name: `value_up`: entries of order 256 ** -0.5 or larger. `pool_weight`: entries of order 64 ** -0.5 or larger.
All inputs are finite; a program needn't handle non-finite values.
Results may differ from a plain program's by a relative error of at most 0.015.
Values may be sent and summed in bfloat16 or wider, within the bound.
No kernel may reach another device: no remote copies, remote signals or barrier semaphores. Data moves between devices by JAX's collectives and lax.ppermute only.
A program may use at most 64 MiB of HBM per device.

v0:
```python
import math

import jax
import jax.numpy as jnp
from jax import lax
from jax.sharding import PartitionSpec as P

HEADS = 8
NOPE_DIM = 64
ROPE_DIM = 32
VALUE_DIM = 128
KV_LATENT = 256
GROUPS = 16
GROUP_DIM = 64
QK_DIM = 96


EPS = 1e-06
THETA = 10000.0
rim_rows = 16


def in_order(pieces, dim):
    pieces = jnp.moveaxis(pieces, 0, dim)
    dims = pieces.shape
    return pieces.reshape(*dims[:dim], dims[dim] * dims[dim + 1], *dims[dim + 2 :])


def from_everyone(array, axis):
    peers = lax.axis_size(axis)
    return lax.all_to_all(
        jnp.broadcast_to(array[None], (peers, *array.shape)), axis, 0, 0, tiled=True
    )


def collect(array, axis, dim):
    return in_order(from_everyone(array, axis), dim)


def passed_along(array, axis, by):
    peers = lax.axis_size(axis)
    pairs = [(i, i + by) for i in range(peers) if 0 <= i + by < peers]
    return lax.ppermute(array, axis, pairs)


def side_by_side(arrays, axis, dim, along):
    ends, at = ([], 0)
    for a in arrays[:-1]:
        at += a.shape[along]
        ends.append(at)
    both = jnp.concatenate(arrays, axis=along)
    return tuple(jnp.split(lax.all_gather(both, axis, axis=dim, tiled=True), ends, axis=along))


def over_copies(array, axis):
    everything = from_everyone(array, axis)
    return jnp.sum(everything, axis=0)


def packed_total(arrays, axis):
    ends = [0]
    for a in arrays:
        ends.append(ends[-1] + a.size)
    subtotal = over_copies(jnp.concatenate([a.ravel() for a in arrays]), axis)
    return tuple((subtotal[b:e].reshape(a.shape) for a, b, e in zip(arrays, ends, ends[1:])))


def in_blocks(array, dim, peers):
    dims = array.shape
    pieces = array.reshape(*dims[:dim], peers, dims[dim] // peers, *dims[dim + 1 :])
    return jnp.moveaxis(pieces, dim, 0)


def summed_on_arrival(array, axis, dim):
    peers = lax.axis_size(axis)
    pieces = lax.all_to_all(in_blocks(array, dim, peers), axis, 0, 0, tiled=True)
    return jnp.sum(pieces.astype(jnp.float32), axis=0)


def rms_scale(values):
    return lax.rsqrt(jnp.mean(values * values, axis=-1, keepdims=True) + EPS)


def rotate(values, positions):
    half = values.shape[-1] // 2
    inv_freq = 1.0 / THETA ** (jnp.arange(half, dtype=jnp.float32) / half)
    angle = positions[:, None, None] * inv_freq
    cosine = jnp.cos(angle)
    sine = jnp.sin(angle)
    first = values[..., :half]
    second = values[..., half:]
    return jnp.concatenate(
        [first * cosine - second * sine, second * cosine + first * sine], axis=-1
    )


def head_vectors(raw, gain, positions):
    normal = raw * rms_scale(raw) * gain
    turned = rotate(normal[..., NOPE_DIM:], positions)
    return jnp.concatenate([normal[..., :NOPE_DIM], turned], axis=-1).astype(jnp.bfloat16)


def expand_keys(latent_rows, first, key_up, value_up, key_gain):
    count = latent_rows.shape[0]
    heads = key_up.shape[1] // NOPE_DIM
    latent = latent_rows[:, :KV_LATENT].astype(jnp.float32)
    latent_normed = (latent * rms_scale(latent)).astype(jnp.bfloat16)
    plain = jnp.dot(latent_normed, key_up, preferred_element_type=jnp.float32).reshape(
        count, heads, NOPE_DIM
    )
    values = jnp.dot(latent_normed, value_up, preferred_element_type=jnp.float32).astype(
        jnp.bfloat16
    )
    shared = latent_rows[:, KV_LATENT:].astype(jnp.float32)
    shared = shared[:, None, :]
    positions = (first + jnp.arange(count, dtype=jnp.int32)).astype(jnp.float32)
    keys = head_vectors(jnp.concatenate([plain, shared], axis=-1), key_gain, positions)
    return (keys, values.reshape(count, heads, VALUE_DIM))


def attend(state, queries, keys, values, query_pos, key_pos):
    numer, denom = state
    scores = jnp.einsum("qhd,khd->hqk", queries, keys, preferred_element_type=jnp.float32)
    scores = scores * (1.0 / math.sqrt(QK_DIM))
    visible = key_pos[None, None, :] <= query_pos[None, :, None]
    weights = jnp.where(visible, jnp.exp(scores), 0.0)
    numer = numer + jnp.einsum(
        "hqk,khd->qhd", weights.astype(jnp.bfloat16), values, preferred_element_type=jnp.float32
    )
    denom = denom + jnp.sum(weights, axis=-1)
    return (numer, denom)


def keep_state(current):
    return current


def pool_mix(pool_input, before, group_ids, positions):
    count = pool_input.shape[0]
    groups = group_ids.shape[0]
    current = pool_input.astype(jnp.float32).reshape(count, groups, GROUP_DIM)
    extended = jnp.concatenate([before, pool_input], axis=0).astype(jnp.float32)
    extended = extended.reshape(count + rim_rows, groups, GROUP_DIM)
    window = jnp.left_shift(2, group_ids % 4).astype(jnp.float32)
    total = current
    for back in range(1, rim_rows):
        taken = (window > back).astype(jnp.float32)
        total = total + extended[rim_rows - back : rim_rows - back + count] * taken[None, :, None]
    divisor = jnp.minimum(positions[:, None] + 1.0, window[None, :])
    return (total / divisor[:, :, None] - current).astype(jnp.bfloat16)


def local(
    tokens,
    input_gain,
    query_weight,
    latent_down,
    rotary_down,
    pool_down,
    key_up,
    value_up,
    query_gain,
    key_gain,
    pool_weight,
    pool_scale,
    attention_gain,
    pool_gain,
    attention_out,
    pool_out,
):
    width_tp = lax.axis_size("tp")
    block = tokens.shape[1] * width_tp
    heads = HEADS // width_tp
    groups = GROUPS // width_tp
    member = lax.axis_index("tp")
    own_key_up = lax.dynamic_slice_in_dim(key_up, member * heads * NOPE_DIM, heads * NOPE_DIM, 1)
    own_value_up = lax.dynamic_slice_in_dim(
        value_up, member * heads * VALUE_DIM, heads * VALUE_DIM, 1
    )
    own_pool_weight = lax.dynamic_slice_in_dim(pool_weight, member * groups, groups, 0)
    source = tokens[0].astype(jnp.float32)
    normed = (source * rms_scale(source) * input_gain).astype(jnp.bfloat16)
    offset = lax.axis_index("sp") * block
    positions_int = offset + jnp.arange(block, dtype=jnp.int32)
    positions = positions_int.astype(jnp.float32)
    latent_width = KV_LATENT + ROPE_DIM
    query_width = heads * QK_DIM
    piece = collect(normed, "tp", 0)
    projected = jnp.concatenate(
        [
            jnp.dot(piece, latent_down, preferred_element_type=jnp.float32),
            jnp.dot(piece, rotary_down, preferred_element_type=jnp.float32),
            jnp.dot(piece, query_weight, preferred_element_type=jnp.float32),
            jnp.dot(piece, pool_down, preferred_element_type=jnp.float32),
        ],
        axis=1,
    )
    latent_rows = projected[:, :latent_width].astype(jnp.bfloat16)
    query_raw = projected[:, latent_width : latent_width + query_width]
    pool_input = projected[:, latent_width + query_width :].astype(jnp.bfloat16)
    pool_channels = pool_input.shape[1]
    rim = pool_input[block - rim_rows :]
    before = passed_along(rim, "sp", 1)
    queries = head_vectors(query_raw.reshape(block, heads, QK_DIM), query_gain, positions)
    last_query = offset + block - 1
    start_state = (
        jnp.zeros((block, heads, VALUE_DIM), jnp.float32),
        jnp.zeros((heads, block), jnp.float32),
    )
    own_keys, own_values = expand_keys(latent_rows, offset, own_key_up, own_value_up, key_gain)
    flat_keys = own_keys.reshape(block, heads * QK_DIM)
    flat_values = own_values.reshape(block, heads * VALUE_DIM)
    piece_keys, piece_values = side_by_side((flat_keys, flat_values), "sp", 0, 1)

    def one_block(index, inner):
        first = index * block

        def work(current):
            keys = lax.dynamic_slice_in_dim(piece_keys, index * block, block, 0)
            values = lax.dynamic_slice_in_dim(piece_values, index * block, block, 0)
            key_pos = first + jnp.arange(block, dtype=jnp.int32)
            return attend(
                current,
                queries,
                keys.reshape(block, heads, QK_DIM),
                values.reshape(block, heads, VALUE_DIM),
                positions_int,
                key_pos,
            )

        return lax.cond(first <= last_query, work, keep_state, inner)

    numer, denom = lax.fori_loop(0, piece_keys.shape[0] // block, one_block, start_state)
    attended = (numer / jnp.transpose(denom)[:, :, None]).reshape(block, heads * VALUE_DIM)
    group_ids = member * groups + jnp.arange(groups, dtype=jnp.int32)
    pooled_mean = pool_mix(pool_input, before, group_ids, positions)
    pooled = jnp.einsum(
        "rgc,gcd->rgd", pooled_mean, own_pool_weight, preferred_element_type=jnp.float32
    )
    pooled = pooled.reshape(block, pool_channels) * pool_scale
    attention_total, pool_total = packed_total(
        (jnp.sum(attended * attended, axis=1), jnp.sum(pooled * pooled, axis=1)), "tp"
    )
    attention_factor = lax.rsqrt(attention_total / (HEADS * VALUE_DIM) + EPS)
    pool_factor = lax.rsqrt(pool_total / (GROUPS * GROUP_DIM) + EPS)
    attention_mixed = (attended * attention_factor[:, None] * attention_gain).astype(jnp.bfloat16)
    pool_mixed = (pooled * pool_factor[:, None] * pool_gain).astype(jnp.bfloat16)
    term = jnp.dot(attention_mixed, attention_out, preferred_element_type=jnp.float32)
    summed = summed_on_arrival(
        (term + jnp.dot(pool_mixed, pool_out, preferred_element_type=jnp.float32)).astype(
            jnp.bfloat16
        ),
        "tp",
        0,
    )
    return summed.astype(jnp.bfloat16)[None]


def solution(mesh):
    placed = (
        P("fs", ("sp", "tp"), None),
        P(),
        P(None, "tp"),
        P(),
        P(),
        P(None, "tp"),
        P(),
        P(),
        P(),
        P(),
        P(),
        P("tp"),
        P("tp"),
        P("tp"),
        P("tp", None),
        P("tp", None),
    )
    return jax.shard_map(
        local, mesh=mesh, in_specs=placed, out_specs=P("fs", ("sp", "tp"), None), check_vma=False
    )
```

profile of v0, /device:TPU:480, one launch (start us, length us, event | category | flops | bytes accessed | tf_op | source)
XLA Modules:
  0.0 220.1 jit_solution(3788211713811370109)
XLA Ops:
  10.4 4.3 %all-to-all-start = ((bf16[8,64,2048]{2,1,0:T(8,128)(2,1)}), bf16[8,64,2048]{2,1,0:T(8,128)(2,1)S(1)}, u32[]{:S(2)}, u32[]{:S(2)}) async-start(bf16[8,64,2048]{2,1,0:T(8,128)(2,1)} %broadcast_in_dim.18), calls=%async_computation | async-start | bytes 4194304 | tf_op jit(solution)/shard_map/all_to_all | solution.py:31
  14.8 27.1 %all-to-all-done = bf16[8,64,2048]{2,1,0:T(8,128)(2,1)S(1)} async-done(((bf16[8,64,2048]{2,1,0:T(8,128)(2,1)}), bf16[8,64,2048]{2,1,0:T(8,128)(2,1)S(1)}, u32[]{:S(2)}, u32[]{:S(2)}) %all-to-all-start) | async-done | bytes 2097184 | tf_op jit(solution)/shard_map/all_to_all | solution.py:31
  55.1 3.4 %collective-permute-done = bf16[16,128]{1,0:T(8,128)(2,1)S(1)} collective-permute-done((bf16[16,128]{1,0:T(8,128)(2,1)S(1)}, bf16[16,128]{1,0:T(8,128)(2,1)S(1)}, u32[]{:S(2)}, u32[]{:S(2)}) %collective-permute-start) | collective-permute-done | bytes 4128 | tf_op jit(solution)/shard_map/ppermute | solution.py:43
  78.2 43.5 %all-gather.2.cloned.1.call-done = bf16[8192,224]{0,1:T(8,128)(2,1)} async-done(((bf16[512,224]{0,1:T(8,128)(2,1)}), bf16[8192,224]{0,1:T(8,128)(2,1)}) %all-gather.2.cloned.1.call-update) | async-done | bytes 3670032 | tf_op jit(solution)/shard_map/all_gather | solution.py:52
  123.3 2.4 %copy.76 = bf16[8192,128]{1,0:T(8,128)(2,1)} copy(bf16[8192,128]{0,1:T(8,128)(2,1)S(1)} %slice-done) | data formatting | bytes 4194304
  129.7 41.2 %while.16 = (s32[]{:T(128)}, f32[512,1,128]{0,2,1:T(8,128)S(1)}, f32[1,512]{1,0:T(1,128)S(1)}, s32[]{:T(128)}, bf16[8192,128]{1,0:T(8,128)(2,1)}, /*index=5*/bf1...) while((s32[]{:T(128)}, f32[512,1,128]{0,2,1:T(8,128)S(1)}, ...), condition=%wide.region_8.9_spmd.clone, body=%wide.region_4.8_spmd.clone.sunk | while | flops 118817792 | bytes 1954101 | solution.py:233
  129.7 2.6 %conditional.3 = ((f32[512,1,128]{0,2,1:T(8,128)S(1)}, f32[1,512]{1,0:T(1,128)S(1)})) conditional(s32[]{:T(128)} %convert_element_type.344, (f32[512,1,128]{0,2,1:T(8,128)S(1)}, f32[1,512]{1,0:T(1,128)S(1)}) %tuple.78, (s32[]{:T(128)}, bf16[8192,128]{1,0:T(8,128)(2,1)}, s32[]{:T(128)}, s32[]{:T(128)}, bf16[8192,96]{1,0:T(8,128)(2,1)}, ...), branch_computations={%region_5.0_spmd, %region_6.7_spmd} | conditional | flops 118817792 | bytes 1951830 | solution.py:231
  132.3 2.5 %conditional.3 = ((f32[512,1,128]{0,2,1:T(8,128)S(1)}, f32[1,512]{1,0:T(1,128)S(1)})) conditional(s32[]{:T(128)} %convert_element_type.344, (f32[512,1,128]{0,2,1:T(8,128)S(1)}, f32[1,512]{1,0:T(1,128)S(1)}) %tuple.78, (s32[]{:T(128)}, bf16[8192,128]{1,0:T(8,128)(2,1)}, s32[]{:T(128)}, s32[]{:T(128)}, bf16[8192,96]{1,0:T(8,128)(2,1)}, ...), branch_computations={%region_5.0_spmd, %region_6.7_spmd} | conditional | flops 118817792 | bytes 1951830 | solution.py:231
  134.9 2.5 %conditional.3 = ((f32[512,1,128]{0,2,1:T(8,128)S(1)}, f32[1,512]{1,0:T(1,128)S(1)})) conditional(s32[]{:T(128)} %convert_element_type.344, (f32[512,1,128]{0,2,1:T(8,128)S(1)}, f32[1,512]{1,0:T(1,128)S(1)}) %tuple.78, (s32[]{:T(128)}, bf16[8192,128]{1,0:T(8,128)(2,1)}, s32[]{:T(128)}, s32[]{:T(128)}, bf16[8192,96]{1,0:T(8,128)(2,1)}, ...), branch_computations={%region_5.0_spmd, %region_6.7_spmd} | conditional | flops 118817792 | bytes 1951830 | solution.py:231
  137.5 2.5 %conditional.3 = ((f32[512,1,128]{0,2,1:T(8,128)S(1)}, f32[1,512]{1,0:T(1,128)S(1)})) conditional(s32[]{:T(128)} %convert_element_type.344, (f32[512,1,128]{0,2,1:T(8,128)S(1)}, f32[1,512]{1,0:T(1,128)S(1)}) %tuple.78, (s32[]{:T(128)}, bf16[8192,128]{1,0:T(8,128)(2,1)}, s32[]{:T(128)}, s32[]{:T(128)}, bf16[8192,96]{1,0:T(8,128)(2,1)}, ...), branch_computations={%region_5.0_spmd, %region_6.7_spmd} | conditional | flops 118817792 | bytes 1951830 | solution.py:231
  140.1 2.5 %conditional.3 = ((f32[512,1,128]{0,2,1:T(8,128)S(1)}, f32[1,512]{1,0:T(1,128)S(1)})) conditional(s32[]{:T(128)} %convert_element_type.344, (f32[512,1,128]{0,2,1:T(8,128)S(1)}, f32[1,512]{1,0:T(1,128)S(1)}) %tuple.78, (s32[]{:T(128)}, bf16[8192,128]{1,0:T(8,128)(2,1)}, s32[]{:T(128)}, s32[]{:T(128)}, bf16[8192,96]{1,0:T(8,128)(2,1)}, ...), branch_computations={%region_5.0_spmd, %region_6.7_spmd} | conditional | flops 118817792 | bytes 1951830 | solution.py:231
  142.6 2.5 %conditional.3 = ((f32[512,1,128]{0,2,1:T(8,128)S(1)}, f32[1,512]{1,0:T(1,128)S(1)})) conditional(s32[]{:T(128)} %convert_element_type.344, (f32[512,1,128]{0,2,1:T(8,128)S(1)}, f32[1,512]{1,0:T(1,128)S(1)}) %tuple.78, (s32[]{:T(128)}, bf16[8192,128]{1,0:T(8,128)(2,1)}, s32[]{:T(128)}, s32[]{:T(128)}, bf16[8192,96]{1,0:T(8,128)(2,1)}, ...), branch_computations={%region_5.0_spmd, %region_6.7_spmd} | conditional | flops 118817792 | bytes 1951830 | solution.py:231
  145.2 2.5 %conditional.3 = ((f32[512,1,128]{0,2,1:T(8,128)S(1)}, f32[1,512]{1,0:T(1,128)S(1)})) conditional(s32[]{:T(128)} %convert_element_type.344, (f32[512,1,128]{0,2,1:T(8,128)S(1)}, f32[1,512]{1,0:T(1,128)S(1)}) %tuple.78, (s32[]{:T(128)}, bf16[8192,128]{1,0:T(8,128)(2,1)}, s32[]{:T(128)}, s32[]{:T(128)}, bf16[8192,96]{1,0:T(8,128)(2,1)}, ...), branch_computations={%region_5.0_spmd, %region_6.7_spmd} | conditional | flops 118817792 | bytes 1951830 | solution.py:231
  147.8 2.5 %conditional.3 = ((f32[512,1,128]{0,2,1:T(8,128)S(1)}, f32[1,512]{1,0:T(1,128)S(1)})) conditional(s32[]{:T(128)} %convert_element_type.344, (f32[512,1,128]{0,2,1:T(8,128)S(1)}, f32[1,512]{1,0:T(1,128)S(1)}) %tuple.78, (s32[]{:T(128)}, bf16[8192,128]{1,0:T(8,128)(2,1)}, s32[]{:T(128)}, s32[]{:T(128)}, bf16[8192,96]{1,0:T(8,128)(2,1)}, ...), branch_computations={%region_5.0_spmd, %region_6.7_spmd} | conditional | flops 118817792 | bytes 1951830 | solution.py:231
  150.3 2.5 %conditional.3 = ((f32[512,1,128]{0,2,1:T(8,128)S(1)}, f32[1,512]{1,0:T(1,128)S(1)})) conditional(s32[]{:T(128)} %convert_element_type.344, (f32[512,1,128]{0,2,1:T(8,128)S(1)}, f32[1,512]{1,0:T(1,128)S(1)}) %tuple.78, (s32[]{:T(128)}, bf16[8192,128]{1,0:T(8,128)(2,1)}, s32[]{:T(128)}, s32[]{:T(128)}, bf16[8192,96]{1,0:T(8,128)(2,1)}, ...), branch_computations={%region_5.0_spmd, %region_6.7_spmd} | conditional | flops 118817792 | bytes 1951830 | solution.py:231
  152.9 2.5 %conditional.3 = ((f32[512,1,128]{0,2,1:T(8,128)S(1)}, f32[1,512]{1,0:T(1,128)S(1)})) conditional(s32[]{:T(128)} %convert_element_type.344, (f32[512,1,128]{0,2,1:T(8,128)S(1)}, f32[1,512]{1,0:T(1,128)S(1)}) %tuple.78, (s32[]{:T(128)}, bf16[8192,128]{1,0:T(8,128)(2,1)}, s32[]{:T(128)}, s32[]{:T(128)}, bf16[8192,96]{1,0:T(8,128)(2,1)}, ...), branch_computations={%region_5.0_spmd, %region_6.7_spmd} | conditional | flops 118817792 | bytes 1951830 | solution.py:231
  155.5 2.5 %conditional.3 = ((f32[512,1,128]{0,2,1:T(8,128)S(1)}, f32[1,512]{1,0:T(1,128)S(1)})) conditional(s32[]{:T(128)} %convert_element_type.344, (f32[512,1,128]{0,2,1:T(8,128)S(1)}, f32[1,512]{1,0:T(1,128)S(1)}) %tuple.78, (s32[]{:T(128)}, bf16[8192,128]{1,0:T(8,128)(2,1)}, s32[]{:T(128)}, s32[]{:T(128)}, bf16[8192,96]{1,0:T(8,128)(2,1)}, ...), branch_computations={%region_5.0_spmd, %region_6.7_spmd} | conditional | flops 118817792 | bytes 1951830 | solution.py:231
  158.1 2.5 %conditional.3 = ((f32[512,1,128]{0,2,1:T(8,128)S(1)}, f32[1,512]{1,0:T(1,128)S(1)})) conditional(s32[]{:T(128)} %convert_element_type.344, (f32[512,1,128]{0,2,1:T(8,128)S(1)}, f32[1,512]{1,0:T(1,128)S(1)}) %tuple.78, (s32[]{:T(128)}, bf16[8192,128]{1,0:T(8,128)(2,1)}, s32[]{:T(128)}, s32[]{:T(128)}, bf16[8192,96]{1,0:T(8,128)(2,1)}, ...), branch_computations={%region_5.0_spmd, %region_6.7_spmd} | conditional | flops 118817792 | bytes 1951830 | solution.py:231
  160.6 2.5 %conditional.3 = ((f32[512,1,128]{0,2,1:T(8,128)S(1)}, f32[1,512]{1,0:T(1,128)S(1)})) conditional(s32[]{:T(128)} %convert_element_type.344, (f32[512,1,128]{0,2,1:T(8,128)S(1)}, f32[1,512]{1,0:T(1,128)S(1)}) %tuple.78, (s32[]{:T(128)}, bf16[8192,128]{1,0:T(8,128)(2,1)}, s32[]{:T(128)}, s32[]{:T(128)}, bf16[8192,96]{1,0:T(8,128)(2,1)}, ...), branch_computations={%region_5.0_spmd, %region_6.7_spmd} | conditional | flops 118817792 | bytes 1951830 | solution.py:231
  163.2 2.5 %conditional.3 = ((f32[512,1,128]{0,2,1:T(8,128)S(1)}, f32[1,512]{1,0:T(1,128)S(1)})) conditional(s32[]{:T(128)} %convert_element_type.344, (f32[512,1,128]{0,2,1:T(8,128)S(1)}, f32[1,512]{1,0:T(1,128)S(1)}) %tuple.78, (s32[]{:T(128)}, bf16[8192,128]{1,0:T(8,128)(2,1)}, s32[]{:T(128)}, s32[]{:T(128)}, bf16[8192,96]{1,0:T(8,128)(2,1)}, ...), branch_computations={%region_5.0_spmd, %region_6.7_spmd} | conditional | flops 118817792 | bytes 1951830 | solution.py:231
  165.8 2.5 %conditional.3 = ((f32[512,1,128]{0,2,1:T(8,128)S(1)}, f32[1,512]{1,0:T(1,128)S(1)})) conditional(s32[]{:T(128)} %convert_element_type.344, (f32[512,1,128]{0,2,1:T(8,128)S(1)}, f32[1,512]{1,0:T(1,128)S(1)}) %tuple.78, (s32[]{:T(128)}, bf16[8192,128]{1,0:T(8,128)(2,1)}, s32[]{:T(128)}, s32[]{:T(128)}, bf16[8192,96]{1,0:T(8,128)(2,1)}, ...), branch_computations={%region_5.0_spmd, %region_6.7_spmd} | conditional | flops 118817792 | bytes 1951830 | solution.py:231
  168.4 2.5 %conditional.3 = ((f32[512,1,128]{0,2,1:T(8,128)S(1)}, f32[1,512]{1,0:T(1,128)S(1)})) conditional(s32[]{:T(128)} %convert_element_type.344, (f32[512,1,128]{0,2,1:T(8,128)S(1)}, f32[1,512]{1,0:T(1,128)S(1)}) %tuple.78, (s32[]{:T(128)}, bf16[8192,128]{1,0:T(8,128)(2,1)}, s32[]{:T(128)}, s32[]{:T(128)}, bf16[8192,96]{1,0:T(8,128)(2,1)}, ...), branch_computations={%region_5.0_spmd, %region_6.7_spmd} | conditional | flops 118817792 | bytes 1951830 | solution.py:231
  171.0 9.5 %all_to_all.16 = f32[8,1,1024]{2,1,0:T(1,128)S(1)} all-to-all(f32[8,1,1024]{2,1,0:T(1,128)S(1)} %broadcast_in_dim.19), channel_id=1, replica_groups=mesh['sp'=16,'fs'=4,'tp'=8] {'tp'}, dimensions={0} | all-to-all | bytes 65536 | tf_op jit(solution)/shard_map/all_to_all | solution.py:31
  182.5 29.7 %all_to_all.17 = bf16[8,64,2048]{2,1,0:T(8,128)(2,1)S(1)} all-to-all(bf16[8,64,2048]{2,1,0:T(8,128)(2,1)S(1)} %bitcast.94), channel_id=1, replica_groups=mesh['sp'=16,'fs'=4,'tp'=8] {'tp'}, dimensions={0} | all-to-all | bytes 4194304 | tf_op jit(solution)/shard_map/all_to_all | solution.py:76
  (180 shorter events, 85.0 us)
Async XLA Ops:
  6.5 37.8 %copy-start = (bf16[2048,256]{1,0:T(8,128)(2,1)S(1)}, bf16[2048,256]{1,0:T(8,128)(2,1)}, u32[]{:S(2)}) copy-start(bf16[2048,256]{1,0:T(8,128)(2,1)} %param.23) | copy-start | bytes 3145732
  10.4 31.5 %all-to-all-start = ((bf16[8,64,2048]{2,1,0:T(8,128)(2,1)}), bf16[8,64,2048]{2,1,0:T(8,128)(2,1)S(1)}, u32[]{:S(2)}, u32[]{:S(2)}) async-start(bf16[8,64,2048]{2,1,0:T(8,128)(2,1)} %broadcast_in_dim.18), calls=%async_computation | async-start | bytes 4194304 | tf_op jit(solution)/shard_map/all_to_all | solution.py:31
  14.7 28.8 %copy-start.7 = (bf16[2048,96]{0,1:T(8,128)(2,1)S(1)}, bf16[2048,96]{0,1:T(8,128)(2,1)}, u32[]{:S(2)}) copy-start(bf16[2048,96]{0,1:T(8,128)(2,1)} %param.22) | copy-start | bytes 1179652
  14.7 107.0 %all-gather.2.cloned.1.call-start = ((), (), s32[]{:S(2)}) async-start(), calls=%async_computation.3 | async-start | bytes 3899392 | tf_op jit(solution)/shard_map/all_gather | solution.py:52
  44.4 2.0 copy-start.8
  44.4 3.2 %copy-start.9 = (f32[96]{0:T(128)S(1)}, f32[96]{0:T(128)}, u32[]{:S(2)}) copy-start(f32[96]{0:T(128)} %param.28) | copy-start | bytes 1156
  45.1 3.5 %copy-start.10 = (f32[128]{0:T(128)S(1)}, f32[128]{0:T(128)}, u32[]{:S(2)}) copy-start(f32[128]{0:T(128)} %param.31) | copy-start | bytes 1540
  52.9 5.5 %collective-permute-start = (bf16[16,128]{1,0:T(8,128)(2,1)S(1)}, bf16[16,128]{1,0:T(8,128)(2,1)S(1)}, u32[]{:S(2)}, u32[]{:S(2)}) collective-permute-start(bf16[16,128]{1,0:T(8,128)(2,1)S(1)} %slice.178), channel_id=1, source_target_pairs={{0,32},{32,64},{64,96},{96,128},{128,160},{160,192},{192,224},{224... | collective-permute-start | bytes 12296 | tf_op jit(solution)/shard_map/ppermute | solution.py:43
  72.2 3.8 %copy-start.1 = (f32[512,128]{0,1:T(8,128)S(1)}, f32[512,128]{0,1:T(8,128)}, u32[]{:S(2)}) copy-start(f32[512,128]{0,1:T(8,128)} %copy.79) | copy-start | bytes 786436
  73.0 3.0 %copy-start.2 = (f32[512,128]{0,1:T(8,128)S(1)}, f32[512,128]{0,1:T(8,128)}, u32[]{:S(2)}) copy-start(f32[512,128]{0,1:T(8,128)} %copy.88) | copy-start | bytes 786436
  73.9 2.1 copy-start.3
  74.7 1.3 copy-start.4
  121.7 1.6 slice-start
  125.8 1.4 slice-start.1
  129.6 50.9 %copy-start.11 = (f32[128]{0:T(128)S(1)}, f32[128]{0:T(128)}, u32[]{:S(2)}) copy-start(f32[128]{0:T(128)} %param.33) | copy-start | bytes 1540
  129.7 51.0 %copy-start.5 = (bf16[128,2048]{1,0:T(8,128)(2,1)S(1)}, bf16[128,2048]{1,0:T(8,128)(2,1)}, u32[]{:S(2)}) copy-start(bf16[128,2048]{1,0:T(8,128)(2,1)} %param.34) | copy-start | bytes 1572868
  129.7 51.0 %copy-start.12 = (f32[128]{0:T(128)S(1)}, f32[128]{0:T(128)}, u32[]{:S(2)}) copy-start(f32[128]{0:T(128)} %param.32) | copy-start | bytes 1540
  180.7 1.0 copy-start.6
Sparse Core Ops, SparseCore 0:
  48.7 72.9 all-gather.1
where the time goes:
time: 221 us; the launch traced here: 220 us
  waiting for transfers between devices  74 us (33%)
  matrix products  50.4 us (23%)
  blocking collectives  39.1 us (18%)
  local copies, waits for them, and re-layouts  28.3 us (13%)
  between operations  13.8 us (6%)
  other arithmetic  7.48 us (3%)
  starting transfers between devices  5.63 us (3%)
    all_gather x1, waiting for transfers between devices, side_by_side(): lax.all_gather(both, axis, axis=dim, tiled=True)  43.5 us
    all_to_all x1, blocking collectives, summed_on_arrival(): lax.all_to_all(in_blocks(array, dim, peers), axis, 0, 0, tiled=True)  29.7 us
    all_to_all x1, waiting for transfers between devices, from_everyone(): lax.all_to_all(jnp.broadcast_to(array[None], (peers, *array.shape)), axis...  27.1 us
    dot_general x16, matrix products, attend(): jnp.einsum('qhd,khd->hqk', queries, keys, preferred_element_type=jnp.floa...  20.7 us
    dot_general x16, matrix products, attend(): jnp.einsum('hqk,khd->qhd', weights.astype(jnp.bfloat16), values, preferre...  18.8 us
    slice x16, local copies, waits for them, and re-layouts, pool_mix(): extended[rim_rows - back:rim_rows - back + count] * taken[None, :, None]  17.5 us
    all_to_all x1, blocking collectives, from_everyone(): lax.all_to_all(jnp.broadcast_to(array[None], (peers, *array.shape)), axis...  9.5 us
    unnamed x28, local copies, waits for them, and re-layouts  5.18 us
  transfers between devices with their start and end apart: 3, of which 3 were waited for; matrix products, arithmetic and copies ran while one was open for 11% of the time, Pallas kernels for 0%

commit v1 on v0

v1 whole, which is shorter than its diff:
```python
import math

import jax
import jax.numpy as jnp
import numpy as np
from jax import lax
from jax.experimental import pallas as pl
from jax.experimental.pallas import tpu as pltpu
from jax.sharding import PartitionSpec as P

HEADS = 8
NOPE_DIM = 64
ROPE_DIM = 32
VALUE_DIM = 128
KV_LATENT = 256
GROUP_DIM = 64
QK_DIM = 96
D = 2048
BLOCKS = 16
BLOCK = 512
CHIPS = 4
ROWS = 64
LANES = 128
QROWS = CHIPS * ROWS
KEYS = BLOCKS * 2 * ROWS
HALO = 16
LAT = 384

EPS = 1e-06
THETA = 10000.0
SAME_CORE = [[0, 2, 4, 6], [1, 3, 5, 7]]
F32 = jnp.float32
BF16 = jnp.bfloat16


def angle_tables():
    half = ROPE_DIM // 2
    freq = np.zeros(LANES)
    inv = 1.0 / THETA ** (np.arange(half, dtype=np.float64) / half)
    freq[NOPE_DIM : NOPE_DIM + half] = inv
    freq[NOPE_DIM + half : QK_DIM] = inv
    inside = np.arange(BLOCK)[:, None] * freq[None, :]
    starts = (np.arange(BLOCKS) * BLOCK)[:, None] * freq[None, :]
    inside = np.stack([np.cos(inside), np.sin(inside)]).astype(np.float32)
    starts = np.stack([np.cos(starts), np.sin(starts)]).astype(np.float32)
    return inside.reshape(2, CHIPS, 2, ROWS, LANES), starts


def among_chips(array):
    return lax.all_to_all(array, "tp", 0, 0, axis_index_groups=SAME_CORE, tiled=True)


def to_partner(array):
    return lax.ppermute(array, "tp", [(i, i ^ 1) for i in range(2 * CHIPS)])


def whole(kernel, out_shape, *args, smem=1, scratch=(), name=None):
    single = not isinstance(out_shape, (list, tuple))
    outs = [out_shape] if single else list(out_shape)
    specs = [pl.BlockSpec(memory_space=pltpu.SMEM)] * smem
    specs += [pl.BlockSpec(memory_space=pltpu.VMEM)] * (len(args) - smem)
    out_specs = [pl.BlockSpec(memory_space=pltpu.VMEM)] * len(outs)
    return pl.pallas_call(
        kernel,
        out_shape=out_shape,
        in_specs=specs,
        out_specs=out_specs[0] if single else out_specs,
        scratch_shapes=list(scratch),
        compiler_params=pltpu.CompilerParams(vmem_limit_bytes=56 * 1024 * 1024),
        name=name,
    )(*args)


def dot(a, b, dims=((1,), (0,)), precision=None):
    return lax.dot_general(
        a, b, (dims, ((), ())), preferred_element_type=F32, precision=precision
    )


def turn(vectors, cosine, sine):
    lane = lax.broadcasted_iota(jnp.int32, vectors.shape, vectors.ndim - 1)
    half = ROPE_DIM // 2
    ahead = pltpu.roll(vectors, LANES - half, vectors.ndim - 1)
    behind = pltpu.roll(vectors, half, vectors.ndim - 1)
    return vectors * cosine + jnp.where(lane < NOPE_DIM + half, -ahead, behind) * sine


def at_block(inside_cos, inside_sin, start_cos, start_sin):
    cosine = start_cos * inside_cos - start_sin * inside_sin
    sine = start_sin * inside_cos + start_cos * inside_sin
    return cosine, sine


def norm_kernel(tokens, gain, latent_down, rotary_down, normed_out, latent_out):
    source = tokens[0].astype(F32)
    scale = lax.rsqrt(jnp.mean(source * source, axis=-1, keepdims=True) + EPS)
    normed = (source * scale * gain[...]).astype(BF16)
    for chip in range(CHIPS):
        normed_out[chip] = normed
    latent_out[:, :KV_LATENT] = dot(normed, latent_down[...]).astype(BF16)
    latent_out[:, KV_LATENT:] = dot(normed, rotary_down[...]).astype(BF16)


def project_kernel(coords, rows, own, other, gain, inside, starts, query_out, pool_out):
    z, p = coords[0], coords[2]
    piece = rows[...].reshape(QROWS, D)
    start_cos = starts[0, pl.ds(z, 1), :]
    start_sin = starts[1, pl.ds(z, 1), :]
    inside_cos = jnp.concatenate([inside[0, c, p] for c in range(CHIPS)], axis=0)
    inside_sin = jnp.concatenate([inside[1, c, p] for c in range(CHIPS)], axis=0)
    cosine, sine = at_block(inside_cos, inside_sin, start_cos, start_sin)
    for weights, slot in ((own, p), (other, 1 - p)):
        both = dot(piece, weights[...])
        raw = both[:, :LANES]
        square = jnp.sum(raw * raw, axis=-1, keepdims=True) * (1.0 / QK_DIM)
        normal = raw * lax.rsqrt(square + EPS) * gain[...]
        queries = turn(normal, cosine, sine).astype(BF16)
        for chip in range(CHIPS):
            query_out[chip, slot] = queries
        pool_out[slot] = both[:, LANES:].astype(BF16)


def expand_kernel(coords, own, other, key_up, gain, inside, starts, keys_out, latent_out):
    z, x, p = coords[0], coords[1], coords[2]
    lane = lax.broadcasted_iota(jnp.int32, (1, LANES), 1)
    plain_gain = jnp.where(lane < NOPE_DIM, gain[...], 0.0)
    rotary_gain = jnp.where(lane < NOPE_DIM, 0.0, gain[...])

    def one(block, carry):
        start_cos = starts[0, pl.ds(block, 1), :]
        start_sin = starts[1, pl.ds(block, 1), :]
        for rows, slot in ((own, p), (other, 1 - p)):
            at = block * 2 * ROWS + slot * ROWS
            at = pl.multiple_of(at, ROWS)
            packed = rows[block].astype(F32)
            latent = packed[:, :KV_LATENT]
            scale = lax.rsqrt(jnp.mean(latent * latent, axis=-1, keepdims=True) + EPS)
            normed = (latent * scale).astype(BF16)
            latent_out[pl.ds(at, ROWS), :] = normed
            shared = packed[:, KV_LATENT:]
            shared_square = jnp.sum(shared * shared, axis=-1, keepdims=True)
            cosine, sine = at_block(inside[0, x, slot], inside[1, x, slot], start_cos, start_sin)
            turned = turn(shared * rotary_gain, cosine, sine)
            plain = dot(normed, key_up[...])
            for head in range(HEADS):
                part = plain[:, head * LANES : (head + 1) * LANES]
                square = jnp.sum(part * part, axis=-1, keepdims=True) + shared_square
                factor = lax.rsqrt(square * (1.0 / QK_DIM) + EPS)
                keys_out[head, pl.ds(at, ROWS), :] = (
                    (part * plain_gain + turned) * factor
                ).astype(BF16)
        return carry

    lax.fori_loop(0, jnp.minimum((z // 2) * 2 + 2, BLOCKS), one, 0)


def attend_kernel(coords, queries, keys, latents, value_up, out, sums, totals):
    z, x, p = coords[0], coords[1], coords[2]
    factor = math.log2(math.e) / math.sqrt(QK_DIM)
    wide = 4 * ROWS

    def chunk(at, mask, first):
        at = pl.multiple_of(at, wide)
        latent = latents[pl.ds(at, wide), :]
        for head in range(HEADS):
            scores = dot(queries[head], keys[head, pl.ds(at, wide), :], ((1,), (1,)))
            weights = jnp.exp2(scores * factor)
            if mask is not None:
                weights = jnp.where(mask, weights, 0.0)
            part = weights[:, :LANES] + weights[:, LANES:]
            numer = dot(weights.astype(BF16), latent)
            if first:
                totals[head] = part
                sums[head] = numer
            else:
                totals[head] += part
                sums[head] += numer

    pair = z // 2
    row = lax.broadcasted_iota(jnp.int32, (QROWS, wide), 0)
    col = lax.broadcasted_iota(jnp.int32, (QROWS, wide), 1)
    query_pos = z * BLOCK + (row // ROWS) * (2 * ROWS) + p * ROWS + row % ROWS
    key_pos = (2 * pair + col // (2 * ROWS)) * BLOCK + x * (2 * ROWS) + col % (2 * ROWS)
    chunk(pair * wide, key_pos <= query_pos, True)

    def body(index, carry):
        chunk(index * wide, None, False)
        return carry

    lax.fori_loop(0, pair, body, 0)
    ones = jnp.ones((HALO, LANES), F32)
    line = lax.broadcasted_iota(jnp.int32, (HALO, QROWS), 0)
    for chip in range(CHIPS):
        tail = jnp.zeros((HALO, QROWS), F32)
        for slot in range(2):
            head = 2 * chip + slot
            values = value_up[:, head * VALUE_DIM : (head + 1) * VALUE_DIM]
            numer = dot(sums[head].astype(BF16), values)
            out[chip, :QROWS, slot * LANES : (slot + 1) * LANES] = numer.astype(BF16)
            denom = dot(ones, totals[head], ((1,), (1,)), lax.Precision.HIGHEST)
            high = denom.astype(BF16).astype(F32)
            tail = jnp.where(line == 2 * slot, high, tail)
            tail = jnp.where(line == 2 * slot + 1, denom - high, tail)
        out[chip, QROWS:, :] = tail.astype(BF16)


def pool_kernel(coords, pool_rows, halo, first_halo, weights, own, other, pooled_out, squares_out):
    z, p = coords[0], coords[2]
    lane = lax.broadcasted_iota(jnp.int32, (1, LANES), 1)
    row = lax.broadcasted_iota(jnp.int32, (ROWS, 1), 0)
    squares = jnp.zeros((QROWS, LANES), F32)
    for slot in range(2):
        scale = jnp.where(p == slot, own[0:1, :], other[0:1, :])
        small, large = (2, 4) if slot == 0 else (8, 16)
        window = jnp.where(lane < GROUP_DIM, small, large).astype(F32)
        means = []
        for chip in range(CHIPS):
            current = pool_rows[slot, chip * ROWS : (chip + 1) * ROWS, :].astype(F32)
            index = jnp.where(p == 1, chip, max(chip - 1, 0))
            before = halo[slot, index].astype(F32)
            if chip == 0:
                before = jnp.where(p == 1, before, first_halo[slot].astype(F32))
            total = jnp.concatenate([before, current], axis=0)
            reach = 1
            while reach < small:
                total = total + pltpu.roll(total, reach, 0)
                reach *= 2
            longer = total + pltpu.roll(total, reach, 0)
            total = jnp.where(lane < GROUP_DIM, total, longer)[HALO:]
            position = (z * BLOCK + chip * 2 * ROWS + p * ROWS + row).astype(F32)
            divisor = jnp.minimum(position + 1.0, window)
            means.append((total / divisor - current).astype(BF16))
        pooled = dot(jnp.concatenate(means, axis=0), weights[slot]) * scale
        pooled_out[slot] = pooled
        squares = squares + pooled * pooled
    squares_out[...] = squares


def join_kernel(parts, pool_squares, attended_out, squares_out):
    tail = jnp.zeros((HALO, QROWS), F32)
    for chip in range(CHIPS):
        tail = tail + parts[chip, QROWS:, :].astype(F32)
    columns = jnp.transpose(tail)
    squares = jnp.zeros((QROWS, LANES), F32)
    for slot in range(2):
        numer = jnp.zeros((QROWS, LANES), F32)
        for chip in range(CHIPS):
            numer = numer + parts[chip, :QROWS, slot * LANES : (slot + 1) * LANES].astype(F32)
        denom = columns[:, 2 * slot : 2 * slot + 1] + columns[:, 2 * slot + 1 : 2 * slot + 2]
        attended = numer / denom
        attended_out[slot] = attended
        squares = squares + attended * attended
    ones = jnp.ones((8, LANES), F32)
    exact = lax.Precision.HIGHEST
    line = lax.broadcasted_iota(jnp.int32, (8, QROWS), 0)
    mine = dot(ones, squares, ((1,), (1,)), exact)
    pools = dot(ones, pool_squares[...], ((1,), (1,)), exact)
    for chip in range(CHIPS):
        squares_out[chip] = jnp.where(line < 4, mine, pools)


def mix_kernel(
    coords, attended, pooled, squares, own_gain, other_gain, own_out, other_out, partial_out
):
    p = coords[2]
    total = jnp.transpose(squares[0] + squares[1] + squares[2] + squares[3])
    attention_factor = lax.rsqrt(total[:, 0:1] * (1.0 / (HEADS * VALUE_DIM)) + EPS)
    pool_factor = lax.rsqrt(total[:, 4:5] * (1.0 / (HEADS * VALUE_DIM)) + EPS)
    sides = []
    for gain, slot in ((own_gain, p), (other_gain, 1 - p)):
        sides.append(
            jnp.concatenate(
                [
                    (attended[slot] * attention_factor * gain[1:2, :]).astype(BF16),
                    (pooled[slot] * pool_factor * gain[2:3, :]).astype(BF16),
                ],
                axis=1,
            )
        )
    step = 512
    for at in range(0, D, step):
        both = dot(sides[0], own_out[:, at : at + step])
        both = both + dot(sides[1], other_out[:, at : at + step])
        partial_out[:, :, at : at + step] = both.astype(BF16).reshape(CHIPS, ROWS, step)


def sum_kernel(parts, out):
    total = parts[0].astype(F32) + parts[1].astype(F32)
    total = total + parts[2].astype(F32) + parts[3].astype(F32)
    out[0] = total.astype(BF16)


def local(
    tokens,
    input_gain,
    query_weight,
    latent_down,
    rotary_down,
    pool_down,
    key_up,
    value_up,
    query_gain,
    key_gain,
    pool_weight,
    pool_scale,
    attention_gain,
    pool_gain,
    attention_out,
    pool_out,
):
    member = lax.axis_index("tp")
    z = lax.axis_index("sp")
    x = member // 2
    coords = jnp.stack([z, x, member % 2]).astype(jnp.int32)
    inside, starts = (jnp.asarray(t) for t in angle_tables())
    pad = LANES - QK_DIM

    own_down = jnp.concatenate(
        [query_weight, jnp.zeros((D, pad), BF16), pool_down], axis=1
    )
    other_down = to_partner(own_down)
    rotary_wide = jnp.pad(rotary_down, ((0, 0), (NOPE_DIM, pad)))
    normed, latent_rows = whole(
        norm_kernel,
        (
            jax.ShapeDtypeStruct((CHIPS, ROWS, D), BF16),
            jax.ShapeDtypeStruct((ROWS, LAT), BF16),
        ),
        tokens,
        input_gain[None],
        latent_down,
        rotary_wide,
        smem=0,
        name="norm",
    )
    rows = among_chips(normed)
    own_latents = lax.all_gather(latent_rows, "sp", axis=0, tiled=False)
    other_latents = to_partner(own_latents)

    queries, pool_rows = whole(
        project_kernel,
        (
            jax.ShapeDtypeStruct((CHIPS, 2, QROWS, LANES), BF16),
            jax.ShapeDtypeStruct((2, QROWS, LANES), BF16),
        ),
        coords,
        rows,
        own_down,
        other_down,
        jnp.pad(query_gain, (0, pad))[None],
        inside,
        starts,
        name="project",
    )
    queries = among_chips(queries).reshape(HEADS, QROWS, LANES)

    key_wide = jnp.pad(
        key_up.reshape(KV_LATENT, HEADS, NOPE_DIM), ((0, 0), (0, 0), (0, LANES - NOPE_DIM))
    ).reshape(KV_LATENT, HEADS * LANES)
    keys, latents = whole(
        expand_kernel,
        (
            jax.ShapeDtypeStruct((HEADS, KEYS, LANES), BF16),
            jax.ShapeDtypeStruct((KEYS, KV_LATENT), BF16),
        ),
        coords,
        own_latents,
        other_latents,
        key_wide,
        jnp.pad(key_gain, (0, pad))[None],
        inside,
        starts,
        name="expand",
    )
    numer = whole(
        attend_kernel,
        jax.ShapeDtypeStruct((CHIPS, QROWS + HALO, 2 * LANES), BF16),
        coords,
        queries,
        keys,
        latents,
        value_up,
        scratch=(
            pltpu.VMEM((HEADS, QROWS, KV_LATENT), F32),
            pltpu.VMEM((HEADS, QROWS, LANES), F32),
        ),
        name="attend",
    )
    parts = among_chips(numer)

    tails = pool_rows.reshape(2, CHIPS, ROWS, LANES)[:, :, ROWS - HALO :]
    halo = to_partner(tails)
    width = 2 * CHIPS
    steps = [
        (block * width + 2 * chip + 1, (block + 1) * width + 2 * chip)
        for block in range(BLOCKS - 1)
        for chip in range(CHIPS)
    ]
    first_halo = lax.ppermute(tails[:, CHIPS - 1], ("sp", "tp"), steps)
    own_gain = jnp.stack([pool_scale, attention_gain, pool_gain])
    other_gain = to_partner(own_gain)
    own_out = jnp.concatenate([attention_out, pool_out], axis=0)
    other_out = to_partner(own_out)
    maps = lax.dynamic_slice_in_dim(pool_weight, x * 4, 4, 0).reshape(2, 2, GROUP_DIM, GROUP_DIM)
    same = jnp.eye(2, dtype=BF16)[None, :, None, :, None]
    maps = (maps[:, :, :, None, :] * same).reshape(2, LANES, LANES)
    pooled, pool_squares = whole(
        pool_kernel,
        (
            jax.ShapeDtypeStruct((2, QROWS, LANES), F32),
            jax.ShapeDtypeStruct((QROWS, LANES), F32),
        ),
        coords,
        pool_rows,
        halo,
        first_halo,
        maps,
        own_gain,
        other_gain,
        name="pool",
    )
    attended, squares = whole(
        join_kernel,
        (
            jax.ShapeDtypeStruct((2, QROWS, LANES), F32),
            jax.ShapeDtypeStruct((CHIPS, 8, QROWS), F32),
        ),
        parts,
        pool_squares,
        smem=0,
        name="join",
    )
    squares = among_chips(squares)
    partial = whole(
        mix_kernel,
        jax.ShapeDtypeStruct((CHIPS, ROWS, D), BF16),
        coords,
        attended,
        pooled,
        squares,
        own_gain,
        other_gain,
        own_out,
        other_out,
        name="mix",
    )
    return whole(
        sum_kernel, jax.ShapeDtypeStruct((1, ROWS, D), BF16), among_chips(partial), smem=0, name="sum"
    )


def solution(mesh):
    placed = (
        P("fs", ("sp", "tp"), None),
        P(),
        P(None, "tp"),
        P(),
        P(),
        P(None, "tp"),
        P(),
        P(),
        P(),
        P(),
        P(),
        P("tp"),
        P("tp"),
        P("tp"),
        P("tp", None),
        P("tp", None),
    )
    return jax.shard_map(
        local, mesh=mesh, in_specs=placed, out_specs=P("fs", ("sp", "tp"), None), check_vma=False
    )
```

time: 221 us -> 144 us (0.65)
  waiting for transfers between devices: 74 us -> 9.63 us
  matrix products: 50.4 us -> 0 us
  Pallas kernels: 0 us -> 39.5 us
  starting transfers between devices: 5.63 us -> 29.3 us
  local copies, waits for them, and re-layouts: 28.3 us -> 12.8 us
  between operations: 13.8 us -> 0.29 us
  blocking collectives: 39.1 us -> 47.6 us
  other arithmetic: 7.48 us -> 2.64 us
    dot_general x41 -> x0, matrix products: 50.4 us -> none  [the longest x16 20.7 us: attend(): jnp.einsum('qhd,khd->hqk', queries, keys, preferred_element_type=jnp.floa...]
    all_gather x1 -> x0, waiting for transfers between devices: 43.5 us -> none  [side_by_side(): lax.all_gather(both, axis, axis=dim, tiled=True)]
    pallas_call x0 -> x8, Pallas kernels: none -> 39.5 us  [whole(): pl.pallas_call(kernel, out_shape=out_shape, in_specs=specs, out_specs=out...]
    all_gather x0 -> x1, blocking collectives: none -> 30.5 us  [local(): own_latents = lax.all_gather(latent_rows, 'sp', axis=0, tiled=False)]
    all_to_all x2 -> x1, blocking collectives: 39.2 us -> 17.1 us  [among_chips(): lax.all_to_all(array, 'tp', 0, 0, axis_index_groups=SAME_CORE, tiled=True)]
    all_to_all x1 -> x4, waiting for transfers between devices: 27.1 us -> 6.58 us  [among_chips(): lax.all_to_all(array, 'tp', 0, 0, axis_index_groups=SAME_CORE, tiled=True)]
    slice x18 -> x1, local copies, waits for them, and re-layouts: 17.5 us -> 0.76 us  [local(): tails = pool_rows.reshape(2, CHIPS, ROWS, LANES)[:, :, ROWS - HALO:]]
    all_to_all x1 -> x4, starting transfers between devices: 4.3 us -> 17.5 us  [among_chips(): lax.all_to_all(array, 'tp', 0, 0, axis_index_groups=SAME_CORE, tiled=True)]
  transfers between devices with their start and end apart: 3 -> 10, of which waited for: 3 -> 3; matrix products, arithmetic and copies ran while one was open for 11% -> 6% of each run, Pallas kernels for 0% -> 22%
where the time goes in v1:
time: 144 us; the launch traced here: 142 us
  blocking collectives  47.6 us (33%)
  Pallas kernels  39.5 us (27%)
  starting transfers between devices  29.3 us (20%)
  local copies, waits for them, and re-layouts  12.8 us (9%)
  waiting for transfers between devices  9.63 us (7%)
  other arithmetic  2.64 us (2%)
    pallas_call x8, Pallas kernels, whole(): pl.pallas_call(kernel, out_shape=out_shape, in_specs=specs, out_specs=out...  39.5 us
    all_gather x1, blocking collectives, local(): own_latents = lax.all_gather(latent_rows, 'sp', axis=0, tiled=False)  30.5 us
    all_to_all x4, starting transfers between devices, among_chips(): lax.all_to_all(array, 'tp', 0, 0, axis_index_groups=SAME_CORE, tiled=True)  17.5 us
    all_to_all x1, blocking collectives, among_chips(): lax.all_to_all(array, 'tp', 0, 0, axis_index_groups=SAME_CORE, tiled=True)  17.1 us
    ppermute x5, starting transfers between devices, to_partner(): return lax.ppermute(array, 'tp', [(i, i ^ 1) for i in range(2 * CHIPS)])  10.5 us
    unnamed x46, local copies, waits for them, and re-layouts  6.91 us
    all_to_all x4, waiting for transfers between devices, among_chips(): lax.all_to_all(array, 'tp', 0, 0, axis_index_groups=SAME_CORE, tiled=True)  6.58 us
    ppermute x1, waiting for transfers between devices, local(): first_halo = lax.ppermute(tails[:, CHIPS - 1], ('sp', 'tp'), steps)  3.03 us
  transfers between devices with their start and end apart: 10, of which 3 were waited for; matrix products, arithmetic and copies ran while one was open for 6% of the time, Pallas kernels for 22%

profile of v1, /device:TPU:480, one launch (start us, length us, event | category | flops | bytes accessed | tf_op | source)
XLA Modules:
  0.0 141.7 jit_solution(432954370407425276)
XLA Ops:
  0.0 1.2 copy.22
  2.2 2.7 %norm.1 = (bf16[4,64,2048]{2,1,0:T(8,128)(2,1)}, bf16[64,384]{1,0:T(8,128)(2,1)}) custom-call(bf16[1,64,2048]{2,1,0:T(8,128)(2,1)} %tokens.1, f32[1,2048]{1,0:T(1,128)} %bitcast.29, bf16[2048,256]{1,0:T(8,128)(2,1)} %latent_down.1, bf16[2048,128]{1,0:T(8,128)(2,1)} %pad.15.rotary_down), custom_call_target="tpu_custom_call" | custom-call | tf_op jit(solution)/shard_map/norm/pallas_call | solution.py:63
  4.9 4.4 %all-to-all-start = ((bf16[4,64,2048]{2,1,0:T(8,128)(2,1)}), bf16[4,64,2048]{2,1,0:T(8,128)(2,1)S(1)}, u32[]{:S(2)}, u32[]{:S(2)}) async-start(bf16[4,64,2048]{2,1,0:T(8,128)(2,1)} %get-tuple-element.15), calls=%async_computation | async-start | bytes 2097152 | tf_op jit(solution)/shard_map/all_to_all | solution.py:50
  9.8 1.3 pad_maximum_fusion.own
  11.1 1.9 %collective-permute-start = (bf16[2048,256]{1,0:T(8,128)(2,1)S(1)}, bf16[2048,256]{1,0:T(8,128)(2,1)}, u32[]{:S(2)}, u32[]{:S(2)}) collective-permute-start(bf16[2048,256]{1,0:T(8,128)(2,1)S(1)} %pad_maximum_fusion.own), channel_id=1, source_target_pairs={{0,1},{1,0},{2,3},{3,2},{4,5},{5,4},{6,7},{7,6},{8,9},{9,8},{10,11... | collective-permute-start | bytes 3145736 | tf_op jit(solution)/shard_map/ppermute | solution.py:54
  13.1 30.5 %all-gather = bf16[1024,384]{1,0:T(8,128)(2,1)S(1)} all-gather(bf16[64,384]{1,0:T(8,128)(2,1)S(1)} %copy-done.11), channel_id=2, replica_groups=mesh['sp'=16,'fs'=4,'tp'=8] {'sp'}, dimensions={0}, use_global_device_ids=true | all-gather | bytes 835584 | tf_op jit(solution)/shard_map/all_gather | solution.py:337
  43.5 1.9 %collective-permute-start.1 = (bf16[16,64,384]{2,1,0:T(8,128)(2,1)S(1)}, bf16[16,64,384]{2,1,0:T(8,128)(2,1)}, u32[]{:S(2)}, u32[]{:S(2)}) collective-permute-start(bf16[16,64,384]{2,1,0:T(8,128)(2,1)S(1)} %bitcast.21), channel_id=1, source_target_pairs={{0,1},{1,0},{2,3},{3,2},{4,5},{5,4},{6,7},{7,6},{8,9},{9,8},{10,11... | collective-permute-start | bytes 2359304 | tf_op jit(solution)/shard_map/ppermute | solution.py:54
  47.1 2.4 %collective-permute-start.5 = (bf16[256,2048]{1,0:T(8,128)(2,1)}, bf16[256,2048]{1,0:T(8,128)(2,1)}, u32[]{:S(2)}, u32[]{:S(2)}) collective-permute-start(bf16[256,2048]{1,0:T(8,128)(2,1)} %constant_dynamic-update-slice_fusion.own_out), channel_id=1, source_target_pairs={{0,1},{1,0},{2,3},{3,2},{4,5},{5,4},{6,7},{7,6},{8,9},{9,8},{10,11... | collective-permute-start | bytes 3145736 | tf_op jit(solution)/shard_map/ppermute | solution.py:54
  51.7 3.8 %project.1 = (bf16[4,2,256,128]{3,2,1,0:T(8,128)(2,1)}, bf16[2,256,128]{2,1,0:T(8,128)(2,1)}) custom-call(s32[3]{0:T(128)} %pad_add_fusion.coords, bf16[4,64,2048]{2,1,0:T(8,128)(2,1)} %copy-done.2, bf16[2048,256]{1,0:T(8,128)(2,1)} %copy-done.1, bf16[2048,256]{1,0:T(8,128)(2,1)} %collective-permute-done.other, f32[1,128]{1,0:T(1,128)} %pad_bitcast_fusion.1.gain, ...), custom_call_target="tpu_custom_call" | custom-call | tf_op jit(solution)/shard_map/project/pallas_call | solution.py:63
  55.5 4.6 %all-to-all-start.1 = ((bf16[4,2,256,128]{3,2,1,0:T(8,128)(2,1)}), bf16[4,2,256,128]{3,2,1,0:T(8,128)(2,1)S(1)}, u32[]{:S(2)}, u32[]{:S(2)}) async-start(bf16[4,2,256,128]{3,2,1,0:T(8,128)(2,1)} %get-tuple-element.16), calls=%async_computation.1 | async-start | bytes 1048576 | tf_op jit(solution)/shard_map/all_to_all | solution.py:50
  60.1 1.9 %collective-permute-start.4 = (f32[3,128]{1,0:T(4,128)S(1)}, f32[3,128]{1,0:T(4,128)S(1)}, u32[]{:S(2)}, u32[]{:S(2)}) collective-permute-start(f32[3,128]{1,0:T(4,128)S(1)} %pad_maximum_fusion.1.own.own_gain), channel_id=1, source_target_pairs={{0,1},{1,0},{2,3},{3,2},{4,5},{5,4},{6,7},{7,6},{8,9},{9,8},{10,11... | collective-permute-start | bytes 4616 | tf_op jit(solution)/shard_map/ppermute | solution.py:54
  64.2 11.7 %expand.1 = (bf16[8,2048,128]{2,1,0:T(8,128)(2,1)}, bf16[2048,256]{1,0:T(8,128)(2,1)}) custom-call(s32[3]{0:T(128)} %pad_add_fusion.coords, bf16[16,64,384]{2,1,0:T(8,128)(2,1)} %bitcast.22, bf16[16,64,384]{2,1,0:T(8,128)(2,1)} %collective-permute-done.1.other, bf16[256,1024]{1,0:T(8,128)(2,1)} %copy.27.key_up, f32[1,128]{1,0:T(1,128)} %pad_bitcast_fusion.gain, ...), custom_call_target="tpu_custom_call" | custom-call | tf_op jit(solution)/shard_map/expand/pallas_call | solution.py:63
  76.6 2.4 %collective-permute-start.2 = (bf16[2,4,16,128]{3,2,1,0:T(8,128)(2,1)S(1)}, bf16[2,4,16,128]{3,2,1,0:T(8,128)(2,1)S(1)}, u32[]{:S(2)}, u32[]{:S(2)}) collective-permute-start(bf16[2,4,16,128]{3,2,1,0:T(8,128)(2,1)S(1)} %slice.9), channel_id=1, source_target_pairs={{0,1},{1,0},{2,3},{3,2},{4,5},{5,4},{6,7},{7,6},{8,9},{9,8},{10,11... | collective-permute-start | bytes 98312 | tf_op jit(solution)/shard_map/ppermute | solution.py:54
  79.9 11.4 %attend.1 = bf16[4,272,256]{2,1,0:T(8,128)(2,1)} custom-call(s32[3]{0:T(128)} %pad_add_fusion.coords, bf16[8,256,128]{2,1,0:T(8,128)(2,1)} %bitcast.24, bf16[8,2048,128]{2,1,0:T(8,128)(2,1)} %get-tuple-element.18.keys, bf16[2048,256]{1,0:T(8,128)(2,1)} %get-tuple-element.19.latents, bf16[256,1024]{1,0:T(8,128)(2,1)} %value_up.1), custom_call_target="tpu_custom_call" | custom-call | tf_op jit(solution)/shard_map/attend/pallas_call | solution.py:63
  91.3 4.8 %all-to-all-start.2 = ((bf16[4,272,256]{2,1,0:T(8,128)(2,1)}), bf16[4,272,256]{2,1,0:T(8,128)(2,1)S(1)}, u32[]{:S(2)}, u32[]{:S(2)}) async-start(bf16[4,272,256]{2,1,0:T(8,128)(2,1)} %attend.1), calls=%async_computation.2 | async-start | bytes 1114112 | tf_op jit(solution)/shard_map/all_to_all | solution.py:50
  96.8 1.3 collective-permute-start.3
  98.7 3.0 %collective-permute-done.3.first_halo = bf16[2,16,128]{2,1,0:T(8,128)(2,1)S(1)} collective-permute-done((bf16[2,16,128]{2,1,0:T(8,128)(2,1)S(1)}, bf16[2,16,128]{2,1,0:T(8,128)(2,1)S(1)}, u32[]{:S(2)}, u32[]{:S(2)}) %collective-permute-start.3) | collective-permute-done | bytes 8224 | tf_op jit(solution)/shard_map/ppermute | solution.py:399
  103.0 2.0 %pool.1 = (f32[2,256,128]{2,1,0:T(8,128)}, f32[256,128]{1,0:T(8,128)}) custom-call(s32[3]{0:T(128)} %pad_add_fusion.coords, bf16[2,256,128]{2,1,0:T(8,128)(2,1)} %get-tuple-element.20.pool_rows, bf16[2,4,16,128]{3,2,1,0:T(8,128)(2,1)} %copy-done.12, bf16[2,16,128]{2,1,0:T(8,128)(2,1)} %copy-done.15, bf16[2,128,128]{2,1,0:T(8,128)(2,1)} %broadcast_multiply_fusion.weights, ...), custom_call_target="tpu_custom_call" | custom-call | tf_op jit(solution)/shard_map/pool/pallas_call | solution.py:63
  106.9 2.3 %join.1 = (f32[2,256,128]{2,1,0:T(8,128)}, f32[4,8,256]{2,1,0:T(8,128)}) custom-call(bf16[4,272,256]{2,1,0:T(8,128)(2,1)} %copy-done.4, f32[256,128]{1,0:T(8,128)} %get-tuple-element.21.pool_squares), custom_call_target="tpu_custom_call" | custom-call | tf_op jit(solution)/shard_map/join/pallas_call | solution.py:63
  109.2 3.7 %all-to-all-start.3 = ((f32[4,8,256]{2,1,0:T(8,128)}), f32[4,8,256]{2,1,0:T(8,128)S(1)}, u32[]{:S(2)}, u32[]{:S(2)}) async-start(f32[4,8,256]{2,1,0:T(8,128)} %get-tuple-element.24), calls=%async_computation.3 | async-start | bytes 65536 | tf_op jit(solution)/shard_map/all_to_all | solution.py:50
  112.9 5.4 %all-to-all-done.3.squares = f32[4,8,256]{2,1,0:T(8,128)S(1)} async-done(((f32[4,8,256]{2,1,0:T(8,128)}), f32[4,8,256]{2,1,0:T(8,128)S(1)}, u32[]{:S(2)}, u32[]{:S(2)}) %all-to-all-start.3) | async-done | bytes 32800 | tf_op jit(solution)/shard_map/all_to_all | solution.py:50
  118.9 3.6 %mix.1 = bf16[4,64,2048]{2,1,0:T(8,128)(2,1)} custom-call(s32[3]{0:T(128)} %pad_add_fusion.coords, f32[2,256,128]{2,1,0:T(8,128)} %get-tuple-element.22.attended, f32[2,256,128]{2,1,0:T(8,128)} %get-tuple-element.23.pooled, f32[4,8,256]{2,1,0:T(8,128)} %copy-done.10, f32[3,128]{1,0:T(4,128)} %copy-done.13, f32[3,128]{1,0:T(4,128)} %copy-done.14, ...), custom_call_target="tpu_custom_call" | custom-call | tf_op jit(solution)/shard_map/mix/pallas_call | solution.py:63
  122.5 17.1 %all_to_all.25.parts = bf16[4,64,2048]{2,1,0:T(8,128)(2,1)} all-to-all(bf16[4,64,2048]{2,1,0:T(8,128)(2,1)} %mix.1), channel_id=1, replica_groups={{0,2,4,6},{1,3,5,7},{8,10,12,14},{9,11,13,15},{16,18,20,22},{17,19,21,2..., dimensions={0} | all-to-all | bytes 2097152 | tf_op jit(solution)/shard_map/all_to_all | solution.py:50
  139.6 2.1 %sum.1 = bf16[1,64,2048]{2,1,0:T(8,128)(2,1)} custom-call(bf16[4,64,2048]{2,1,0:T(8,128)(2,1)} %all_to_all.25.parts), custom_call_target="tpu_custom_call" | custom-call | tf_op jit(solution)/shard_map/sum/pallas_call | solution.py:63
  (72 shorter events, 14.0 us)
Async XLA Ops:
  0.0 63.2 %copy-start = (bf16[16,64,64]{2,1,0:T(8,128)(2,1)S(1)}, bf16[16,64,64]{2,1,0:T(8,128)(2,1)}, u32[]{:S(2)}) copy-start(bf16[16,64,64]{2,1,0:T(8,128)(2,1)} %param.28) | copy-start | bytes 393220
  2.2 7.1 %copy-start.8 = (bf16[2048,96]{0,1:T(8,128)(2,1)S(1)}, bf16[2048,96]{0,1:T(8,128)(2,1)}, u32[]{:S(2)}) copy-start(bf16[2048,96]{0,1:T(8,128)(2,1)} %param.20) | copy-start | bytes 1179652
  4.9 8.1 %copy-start.11 = (bf16[64,384]{1,0:T(8,128)(2,1)S(1)}, bf16[64,384]{1,0:T(8,128)(2,1)}, u32[]{:S(2)}) copy-start(bf16[64,384]{1,0:T(8,128)(2,1)} %get-tuple-element.17) | copy-start | bytes 147460
  4.9 45.8 %all-to-all-start = ((bf16[4,64,2048]{2,1,0:T(8,128)(2,1)}), bf16[4,64,2048]{2,1,0:T(8,128)(2,1)S(1)}, u32[]{:S(2)}, u32[]{:S(2)}) async-start(bf16[4,64,2048]{2,1,0:T(8,128)(2,1)} %get-tuple-element.15), calls=%async_computation | async-start | bytes 2097152 | tf_op jit(solution)/shard_map/all_to_all | solution.py:50
  9.6 35.8 %copy-start.6 = (bf16[128,2048]{1,0:T(8,128)(2,1)S(1)}, bf16[128,2048]{1,0:T(8,128)(2,1)}, u32[]{:S(2)}) copy-start(bf16[128,2048]{1,0:T(8,128)(2,1)} %param.32) | copy-start | bytes 1572868
  9.7 36.6 %copy-start.7 = (bf16[128,2048]{1,0:T(8,128)(2,1)S(1)}, bf16[128,2048]{1,0:T(8,128)(2,1)}, u32[]{:S(2)}) copy-start(bf16[128,2048]{1,0:T(8,128)(2,1)} %param.33) | copy-start | bytes 1572868
  9.8 39.7 %copy-start.19 = (f32[96]{0:T(128)S(1)}, f32[96]{0:T(128)}, u32[]{:S(2)}) copy-start(f32[96]{0:T(128)} %param.26) | copy-start | bytes 1156
  11.1 39.6 %copy-start.1 = (bf16[2048,256]{1,0:T(8,128)(2,1)}, bf16[2048,256]{1,0:T(8,128)(2,1)S(1)}, u32[]{:S(2)}) copy-start(bf16[2048,256]{1,0:T(8,128)(2,1)S(1)} %pad_maximum_fusion.own) | copy-start | bytes 3145732
  11.1 39.6 %collective-permute-start = (bf16[2048,256]{1,0:T(8,128)(2,1)S(1)}, bf16[2048,256]{1,0:T(8,128)(2,1)}, u32[]{:S(2)}, u32[]{:S(2)}) collective-permute-start(bf16[2048,256]{1,0:T(8,128)(2,1)S(1)} %pad_maximum_fusion.own), channel_id=1, source_target_pairs={{0,1},{1,0},{2,3},{3,2},{4,5},{5,4},{6,7},{7,6},{8,9},{9,8},{10,11... | collective-permute-start | bytes 3145736 | tf_op jit(solution)/shard_map/ppermute | solution.py:54
  43.5 12.0 %copy-start.3 = (bf16[1024,384]{1,0:T(8,128)(2,1)}, bf16[1024,384]{1,0:T(8,128)(2,1)S(1)}, u32[]{:S(2)}) copy-start(bf16[1024,384]{1,0:T(8,128)(2,1)S(1)} %all-gather) | copy-start | bytes 2359300
  43.5 20.7 %collective-permute-start.1 = (bf16[16,64,384]{2,1,0:T(8,128)(2,1)S(1)}, bf16[16,64,384]{2,1,0:T(8,128)(2,1)}, u32[]{:S(2)}, u32[]{:S(2)}) collective-permute-start(bf16[16,64,384]{2,1,0:T(8,128)(2,1)S(1)} %bitcast.21), channel_id=1, source_target_pairs={{0,1},{1,0},{2,3},{3,2},{4,5},{5,4},{6,7},{7,6},{8,9},{9,8},{10,11... | collective-permute-start | bytes 2359304 | tf_op jit(solution)/shard_map/ppermute | solution.py:54
  47.1 65.8 %collective-permute-start.5 = (bf16[256,2048]{1,0:T(8,128)(2,1)}, bf16[256,2048]{1,0:T(8,128)(2,1)}, u32[]{:S(2)}, u32[]{:S(2)}) collective-permute-start(bf16[256,2048]{1,0:T(8,128)(2,1)} %constant_dynamic-update-slice_fusion.own_out), channel_id=1, source_target_pairs={{0,1},{1,0},{2,3},{3,2},{4,5},{5,4},{6,7},{7,6},{8,9},{9,8},{10,11... | collective-permute-start | bytes 3145736 | tf_op jit(solution)/shard_map/ppermute | solution.py:54
  50.7 9.4 %copy-start.16 = (f32[128]{0:T(128)S(1)}, f32[128]{0:T(128)}, u32[]{:S(2)}) copy-start(f32[128]{0:T(128)} %param.31) | copy-start | bytes 1540
  50.7 9.4 %copy-start.17 = (f32[128]{0:T(128)S(1)}, f32[128]{0:T(128)}, u32[]{:S(2)}) copy-start(f32[128]{0:T(128)} %param.30) | copy-start | bytes 1540
  50.7 9.4 %copy-start.18 = (f32[128]{0:T(128)S(1)}, f32[128]{0:T(128)}, u32[]{:S(2)}) copy-start(f32[128]{0:T(128)} %param.29) | copy-start | bytes 1540
  50.7 11.3 %copy-start.9 = (bf16[256,512]{1,0:T(8,128)(2,1)S(1)}, bf16[256,512]{1,0:T(8,128)(2,1)}, u32[]{:S(2)}) copy-start(bf16[256,512]{1,0:T(8,128)(2,1)} %param.24) | copy-start | bytes 786436
  55.5 8.2 %copy-start.20 = (f32[96]{0:T(128)S(1)}, f32[96]{0:T(128)}, u32[]{:S(2)}) copy-start(f32[96]{0:T(128)} %param.27) | copy-start | bytes 1156
  55.5 23.6 %all-to-all-start.1 = ((bf16[4,2,256,128]{3,2,1,0:T(8,128)(2,1)}), bf16[4,2,256,128]{3,2,1,0:T(8,128)(2,1)S(1)}, u32[]{:S(2)}, u32[]{:S(2)}) async-start(bf16[4,2,256,128]{3,2,1,0:T(8,128)(2,1)} %get-tuple-element.16), calls=%async_computation.1 | async-start | bytes 1048576 | tf_op jit(solution)/shard_map/all_to_all | solution.py:50
  60.1 15.8 %copy-start.13 = (f32[3,128]{1,0:T(4,128)}, f32[3,128]{1,0:T(4,128)S(1)}, u32[]{:S(2)}) copy-start(f32[3,128]{1,0:T(4,128)S(1)} %pad_maximum_fusion.1.own.own_gain) | copy-start | bytes 4612
  60.1 38.6 %collective-permute-start.4 = (f32[3,128]{1,0:T(4,128)S(1)}, f32[3,128]{1,0:T(4,128)S(1)}, u32[]{:S(2)}, u32[]{:S(2)}) collective-permute-start(f32[3,128]{1,0:T(4,128)S(1)} %pad_maximum_fusion.1.own.own_gain), channel_id=1, source_target_pairs={{0,1},{1,0},{2,3},{3,2},{4,5},{5,4},{6,7},{7,6},{8,9},{9,8},{10,11... | collective-permute-start | bytes 4616 | tf_op jit(solution)/shard_map/ppermute | solution.py:54
  76.6 25.2 %collective-permute-start.2 = (bf16[2,4,16,128]{3,2,1,0:T(8,128)(2,1)S(1)}, bf16[2,4,16,128]{3,2,1,0:T(8,128)(2,1)S(1)}, u32[]{:S(2)}, u32[]{:S(2)}) collective-permute-start(bf16[2,4,16,128]{3,2,1,0:T(8,128)(2,1)S(1)} %slice.9), channel_id=1, source_target_pairs={{0,1},{1,0},{2,3},{3,2},{4,5},{5,4},{6,7},{7,6},{8,9},{9,8},{10,11... | collective-permute-start | bytes 98312 | tf_op jit(solution)/shard_map/ppermute | solution.py:54
  91.3 14.8 %all-to-all-start.2 = ((bf16[4,272,256]{2,1,0:T(8,128)(2,1)}), bf16[4,272,256]{2,1,0:T(8,128)(2,1)S(1)}, u32[]{:S(2)}, u32[]{:S(2)}) async-start(bf16[4,272,256]{2,1,0:T(8,128)(2,1)} %attend.1), calls=%async_computation.2 | async-start | bytes 1114112 | tf_op jit(solution)/shard_map/all_to_all | solution.py:50
  96.8 5.0 %collective-permute-start.3 = (bf16[2,16,128]{2,1,0:T(8,128)(2,1)S(1)}, bf16[2,16,128]{2,1,0:T(8,128)(2,1)S(1)}, u32[]{:S(2)}, u32[]{:S(2)}) collective-permute-start(bf16[2,16,128]{2,1,0:T(8,128)(2,1)S(1)} %slice_bitcast_fusion), channel_id=1, source_target_pairs={{1,32},{3,34},{5,36},{7,38},{33,64},{35,66},{37,68},{39,70},{65,96... | collective-permute-start | bytes 24584 | tf_op jit(solution)/shard_map/ppermute | solution.py:399
  109.2 9.1 %all-to-all-start.3 = ((f32[4,8,256]{2,1,0:T(8,128)}), f32[4,8,256]{2,1,0:T(8,128)S(1)}, u32[]{:S(2)}, u32[]{:S(2)}) async-start(f32[4,8,256]{2,1,0:T(8,128)} %get-tuple-element.24), calls=%async_computation.3 | async-start | bytes 65536 | tf_op jit(solution)/shard_map/all_to_all | solution.py:50
  (7 other events, 7.5 us)

commit v2 on v1

v2 whole, which is shorter than its diff:
```python
import math

import jax
import jax.numpy as jnp
import numpy as np
from jax import lax
from jax.experimental import pallas as pl
from jax.experimental.pallas import tpu as pltpu
from jax.sharding import PartitionSpec as P

HEADS = 8
NOPE_DIM = 64
ROPE_DIM = 32
VALUE_DIM = 128
KV_LATENT = 256
GROUP_DIM = 64
QK_DIM = 96
D = 2048
BLOCKS = 16
BLOCK = 512
CHIPS = 4
ROWS = 64
LANES = 128
QROWS = CHIPS * ROWS
KEYS = BLOCKS * 2 * ROWS
HALO = 16
LAT = 384

EPS = 1e-06
THETA = 10000.0
SAME_CORE = [[0, 2, 4, 6], [1, 3, 5, 7]]
F32 = jnp.float32
BF16 = jnp.bfloat16


def angle_tables():
    half = ROPE_DIM // 2
    freq = np.zeros(LANES)
    inv = 1.0 / THETA ** (np.arange(half, dtype=np.float64) / half)
    freq[NOPE_DIM : NOPE_DIM + half] = inv
    freq[NOPE_DIM + half : QK_DIM] = inv
    inside = np.arange(BLOCK)[:, None] * freq[None, :]
    starts = (np.arange(BLOCKS) * BLOCK)[:, None] * freq[None, :]
    inside = np.stack([np.cos(inside), np.sin(inside)]).astype(np.float32)
    starts = np.stack([np.cos(starts), np.sin(starts)]).astype(np.float32)
    return inside.reshape(2, CHIPS, 2, ROWS, LANES), starts


def among_chips(array):
    return lax.all_to_all(array, "tp", 0, 0, axis_index_groups=SAME_CORE, tiled=True)


def to_partner(array):
    return lax.ppermute(array, "tp", [(i, i ^ 1) for i in range(2 * CHIPS)])


MIB = 1024 * 1024
VECTOR = pl.BlockSpec(memory_space=pltpu.VMEM)
AWAY = pl.BlockSpec(memory_space=pltpu.HBM)
FLAT = 8192
AT_GAINS = 1536
AT_POOL = 2048
AT_OUT = 4096


def whole(kernel, out_shape, *args, specs=None, scratch=(), name=None, room=14):
    single = not isinstance(out_shape, (list, tuple))
    return pl.pallas_call(
        kernel,
        grid=() if specs is None else (1,),
        out_shape=out_shape,
        in_specs=[VECTOR] * len(args) if specs is None else specs,
        out_specs=VECTOR if single else [VECTOR] * len(out_shape),
        scratch_shapes=list(scratch),
        compiler_params=pltpu.CompilerParams(vmem_limit_bytes=room * MIB),
        name=name,
    )(*args)


def place():
    member = lax.axis_index("tp")
    return lax.axis_index("sp"), member // 2, member % 2


def shape(dims, dtype):
    return jax.ShapeDtypeStruct(dims, dtype)


def far(dims, dtype):
    return pltpu.HBM(dims, dtype)


def dot(a, b, dims=((1,), (0,)), precision=None):
    return lax.dot_general(
        a, b, (dims, ((), ())), preferred_element_type=F32, precision=precision
    )


def turn(vectors, cosine, sine):
    lane = lax.broadcasted_iota(jnp.int32, vectors.shape, vectors.ndim - 1)
    half = ROPE_DIM // 2
    ahead = pltpu.roll(vectors, LANES - half, vectors.ndim - 1)
    behind = pltpu.roll(vectors, half, vectors.ndim - 1)
    return vectors * cosine + jnp.where(lane < NOPE_DIM + half, -ahead, behind) * sine


def at_block(inside_cos, inside_sin, start_cos, start_sin):
    cosine = start_cos * inside_cos - start_sin * inside_sin
    sine = start_sin * inside_cos + start_cos * inside_sin
    return cosine, sine


def norm_kernel(tokens, gain, latent_down, rotary_down, normed_out, latent_out):
    source = tokens[0].astype(F32)
    scale = lax.rsqrt(jnp.mean(source * source, axis=-1, keepdims=True) + EPS)
    normed = (source * scale * gain[...]).astype(BF16)
    for chip in range(CHIPS):
        normed_out[chip] = normed
    latent_out[:, :KV_LATENT] = dot(normed, latent_down[...]).astype(BF16)
    above = jnp.zeros((NOPE_DIM, D), BF16)
    below = jnp.zeros((LANES - QK_DIM, D), BF16)
    rotary = jnp.concatenate([above, rotary_down[...], below], axis=0)
    latent_out[:, KV_LATENT:] = dot(normed, rotary, ((1,), (1,))).astype(BF16)


def bundle_kernel(query_t, pool_down, attention_out, pool_out, gains, after, flat):
    for at in range(D // LANES):
        lanes = slice(at * LANES, (at + 1) * LANES)
        flat[at * QK_DIM : (at + 1) * QK_DIM, :] = query_t[:, lanes]
        base = AT_OUT + at * 2 * LANES
        flat[base : base + LANES, :] = attention_out[:, lanes]
        flat[base + LANES : base + 2 * LANES, :] = pool_out[:, lanes]
    flat[AT_POOL:AT_OUT, :] = pool_down[...]
    rest = gains[...]
    rows = []
    for _ in range(3):
        piece = rest.astype(BF16)
        rest = rest - piece.astype(F32)
        rows.append(piece.astype(F32))
    rows.append(jnp.zeros((4, LANES), F32))
    flat[AT_GAINS : AT_GAINS + HALO, :] = jnp.concatenate(rows, axis=0).astype(BF16)


def unbundled_gains(rows):
    rows = rows.astype(F32)
    return rows[0:4] + rows[4:8] + rows[8:12]


def project_kernel(rows, own, other, gain, inside, starts, query_out, token_out):
    z, x, p = place()
    piece = rows[...].reshape(QROWS, D)
    start_cos = starts[0, pl.ds(z, 1), :]
    start_sin = starts[1, pl.ds(z, 1), :]
    inside_cos = jnp.concatenate([inside[0, c, p] for c in range(CHIPS)], axis=0)
    inside_sin = jnp.concatenate([inside[1, c, p] for c in range(CHIPS)], axis=0)
    cosine, sine = at_block(inside_cos, inside_sin, start_cos, start_sin)
    empty = jnp.zeros((LANES - QK_DIM, D), BF16)
    wide_gain = jnp.concatenate([gain[...], jnp.zeros((1, LANES - QK_DIM), F32)], axis=1)
    theirs = jnp.concatenate(
        [other[at * QK_DIM : (at + 1) * QK_DIM, :] for at in range(D // LANES)], axis=1
    )
    for weights, slot in ((own[...], p), (theirs, 1 - p)):
        raw = dot(piece, jnp.concatenate([weights, empty], axis=0), ((1,), (1,)))
        square = jnp.sum(raw * raw, axis=-1, keepdims=True) * (1.0 / QK_DIM)
        normal = raw * lax.rsqrt(square + EPS) * wide_gain
        queries = turn(normal, cosine, sine).astype(BF16)
        for chip in range(CHIPS):
            query_out[chip, slot] = queries
    token_out[...] = cosine[:8]


def pool_project_kernel(rows, own, other, after, pool_out, tails_out, last_out):
    z, x, p = place()
    piece = rows[...].reshape(QROWS, D)
    for weights, slot in ((own, p), (other, 1 - p)):
        result = dot(piece, weights[...]).astype(BF16)
        pool_out[slot] = result
        for chip in range(CHIPS):
            end = (chip + 1) * ROWS
            tails_out[slot, chip] = result[end - HALO : end]
        last_out[slot] = result[QROWS - HALO :]


def expand_kernel(own, other, key_up, gain, inside, starts, keys_out, latent_out):
    z, x, p = place()
    step = pl.program_id(0)

    @pl.when(step <= z // 2)
    def _():
        lane = lax.broadcasted_iota(jnp.int32, (1, LANES), 1)
        wide_gain = jnp.concatenate([gain[...], jnp.zeros((1, LANES - QK_DIM), F32)], axis=1)
        plain_gain = jnp.where(lane < NOPE_DIM, wide_gain, 0.0)
        rotary_gain = jnp.where(lane < NOPE_DIM, 0.0, wide_gain)
        pieces, cosines, sines = [], [], []
        for k in range(2):
            mine, theirs = own[k].astype(F32), other[k].astype(F32)
            pieces += [jnp.where(p == 0, mine, theirs), jnp.where(p == 0, theirs, mine)]
            start_cos = starts[0, pl.ds(2 * step + k, 1), :]
            start_sin = starts[1, pl.ds(2 * step + k, 1), :]
            for c in range(2):
                cosine, sine = at_block(inside[0, 0, c], inside[1, 0, c], start_cos, start_sin)
                cosines.append(cosine)
                sines.append(sine)
        packed = jnp.concatenate(pieces, axis=0)
        cosine = jnp.concatenate(cosines, axis=0)
        sine = jnp.concatenate(sines, axis=0)
        latent = packed[:, :KV_LATENT]
        scale = lax.rsqrt(jnp.mean(latent * latent, axis=-1, keepdims=True) + EPS)
        normed = (latent * scale).astype(BF16)
        latent_out[...] = normed
        shared = packed[:, KV_LATENT:]
        shared_square = jnp.sum(shared * shared, axis=-1, keepdims=True)
        turned = turn(shared * rotary_gain, cosine, sine)
        plain = dot(normed, key_up[...])
        for pair in range(HEADS // 2):
            group = plain[:, pair * LANES : (pair + 1) * LANES]
            for part, head in ((group, 2 * pair), (pltpu.roll(group, NOPE_DIM, 1), 2 * pair + 1)):
                part = jnp.where(lane < NOPE_DIM, part, 0.0)
                square = jnp.sum(part * part, axis=-1, keepdims=True) + shared_square
                factor = lax.rsqrt(square * (1.0 / QK_DIM) + EPS)
                keys_out[head] = ((part * plain_gain + turned) * factor).astype(BF16)


def attend_kernel(
    queries, keys_far, latents_far, value_far, out, keys, latents, value_up, sums, totals, arrived
):
    z, x, p = place()
    factor = math.log2(math.e) / math.sqrt(QK_DIM)
    wide = 4 * ROWS
    pair = z // 2

    def copies(index):
        at = pl.multiple_of(index * wide, wide)
        return (
            pltpu.make_async_copy(
                keys_far.at[:, pl.ds(at, wide), :],
                keys.at[:, pl.ds(at, wide), :],
                arrived.at[0, index],
            ),
            pltpu.make_async_copy(
                latents_far.at[pl.ds(at, wide), :],
                latents.at[pl.ds(at, wide), :],
                arrived.at[1, index],
            ),
        )

    def fetch(index, carry):
        for copy in copies(pair - index):
            copy.start()
        return carry

    lax.fori_loop(0, pair + 1, fetch, 0)
    value_copy = pltpu.make_async_copy(value_far, value_up, arrived.at[0, BLOCKS // 2])
    value_copy.start()

    def chunk(index, mask, first):
        at = pl.multiple_of(index * wide, wide)
        for copy in copies(index):
            copy.wait()
        latent = latents[pl.ds(at, wide), :]
        for head in range(HEADS):
            scores = dot(queries[head], keys[head, pl.ds(at, wide), :], ((1,), (1,)))
            weights = jnp.exp2(scores * factor)
            if mask is not None:
                weights = jnp.where(mask, weights, 0.0)
            part = weights[:, :LANES] + weights[:, LANES:]
            numer = dot(weights.astype(BF16), latent)
            if first:
                totals[head] = part
                sums[head] = numer
            else:
                totals[head] += part
                sums[head] += numer

    row = lax.broadcasted_iota(jnp.int32, (QROWS, wide), 0)
    col = lax.broadcasted_iota(jnp.int32, (QROWS, wide), 1)
    query_pos = z * BLOCK + (row // ROWS) * (2 * ROWS) + p * ROWS + row % ROWS
    key_pos = (2 * pair + col // (2 * ROWS)) * BLOCK + x * (2 * ROWS) + col % (2 * ROWS)
    chunk(pair, key_pos <= query_pos, True)

    def body(index, carry):
        chunk(pair - 1 - index, None, False)
        return carry

    lax.fori_loop(0, pair, body, 0)
    value_copy.wait()
    ones = jnp.ones((HALO, LANES), F32)
    line = lax.broadcasted_iota(jnp.int32, (HALO, QROWS), 0)
    for chip in range(CHIPS):
        tail = jnp.zeros((HALO, QROWS), F32)
        for slot in range(2):
            head = 2 * chip + slot
            values = value_up[:, head * VALUE_DIM : (head + 1) * VALUE_DIM]
            numer = dot(sums[head].astype(BF16), values)
            out[chip, :QROWS, slot * LANES : (slot + 1) * LANES] = numer.astype(BF16)
            denom = dot(ones, totals[head], ((1,), (1,)), lax.Precision.HIGHEST)
            high = denom.astype(BF16).astype(F32)
            tail = jnp.where(line == 2 * slot, high, tail)
            tail = jnp.where(line == 2 * slot + 1, denom - high, tail)
        out[chip, QROWS:, :] = tail.astype(BF16)


def pool_kernel(pool_rows, halo, first_halo, maps, own, other, pooled_out, squares_out):
    z, x, p = place()
    theirs = unbundled_gains(other[...])
    empty = jnp.zeros((GROUP_DIM, GROUP_DIM), F32)
    lane = lax.broadcasted_iota(jnp.int32, (1, LANES), 1)
    row = lax.broadcasted_iota(jnp.int32, (ROWS, 1), 0)
    squares = jnp.zeros((QROWS, LANES), F32)
    for slot in range(2):
        scale = jnp.where(p == slot, own[0:1, :], theirs[0:1, :])
        upper = jnp.concatenate([maps[4 * x + 2 * slot].astype(F32), empty], axis=1)
        lower = jnp.concatenate([empty, maps[4 * x + 2 * slot + 1].astype(F32)], axis=1)
        weights = jnp.concatenate([upper, lower], axis=0).astype(BF16)
        small, large = (2, 4) if slot == 0 else (8, 16)
        window = jnp.where(lane < GROUP_DIM, small, large).astype(F32)
        means = []
        for chip in range(CHIPS):
            current = pool_rows[slot, chip * ROWS : (chip + 1) * ROWS, :].astype(F32)
            index = jnp.where(p == 1, chip, max(chip - 1, 0))
            before = halo[slot, index].astype(F32)
            if chip == 0:
                before = jnp.where(p == 1, before, first_halo[slot].astype(F32))
            total = jnp.concatenate([before, current], axis=0)
            reach = 1
            while reach < small:
                total = total + pltpu.roll(total, reach, 0)
                reach *= 2
            longer = total + pltpu.roll(total, reach, 0)
            total = jnp.where(lane < GROUP_DIM, total, longer)[HALO:]
            position = (z * BLOCK + chip * 2 * ROWS + p * ROWS + row).astype(F32)
            divisor = jnp.minimum(position + 1.0, window)
            means.append((total / divisor - current).astype(BF16))
        pooled = dot(jnp.concatenate(means, axis=0), weights) * scale
        pooled_out[slot] = pooled
        squares = squares + pooled * pooled
    squares_out[...] = squares


def join_kernel(parts, pool_squares, attended_out, squares_out):
    tail = jnp.zeros((HALO, QROWS), F32)
    for chip in range(CHIPS):
        tail = tail + parts[chip, QROWS:, :].astype(F32)
    columns = jnp.transpose(tail)
    squares = jnp.zeros((QROWS, LANES), F32)
    for slot in range(2):
        numer = jnp.zeros((QROWS, LANES), F32)
        for chip in range(CHIPS):
            numer = numer + parts[chip, :QROWS, slot * LANES : (slot + 1) * LANES].astype(F32)
        denom = columns[:, 2 * slot : 2 * slot + 1] + columns[:, 2 * slot + 1 : 2 * slot + 2]
        attended = numer / denom
        attended_out[slot] = attended
        squares = squares + attended * attended
    ones = jnp.ones((8, LANES), F32)
    exact = lax.Precision.HIGHEST
    line = lax.broadcasted_iota(jnp.int32, (8, QROWS), 0)
    mine = dot(ones, squares, ((1,), (1,)), exact)
    pools = dot(ones, pool_squares[...], ((1,), (1,)), exact)
    for chip in range(CHIPS):
        squares_out[chip] = jnp.where(line < 4, mine, pools)


def mix_kernel(
    attended, pooled, squares, own_gain, other_gain, own_attention, own_pool, other_out, partial_out
):
    z, x, p = place()
    total = jnp.transpose(squares[0] + squares[1] + squares[2] + squares[3])
    attention_factor = lax.rsqrt(total[:, 0:1] * (1.0 / (HEADS * VALUE_DIM)) + EPS)
    pool_factor = lax.rsqrt(total[:, 4:5] * (1.0 / (HEADS * VALUE_DIM)) + EPS)
    sides = []
    for gain, slot in ((own_gain[...], p), (unbundled_gains(other_gain[...]), 1 - p)):
        sides.append((attended[slot] * attention_factor * gain[1:2, :]).astype(BF16))
        sides.append((pooled[slot] * pool_factor * gain[2:3, :]).astype(BF16))
    mine = jnp.concatenate(sides[:2], axis=1)
    theirs = jnp.concatenate(sides[2:], axis=1)
    step = 512
    for at in range(0, D, step):
        weights = jnp.concatenate(
            [own_attention[:, at : at + step], own_pool[:, at : at + step]], axis=0
        )
        far = jnp.concatenate(
            [
                other_out[base * 2 * LANES : (base + 1) * 2 * LANES, :]
                for base in range(at // LANES, (at + step) // LANES)
            ],
            axis=1,
        )
        both = dot(mine, weights) + dot(theirs, far)
        partial_out[:, :, at : at + step] = both.astype(BF16).reshape(CHIPS, ROWS, step)


def sum_kernel(parts, out):
    total = parts[0].astype(F32) + parts[1].astype(F32)
    total = total + parts[2].astype(F32) + parts[3].astype(F32)
    out[0] = total.astype(BF16)


def local(
    tokens,
    input_gain,
    query_weight,
    latent_down,
    rotary_down,
    pool_down,
    key_up,
    value_up,
    query_gain,
    key_gain,
    pool_weight,
    pool_scale,
    attention_gain,
    pool_gain,
    attention_out,
    pool_out,
):
    inside, starts = (jnp.asarray(t) for t in angle_tables())
    own_gain = jnp.stack([pool_scale, attention_gain, pool_gain, pool_gain])

    normed, latent_rows = whole(
        norm_kernel,
        (far((CHIPS, ROWS, D), BF16), shape((ROWS, LAT), BF16)),
        tokens,
        input_gain[None],
        latent_down,
        rotary_down.T,
        room=56,
        name="norm",
    )
    rows = among_chips(normed)
    query_t = query_weight.T
    other = to_partner(
        whole(
            bundle_kernel,
            shape((FLAT, LANES), BF16),
            query_t,
            pool_down,
            attention_out,
            pool_out,
            own_gain,
            normed,
            specs=[VECTOR] * 5 + [AWAY],
            room=56,
            name="bundle",
        )
    )
    own_latents = lax.all_gather(latent_rows, "sp", axis=0, tiled=False)
    other_latents = to_partner(own_latents)

    def part(length, at):
        return pl.BlockSpec((length, LANES), lambda i: (at // length, 0))

    queries, token = whole(
        project_kernel,
        (far((CHIPS, 2, QROWS, LANES), BF16), shape((8, LANES), F32)),
        rows,
        query_t,
        other,
        query_gain[None],
        inside,
        starts,
        specs=[VECTOR, VECTOR, part(AT_GAINS, 0), VECTOR, VECTOR, VECTOR],
        name="project",
    )
    queries = among_chips(queries).reshape(HEADS, QROWS, LANES)

    def chip():
        return lax.axis_index("tp") // 2

    def up_to(step):
        return jnp.minimum(step, lax.axis_index("sp") // 2)

    keys, latents = pl.pallas_call(
        expand_kernel,
        grid=(BLOCKS // 2,),
        out_shape=(far((HEADS, KEYS, LANES), BF16), far((KEYS, KV_LATENT), BF16)),
        in_specs=[
            pl.BlockSpec((2, ROWS, LAT), lambda i: (up_to(i), 0, 0)),
            pl.BlockSpec((2, ROWS, LAT), lambda i: (up_to(i), 0, 0)),
            pl.BlockSpec((KV_LATENT, HEADS * NOPE_DIM), lambda i: (0, 0)),
            pl.BlockSpec((1, QK_DIM), lambda i: (0, 0)),
            pl.BlockSpec((2, 1, 2, ROWS, LANES), lambda i: (0, chip(), 0, 0, 0)),
            pl.BlockSpec((2, BLOCKS, LANES), lambda i: (0, 0, 0)),
        ],
        out_specs=[
            pl.BlockSpec((HEADS, 4 * ROWS, LANES), lambda i: (0, up_to(i), 0)),
            pl.BlockSpec((4 * ROWS, KV_LATENT), lambda i: (up_to(i), 0)),
        ],
        compiler_params=pltpu.CompilerParams(vmem_limit_bytes=14 * MIB),
        name="expand",
    )(own_latents, other_latents, key_up, key_gain[None], inside, starts)

    pool_rows, tails, last_tails = whole(
        pool_project_kernel,
        (
            shape((2, QROWS, LANES), BF16),
            shape((2, CHIPS, HALO, LANES), BF16),
            shape((2, HALO, LANES), BF16),
        ),
        rows,
        pool_down,
        other,
        token,
        specs=[VECTOR, VECTOR, part(D, AT_POOL), VECTOR],
        name="pool_project",
    )
    halo = to_partner(tails)
    width = 2 * CHIPS
    steps = [
        (block * width + 2 * chip + 1, (block + 1) * width + 2 * chip)
        for block in range(BLOCKS - 1)
        for chip in range(CHIPS)
    ]
    first_halo = lax.ppermute(last_tails, ("sp", "tp"), steps)

    numer = whole(
        attend_kernel,
        far((CHIPS, QROWS + HALO, 2 * LANES), BF16),
        queries,
        keys,
        latents,
        value_up,
        specs=[VECTOR, AWAY, AWAY, AWAY],
        scratch=(
            pltpu.VMEM((HEADS, KEYS, LANES), BF16),
            pltpu.VMEM((KEYS, KV_LATENT), BF16),
            pltpu.VMEM((KV_LATENT, HEADS * VALUE_DIM), BF16),
            pltpu.VMEM((HEADS, QROWS, KV_LATENT), F32),
            pltpu.VMEM((HEADS, QROWS, LANES), F32),
            pltpu.SemaphoreType.DMA((2, BLOCKS // 2 + 1)),
        ),
        room=56,
        name="attend",
    )
    parts = among_chips(numer)

    pooled, pool_squares = whole(
        pool_kernel,
        (shape((2, QROWS, LANES), F32), shape((QROWS, LANES), F32)),
        pool_rows,
        halo,
        first_halo,
        pool_weight,
        own_gain,
        other,
        specs=[VECTOR] * 5 + [part(HALO, AT_GAINS)],
        name="pool",
    )
    attended, squares = whole(
        join_kernel,
        (shape((2, QROWS, LANES), F32), far((CHIPS, 8, QROWS), F32)),
        parts,
        pool_squares,
        name="join",
    )
    squares = among_chips(squares)
    partial = whole(
        mix_kernel,
        far((CHIPS, ROWS, D), BF16),
        attended,
        pooled,
        squares,
        own_gain,
        other,
        attention_out,
        pool_out,
        other,
        specs=[VECTOR] * 4 + [part(HALO, AT_GAINS), VECTOR, VECTOR, part(AT_OUT, AT_OUT)],
        name="mix",
    )
    return whole(sum_kernel, shape((1, ROWS, D), BF16), among_chips(partial), name="sum")


def solution(mesh):
    placed = (
        P("fs", ("sp", "tp"), None),
        P(),
        P(None, "tp"),
        P(),
        P(),
        P(None, "tp"),
        P(),
        P(),
        P(),
        P(),
        P(),
        P("tp"),
        P("tp"),
        P("tp"),
        P("tp", None),
        P("tp", None),
    )
    return jax.shard_map(
        local, mesh=mesh, in_specs=placed, out_specs=P("fs", ("sp", "tp"), None), check_vma=False
    )
```

time: 144 us -> 130 us (0.903)
  blocking collectives: 47.6 us -> 58.2 us
  starting transfers between devices: 29.3 us -> 21.1 us
  local copies, waits for them, and re-layouts: 12.8 us -> 6 us
  waiting for transfers between devices: 9.63 us -> 4.58 us
  Pallas kernels: 39.5 us -> 36.2 us
    all_to_all x1 -> x2, blocking collectives: 17.1 us -> 25.3 us  [among_chips(): lax.all_to_all(array, 'tp', 0, 0, axis_index_groups=SAME_CORE, tiled=True)]
    all_to_all x4 -> x3, waiting for transfers between devices: 6.58 us -> 0.9 us  [among_chips(): lax.all_to_all(array, 'tp', 0, 0, axis_index_groups=SAME_CORE, tiled=True)]
    ppermute x5 -> x3, starting transfers between devices: 10.5 us -> 6 us  [to_partner(): return lax.ppermute(array, 'tp', [(i, i ^ 1) for i in range(2 * CHIPS)])]
    all_to_all x4 -> x3, starting transfers between devices: 17.5 us -> 13.8 us  [among_chips(): lax.all_to_all(array, 'tp', 0, 0, axis_index_groups=SAME_CORE, tiled=True)]
    pallas_call x8 -> x10, Pallas kernels: 39.5 us -> 36.2 us  [the longest x9 24.2 us: whole(): pl.pallas_call(kernel, grid=() if specs is None else (1,), out_shape=out_...]
    all_gather x1, blocking collectives: 30.5 us -> 32.8 us  [local(): own_latents = lax.all_gather(latent_rows, 'sp', axis=0, tiled=False)]
    unnamed x46 -> x28, local copies, waits for them, and re-layouts: 6.91 us -> 6 us
  transfers between devices with their start and end apart: 10 -> 7, of which waited for: 3 -> 2; matrix products, arithmetic and copies ran while one was open for 6% -> 0% of each run, Pallas kernels for 22% -> 12%
where the time goes in v2:
time: 130 us; the launch traced here: 128 us
  blocking collectives  58.2 us (45%)
  Pallas kernels  36.2 us (28%)
  starting transfers between devices  21.1 us (16%)
  local copies, waits for them, and re-layouts  6 us (5%)
  waiting for transfers between devices  4.58 us (4%)
  other arithmetic  1.32 us (1%)
    all_gather x1, blocking collectives, local(): own_latents = lax.all_gather(latent_rows, 'sp', axis=0, tiled=False)  32.8 us
    all_to_all x2, blocking collectives, among_chips(): lax.all_to_all(array, 'tp', 0, 0, axis_index_groups=SAME_CORE, tiled=True)  25.3 us
    pallas_call x9, Pallas kernels, whole(): pl.pallas_call(kernel, grid=() if specs is None else (1,), out_shape=out_...  24.2 us
    all_to_all x3, starting transfers between devices, among_chips(): lax.all_to_all(array, 'tp', 0, 0, axis_index_groups=SAME_CORE, tiled=True)  13.8 us
    pallas_call x1, Pallas kernels, local(): pl.pallas_call(expand_kernel, grid=(BLOCKS // 2,), out_shape=(far((HEADS,...  12 us
    unnamed x28, local copies, waits for them, and re-layouts  6 us
    ppermute x3, starting transfers between devices, to_partner(): return lax.ppermute(array, 'tp', [(i, i ^ 1) for i in range(2 * CHIPS)])  6 us
    ppermute x1, waiting for transfers between devices, local(): first_halo = lax.ppermute(last_tails, ('sp', 'tp'), steps)  3.67 us
  transfers between devices with their start and end apart: 7, of which 2 were waited for; matrix products, arithmetic and copies ran while one was open for 0% of the time, Pallas kernels for 12%

profile of v2, /device:TPU:480, one launch (start us, length us, event | category | flops | bytes accessed | tf_op | source)
XLA Modules:
  0.0 127.6 jit_solution(16870907589973329260)
XLA Ops:
  0.0 1.3 %pad_maximum_fusion.gains.own.own_gain = f32[4,128]{1,0:T(4,128)} fusion(f32[1,128]{1,0:T(1,128)} %bitcast.16, f32[1,128]{1,0:T(1,128)} %bitcast.17, f32[1,128]{1,0:T(1,128)} %bitcast.18), kind=kLoop, calls=%fused_computation | loop fusion | flops 1536 | bytes 3584 | tf_op jit(solution)/shard_map/stack | solution.py:417
  1.3 2.5 %norm.1 = (bf16[4,64,2048]{2,1,0:T(8,128)(2,1)}, bf16[64,384]{1,0:T(8,128)(2,1)}) custom-call(bf16[1,64,2048]{2,1,0:T(8,128)(2,1)} %tokens.1, f32[1,2048]{1,0:T(1,128)} %bitcast.15, bf16[2048,256]{1,0:T(8,128)(2,1)} %latent_down.1, bf16[32,2048]{1,0:T(8,128)(2,1)} %bitcast.14), custom_call_target="tpu_custom_call" | custom-call | tf_op jit(solution)/shard_map/norm/pallas_call | solution.py:68
  3.8 3.1 %bundle.1 = bf16[8192,128]{1,0:T(8,128)(2,1)} custom-call(bf16[96,2048]{1,0:T(8,128)(2,1)} %bitcast.10, bf16[2048,128]{1,0:T(8,128)(2,1)} %own.1, bf16[128,2048]{1,0:T(8,128)(2,1)} %own_attention.1, bf16[128,2048]{1,0:T(8,128)(2,1)} %own_pool.1, f32[4,128]{1,0:T(4,128)} %pad_maximum_fusion.gains.own.own_gain, bf16[4,64,2048]{2,1,0:T(8,128)(2,1)} %get-tuple-element.18.after), custom_call_target="tpu_custom_call" | custom-call | tf_op jit(solution)/shard_map/bundle/pallas_call | solution.py:68
  7.0 2.0 %collective-permute-start = (bf16[8192,128]{1,0:T(8,128)(2,1)}, bf16[8192,128]{1,0:T(8,128)(2,1)S(1)}, u32[]{:S(2)}, u32[]{:S(2)}) collective-permute-start(bf16[8192,128]{1,0:T(8,128)(2,1)} %bundle.1), channel_id=1, source_target_pairs={{0,1},{1,0},{2,3},{3,2},{4,5},{5,4},{6,7},{7,6},{8,9},{9,8},{10,11... | collective-permute-start | bytes 6291464 | tf_op jit(solution)/shard_map/ppermute | solution.py:54
  9.0 4.3 %all-to-all-start = ((bf16[4,64,2048]{2,1,0:T(8,128)(2,1)}), bf16[4,64,2048]{2,1,0:T(8,128)(2,1)S(1)}, u32[]{:S(2)}, u32[]{:S(2)}) async-start(bf16[4,64,2048]{2,1,0:T(8,128)(2,1)} %get-tuple-element.18.after), calls=%async_computation | async-start | bytes 2097152 | tf_op jit(solution)/shard_map/all_to_all | solution.py:50
  13.3 32.8 %all-gather = bf16[1024,384]{1,0:T(8,128)(2,1)} all-gather(bf16[64,384]{1,0:T(8,128)(2,1)} %get-tuple-element.20), channel_id=2, replica_groups=mesh['sp'=16,'fs'=4,'tp'=8] {'sp'}, dimensions={0}, use_global_device_ids=true | all-gather | bytes 835584 | tf_op jit(solution)/shard_map/all_gather | solution.py:446
  46.1 1.9 %collective-permute-start.1 = (bf16[16,64,384]{2,1,0:T(8,128)(2,1)}, bf16[16,64,384]{2,1,0:T(8,128)(2,1)}, u32[]{:S(2)}, u32[]{:S(2)}) collective-permute-start(bf16[16,64,384]{2,1,0:T(8,128)(2,1)} %bitcast.8.own), channel_id=1, source_target_pairs={{0,1},{1,0},{2,3},{3,2},{4,5},{5,4},{6,7},{7,6},{8,9},{9,8},{10,11... | collective-permute-start | bytes 2359304 | tf_op jit(solution)/shard_map/ppermute | solution.py:54
  48.1 1.0 copy-done.3
  49.8 1.7 %project.1 = (bf16[4,2,256,128]{3,2,1,0:T(8,128)(2,1)}, f32[8,128]{1,0:T(8,128)S(1)}) custom-call(bf16[4,64,2048]{2,1,0:T(8,128)(2,1)S(1)} %all-to-all-done.rows, bf16[96,2048]{1,0:T(8,128)(2,1)S(1)} %bitcast.11, bf16[8192,128]{1,0:T(8,128)(2,1)S(1)} %collective-permute-done.other.other_gain.other_out, f32[1,96]{1,0:T(1,128)S(1)} %bitcast.12, ...), custom_call_target="tpu_custom_call" | custom-call | tf_op jit(solution)/shard_map/project/pallas_call | solution.py:68
  52.1 4.7 %all-to-all-start.1 = ((bf16[4,2,256,128]{3,2,1,0:T(8,128)(2,1)}), bf16[4,2,256,128]{3,2,1,0:T(8,128)(2,1)}, u32[]{:S(2)}, u32[]{:S(2)}) async-start(bf16[4,2,256,128]{3,2,1,0:T(8,128)(2,1)} %get-tuple-element.19), calls=%async_computation.1 | async-start | bytes 1048576 | tf_op jit(solution)/shard_map/all_to_all | solution.py:50
  56.8 1.0 copy-done.4
  57.9 0.9 copy-done.7
  59.5 12.0 %expand.1 = (bf16[8,2048,128]{2,1,0:T(8,128)(2,1)}, bf16[2048,256]{1,0:T(8,128)(2,1)}) custom-call(bf16[16,64,384]{2,1,0:T(8,128)(2,1)} %bitcast.8.own, bf16[16,64,384]{2,1,0:T(8,128)(2,1)} %collective-permute-done.1.other, bf16[256,512]{1,0:T(8,128)(2,1)S(1)} %copy-done.7, f32[1,96]{1,0:T(1,128)S(1)} %bitcast.13, f32[2,4,2,64,128]{4,3,2,1,0:T(8,128)S(1)} %copy-done.4, ...), custom_call_target="tpu_custom_call" | custom-call | tf_op jit(solution)/shard_map/expand/pallas_call | solution.py:472
  71.5 10.9 %attend.1 = bf16[4,272,256]{2,1,0:T(8,128)(2,1)} custom-call(bf16[8,256,128]{2,1,0:T(8,128)(2,1)} %bitcast.7.queries, bf16[8,2048,128]{2,1,0:T(8,128)(2,1)} %get-tuple-element.21.keys_far, bf16[2048,256]{1,0:T(8,128)(2,1)} %get-tuple-element.22.latents_far, bf16[256,1024]{1,0:T(8,128)(2,1)} %value_far.1), custom_call_target="tpu_custom_call" | custom-call | tf_op jit(solution)/shard_map/attend/pallas_call | solution.py:68
  82.4 4.8 %all-to-all-start.2 = ((bf16[4,272,256]{2,1,0:T(8,128)(2,1)}), bf16[4,272,256]{2,1,0:T(8,128)(2,1)}, u32[]{:S(2)}, u32[]{:S(2)}) async-start(bf16[4,272,256]{2,1,0:T(8,128)(2,1)} %attend.1), calls=%async_computation.2 | async-start | bytes 1114112 | tf_op jit(solution)/shard_map/all_to_all | solution.py:50
  87.2 1.0 copy-done.2
  89.0 2.1 %collective-permute-start.2 = (bf16[2,4,16,128]{3,2,1,0:T(8,128)(2,1)S(1)}, bf16[2,4,16,128]{3,2,1,0:T(8,128)(2,1)S(1)}, u32[]{:S(2)}, u32[]{:S(2)}) collective-permute-start(bf16[2,4,16,128]{3,2,1,0:T(8,128)(2,1)S(1)} %get-tuple-element.25), channel_id=1, source_target_pairs={{0,1},{1,0},{2,3},{3,2},{4,5},{5,4},{6,7},{7,6},{8,9},{9,8},{10,11... | collective-permute-start | bytes 98312 | tf_op jit(solution)/shard_map/ppermute | solution.py:54
  91.0 1.3 %collective-permute-start.3 = (bf16[2,16,128]{2,1,0:T(8,128)(2,1)S(1)}, bf16[2,16,128]{2,1,0:T(8,128)(2,1)S(1)}, u32[]{:S(2)}, u32[]{:S(2)}) collective-permute-start(bf16[2,16,128]{2,1,0:T(8,128)(2,1)S(1)} %get-tuple-element.26), channel_id=1, source_target_pairs={{1,32},{3,34},{5,36},{7,38},{33,64},{35,66},{37,68},{39,70},{65,96... | collective-permute-start | bytes 24584 | tf_op jit(solution)/shard_map/ppermute | solution.py:513
  92.3 3.7 %collective-permute-done.3.first_halo = bf16[2,16,128]{2,1,0:T(8,128)(2,1)S(1)} collective-permute-done((bf16[2,16,128]{2,1,0:T(8,128)(2,1)S(1)}, bf16[2,16,128]{2,1,0:T(8,128)(2,1)S(1)}, u32[]{:S(2)}, u32[]{:S(2)}) %collective-permute-start.3) | collective-permute-done | bytes 8224 | tf_op jit(solution)/shard_map/ppermute | solution.py:513
  96.3 0.9 all-to-all-done.2.parts
  97.2 2.3 %join.1 = (f32[2,256,128]{2,1,0:T(8,128)S(1)}, f32[4,8,256]{2,1,0:T(8,128)}) custom-call(bf16[4,272,256]{2,1,0:T(8,128)(2,1)} %all-to-all-done.2.parts, f32[256,128]{1,0:T(8,128)S(1)} %get-tuple-element.27.pool_squares), custom_call_target="tpu_custom_call" | custom-call | tf_op jit(solution)/shard_map/join/pallas_call | solution.py:68
  99.5 9.4 %all_to_all.25.squares = f32[4,8,256]{2,1,0:T(8,128)S(1)} all-to-all(f32[4,8,256]{2,1,0:T(8,128)} %get-tuple-element.30), channel_id=1, replica_groups={{0,2,4,6},{1,3,5,7},{8,10,12,14},{9,11,13,15},{16,18,20,22},{17,19,21,2..., dimensions={0} | all-to-all | bytes 65536 | tf_op jit(solution)/shard_map/all_to_all | solution.py:50
  108.9 1.9 %mix.1 = bf16[4,64,2048]{2,1,0:T(8,128)(2,1)} custom-call(f32[2,256,128]{2,1,0:T(8,128)S(1)} %get-tuple-element.28.attended, f32[2,256,128]{2,1,0:T(8,128)S(1)} %get-tuple-element.29.pooled, f32[4,8,256]{2,1,0:T(8,128)S(1)} %all_to_all.25.squares, f32[4,128]{1,0:T(4,128)S(1)} %copy-done.9, ...), custom_call_target="tpu_custom_call" | custom-call | tf_op jit(solution)/shard_map/mix/pallas_call | solution.py:68
  110.7 16.0 %all_to_all.26.parts = bf16[4,64,2048]{2,1,0:T(8,128)(2,1)S(1)} all-to-all(bf16[4,64,2048]{2,1,0:T(8,128)(2,1)} %mix.1), channel_id=1, replica_groups={{0,2,4,6},{1,3,5,7},{8,10,12,14},{9,11,13,15},{16,18,20,22},{17,19,21,2..., dimensions={0} | all-to-all | bytes 2097152 | tf_op jit(solution)/shard_map/all_to_all | solution.py:50
  (32 shorter events, 3.8 us)
Async XLA Ops:
  6.9 41.1 %copy-start.5 = (bf16[2048,96]{0,1:T(8,128)(2,1)S(1)}, bf16[2048,96]{0,1:T(8,128)(2,1)}, u32[]{:S(2)}) copy-start(bf16[2048,96]{0,1:T(8,128)(2,1)} %param.20) | copy-start | bytes 1179652
  7.0 41.1 %copy-start.8 = (f32[2,16,128]{2,1,0:T(8,128)S(1)}, f32[2,16,128]{2,1,0:T(8,128)}, u32[]{:S(2)}) copy-start(f32[2,16,128]{2,1,0:T(8,128)} %constant.5.clone.starts) | copy-start | bytes 49156
  7.0 41.1 %collective-permute-start = (bf16[8192,128]{1,0:T(8,128)(2,1)}, bf16[8192,128]{1,0:T(8,128)(2,1)S(1)}, u32[]{:S(2)}, u32[]{:S(2)}) collective-permute-start(bf16[8192,128]{1,0:T(8,128)(2,1)} %bundle.1), channel_id=1, source_target_pairs={{0,1},{1,0},{2,3},{3,2},{4,5},{5,4},{6,7},{7,6},{8,9},{9,8},{10,11... | collective-permute-start | bytes 6291464 | tf_op jit(solution)/shard_map/ppermute | solution.py:54
  9.0 39.1 %all-to-all-start = ((bf16[4,64,2048]{2,1,0:T(8,128)(2,1)}), bf16[4,64,2048]{2,1,0:T(8,128)(2,1)S(1)}, u32[]{:S(2)}, u32[]{:S(2)}) async-start(bf16[4,64,2048]{2,1,0:T(8,128)(2,1)} %get-tuple-element.18.after), calls=%async_computation | async-start | bytes 2097152 | tf_op jit(solution)/shard_map/all_to_all | solution.py:50
  46.1 10.7 %collective-permute-start.1 = (bf16[16,64,384]{2,1,0:T(8,128)(2,1)}, bf16[16,64,384]{2,1,0:T(8,128)(2,1)}, u32[]{:S(2)}, u32[]{:S(2)}) collective-permute-start(bf16[16,64,384]{2,1,0:T(8,128)(2,1)} %bitcast.8.own), channel_id=1, source_target_pairs={{0,1},{1,0},{2,3},{3,2},{4,5},{5,4},{6,7},{7,6},{8,9},{9,8},{10,11... | collective-permute-start | bytes 2359304 | tf_op jit(solution)/shard_map/ppermute | solution.py:54
  48.1 1.0 copy-start.3
  49.1 0.7 copy-start.12
  51.5 0.6 copy-start.10
  52.1 19.4 %all-to-all-start.1 = ((bf16[4,2,256,128]{3,2,1,0:T(8,128)(2,1)}), bf16[4,2,256,128]{3,2,1,0:T(8,128)(2,1)}, u32[]{:S(2)}, u32[]{:S(2)}) async-start(bf16[4,2,256,128]{3,2,1,0:T(8,128)(2,1)} %get-tuple-element.19), calls=%async_computation.1 | async-start | bytes 1048576 | tf_op jit(solution)/shard_map/all_to_all | solution.py:50
  56.8 1.0 copy-start.4
  57.9 0.9 copy-start.7
  58.8 0.7 copy-start.13
  71.5 15.7 %copy-start.11 = (f32[8,128]{1,0:T(8,128)S(1)}, f32[8,128]{1,0:T(8,128)}, u32[]{:S(2)}) copy-start(f32[8,128]{1,0:T(8,128)} %copy-done.10) | copy-start | bytes 12292
  82.4 14.9 %all-to-all-start.2 = ((bf16[4,272,256]{2,1,0:T(8,128)(2,1)}), bf16[4,272,256]{2,1,0:T(8,128)(2,1)}, u32[]{:S(2)}, u32[]{:S(2)}) async-start(bf16[4,272,256]{2,1,0:T(8,128)(2,1)} %attend.1), calls=%async_computation.2 | async-start | bytes 1114112 | tf_op jit(solution)/shard_map/all_to_all | solution.py:50
  87.2 1.0 copy-start.2
  88.2 7.8 %copy-start.6 = (bf16[16,64,64]{2,1,0:T(8,128)(2,1)S(1)}, bf16[16,64,64]{2,1,0:T(8,128)(2,1)}, u32[]{:S(2)}) copy-start(bf16[16,64,64]{2,1,0:T(8,128)(2,1)} %maps.1) | copy-start | bytes 393220
  88.3 7.8 %copy-start.9 = (f32[4,128]{1,0:T(4,128)S(1)}, f32[4,128]{1,0:T(4,128)}, u32[]{:S(2)}) copy-start(f32[4,128]{1,0:T(4,128)} %pad_maximum_fusion.gains.own.own_gain) | copy-start | bytes 6148
  89.0 19.9 %copy-start = (bf16[128,2048]{1,0:T(8,128)(2,1)S(1)}, bf16[128,2048]{1,0:T(8,128)(2,1)}, u32[]{:S(2)}) copy-start(bf16[128,2048]{1,0:T(8,128)(2,1)} %own_attention.1) | copy-start | bytes 1572868
  89.0 19.9 %copy-start.1 = (bf16[128,2048]{1,0:T(8,128)(2,1)S(1)}, bf16[128,2048]{1,0:T(8,128)(2,1)}, u32[]{:S(2)}) copy-start(bf16[128,2048]{1,0:T(8,128)(2,1)} %own_pool.1) | copy-start | bytes 1572868
  89.0 7.0 %collective-permute-start.2 = (bf16[2,4,16,128]{3,2,1,0:T(8,128)(2,1)S(1)}, bf16[2,4,16,128]{3,2,1,0:T(8,128)(2,1)S(1)}, u32[]{:S(2)}, u32[]{:S(2)}) collective-permute-start(bf16[2,4,16,128]{3,2,1,0:T(8,128)(2,1)S(1)} %get-tuple-element.25), channel_id=1, source_target_pairs={{0,1},{1,0},{2,3},{3,2},{4,5},{5,4},{6,7},{7,6},{8,9},{9,8},{10,11... | collective-permute-start | bytes 98312 | tf_op jit(solution)/shard_map/ppermute | solution.py:54
  91.0 5.0 %collective-permute-start.3 = (bf16[2,16,128]{2,1,0:T(8,128)(2,1)S(1)}, bf16[2,16,128]{2,1,0:T(8,128)(2,1)S(1)}, u32[]{:S(2)}, u32[]{:S(2)}) collective-permute-start(bf16[2,16,128]{2,1,0:T(8,128)(2,1)S(1)} %get-tuple-element.26), channel_id=1, source_target_pairs={{1,32},{3,34},{5,36},{7,38},{33,64},{35,66},{37,68},{39,70},{65,96... | collective-permute-start | bytes 24584 | tf_op jit(solution)/shard_map/ppermute | solution.py:513

commit v3 on v2

v3 whole, which is shorter than its diff:
```python
import math

import jax
import jax.numpy as jnp
import numpy as np
from jax import lax
from jax.experimental import pallas as pl
from jax.experimental.pallas import tpu as pltpu
from jax.sharding import PartitionSpec as P

HEADS = 8
NOPE_DIM = 64
ROPE_DIM = 32
VALUE_DIM = 128
KV_LATENT = 256
GROUP_DIM = 64
QK_DIM = 96
D = 2048
BLOCKS = 16
BLOCK = 512
CHIPS = 4
ROWS = 64
LANES = 128
QROWS = CHIPS * ROWS
KEYS = BLOCKS * 2 * ROWS
HALO = 16
PACK = ROWS + 8
QUAD = 4 * 2 * ROWS

EPS = 1e-06
THETA = 10000.0
SAME_CORE = [[0, 2, 4, 6], [1, 3, 5, 7]]
F32 = jnp.float32
BF16 = jnp.bfloat16


def angle_tables():
    half = ROPE_DIM // 2
    freq = np.zeros(LANES)
    inv = 1.0 / THETA ** (np.arange(half, dtype=np.float64) / half)
    freq[NOPE_DIM : NOPE_DIM + half] = inv
    freq[NOPE_DIM + half : QK_DIM] = inv
    inside = np.arange(BLOCK)[:, None] * freq[None, :]
    starts = (np.arange(BLOCKS) * BLOCK)[:, None] * freq[None, :]
    turned = (np.arange(BLOCK)[:, None] * inv[None, :]).reshape(CHIPS, 2 * ROWS, half)
    begins = (np.arange(BLOCKS) * BLOCK)[:, None] * inv[None, :]
    begins = np.broadcast_to(begins[:, :, None], (BLOCKS, half, LANES))
    tables = []
    for angle in (inside, starts, turned.transpose(0, 2, 1), begins):
        tables.append(np.stack([np.cos(angle), np.sin(angle)]).astype(np.float32))
    return tables


def among_chips(array):
    return lax.all_to_all(array, "tp", 0, 0, axis_index_groups=SAME_CORE, tiled=True)


def among_all(array):
    return lax.all_to_all(array, "tp", 0, 0, tiled=True)


def to_partner(array):
    return lax.ppermute(array, "tp", [(i, i ^ 1) for i in range(2 * CHIPS)])


MIB = 1024 * 1024
ROOM_PROJECT = 14
VECTOR = pl.BlockSpec(memory_space=pltpu.VMEM)
AWAY = pl.BlockSpec(memory_space=pltpu.HBM)


def whole(kernel, out_shape, *args, specs=None, scratch=(), room=14):
    single = not isinstance(out_shape, (list, tuple))
    return pl.pallas_call(
        kernel,
        grid=() if specs is None else (1,),
        out_shape=out_shape,
        in_specs=[VECTOR] * len(args) if specs is None else specs,
        out_specs=VECTOR if single else [VECTOR] * len(out_shape),
        scratch_shapes=list(scratch),
        compiler_params=pltpu.CompilerParams(vmem_limit_bytes=room * MIB),
    )(*args)


def place():
    member = lax.axis_index("tp")
    return lax.axis_index("sp"), member // 2, member % 2


def shape(dims, dtype):
    return jax.ShapeDtypeStruct(dims, dtype)


def far(dims, dtype):
    return pltpu.HBM(dims, dtype)


def dot(a, b, dims=((1,), (0,)), precision=None):
    return lax.dot_general(
        a, b, (dims, ((), ())), preferred_element_type=F32, precision=precision
    )


def turn(vectors, cosine, sine):
    lane = lax.broadcasted_iota(jnp.int32, vectors.shape, vectors.ndim - 1)
    half = ROPE_DIM // 2
    ahead = pltpu.roll(vectors, LANES - half, vectors.ndim - 1)
    behind = pltpu.roll(vectors, half, vectors.ndim - 1)
    return vectors * cosine + jnp.where(lane < NOPE_DIM + half, -ahead, behind) * sine


def at_block(inside_cos, inside_sin, start_cos, start_sin):
    cosine = start_cos * inside_cos - start_sin * inside_sin
    sine = start_sin * inside_cos + start_cos * inside_sin
    return cosine, sine


def norm_kernel(tokens, gain, latent_down, rotary_down, normed_out, latent_out):
    source = tokens[0].astype(F32)
    scale = lax.rsqrt(jnp.mean(source * source, axis=-1, keepdims=True) + EPS)
    normed = (source * scale * gain[...]).astype(BF16)
    for member in range(2 * CHIPS):
        normed_out[member] = normed
    latent = dot(normed, latent_down[...]).astype(BF16)
    rotary = dot(rotary_down[...], normed, ((1,), (1,)))
    packed = jnp.concatenate([rotary[at : at + 8] for at in range(0, ROPE_DIM, 8)], axis=1)
    latent_out[:ROWS] = latent
    latent_out[ROWS:] = packed.astype(BF16)


def out_bundle_kernel(attention_out, pool_out, gain_a, gain_p, both):
    both[:LANES, :] = attention_out[...]
    both[LANES : 2 * LANES, :] = pool_out[...]
    rest = jnp.concatenate([gain_a[...], gain_p[...]] * 2, axis=0)
    rows = []
    for _ in range(3):
        piece = rest.astype(BF16)
        rest = rest - piece.astype(F32)
        rows.append(piece.astype(F32))
    rows.append(jnp.zeros((4, LANES), F32))
    rows = jnp.concatenate(rows, axis=0)
    both[2 * LANES :, :] = jnp.concatenate([rows] * (D // LANES), axis=1).astype(BF16)


def project_kernel(rows, query_down, pool_down, gain, inside, starts, query_out, pool_out, tail_out):
    z, _, _ = place()
    piece = rows[...].reshape(BLOCK, D)
    start_cos = starts[0, pl.ds(z, 1), :]
    start_sin = starts[1, pl.ds(z, 1), :]
    cosine, sine = at_block(inside[0], inside[1], start_cos, start_sin)
    empty = jnp.zeros((LANES - QK_DIM, D), BF16)
    wide_gain = jnp.concatenate([gain[...], jnp.zeros((1, LANES - QK_DIM), F32)], axis=1)
    wide_gain = wide_gain * (math.log2(math.e) / math.sqrt(QK_DIM))
    raw = dot(piece, jnp.concatenate([query_down[...], empty], axis=0), ((1,), (1,)))
    square = jnp.sum(raw * raw, axis=-1, keepdims=True) * (1.0 / QK_DIM)
    normal = raw * lax.rsqrt(square + EPS) * wide_gain
    queries = turn(normal, cosine, sine).astype(BF16).reshape(CHIPS, 2, ROWS, LANES)
    for side in range(2):
        mine = queries[:, side].reshape(QROWS, LANES)
        for chip in range(CHIPS):
            query_out[2 * chip + side] = mine
    result = dot(piece, pool_down[...]).astype(BF16)
    pool_out[...] = result
    tail_out[...] = result[BLOCK - HALO :]


def expand_kernel(own, other, key_up, gain, inside, starts, keys_out, latent_out, key_up_t):
    z, _, p = place()
    step = pl.program_id(0)

    @pl.when(step == 0)
    def _():
        key_up_t[...] = jnp.transpose(key_up[...].astype(F32)).astype(BF16)

    @pl.when(step <= z // 4)
    def _():
        wide_gain = jnp.concatenate([gain[...], jnp.zeros((1, LANES - QK_DIM), F32)], axis=1)
        wide_gain = jnp.broadcast_to(wide_gain * math.sqrt(QK_DIM), (8, LANES))
        column = jnp.transpose(wide_gain)[:, 0:1]
        half = ROPE_DIM // 2
        latents, rotaries, cosines, sines = [], [], [], []
        for k in range(4):
            mine, theirs = own[k].astype(F32), other[k].astype(F32)
            for side in (jnp.where(p == 0, mine, theirs), jnp.where(p == 0, theirs, mine)):
                latents.append(side[:ROWS])
                rotaries.append(
                    jnp.concatenate(
                        [side[ROWS:, at : at + ROWS] for at in range(0, KV_LATENT, ROWS)], axis=0
                    )
                )
            cosine, sine = at_block(inside[0, 0], inside[1, 0], starts[0, k], starts[1, k])
            cosines.append(cosine)
            sines.append(sine)
        latent = jnp.concatenate(latents, axis=0)
        rotary = jnp.concatenate(rotaries, axis=1)
        cosine = jnp.concatenate(cosines, axis=1)
        sine = jnp.concatenate(sines, axis=1)
        scale = lax.rsqrt(jnp.mean(latent * latent, axis=-1, keepdims=True) + EPS)
        normed = (latent * scale).astype(BF16)
        latent_out[...] = normed
        shared = jnp.sum(rotary * rotary, axis=0, keepdims=True) + QK_DIM * EPS
        ahead = rotary[:half] * column[NOPE_DIM : NOPE_DIM + half]
        behind = rotary[half:] * column[NOPE_DIM + half : QK_DIM]
        turned = jnp.concatenate(
            [ahead * cosine - behind * sine, behind * cosine + ahead * sine], axis=0
        )
        plain_gain = jnp.broadcast_to(column[:NOPE_DIM], (NOPE_DIM, QUAD))
        for head in range(HEADS):
            rows = key_up_t[head * NOPE_DIM : (head + 1) * NOPE_DIM, :]
            part = dot(rows, normed, ((1,), (1,)))
            factor = lax.rsqrt(jnp.sum(part * part, axis=0, keepdims=True) + shared)
            keys_out[head, :NOPE_DIM, :] = (part * plain_gain * factor).astype(BF16)
            keys_out[head, NOPE_DIM:, :] = (turned * factor).astype(BF16)


def attend_kernel(
    queries, keys_far, latents_far, value_far, out, keys, latents, value_up, sums, totals, arrived
):
    z, x, p = place()
    wide = QUAD
    pair = z // 4

    def copies(index):
        at = pl.multiple_of(index * wide, wide)
        return (
            pltpu.make_async_copy(
                keys_far.at[:, :, pl.ds(at, wide)],
                keys.at[:, :, pl.ds(at, wide)],
                arrived.at[0, index],
            ),
            pltpu.make_async_copy(
                latents_far.at[pl.ds(at, wide), :],
                latents.at[pl.ds(at, wide), :],
                arrived.at[1, index],
            ),
        )

    def fetch(index, carry):
        for copy in copies(pair - index):
            copy.start()
        return carry

    lax.fori_loop(0, pair + 1, fetch, 0)
    value_copy = pltpu.make_async_copy(value_far, value_up, arrived.at[0, BLOCKS // 4])
    value_copy.start()

    def chunk(index, mask, first):
        at = pl.multiple_of(index * wide, wide)
        for copy in copies(index):
            copy.wait()
        latent = latents[pl.ds(at, wide), :]
        for head in range(HEADS):
            scores = dot(queries[head, :, :QK_DIM], keys[head, :, pl.ds(at, wide)])
            weights = jnp.exp2(scores)
            if mask is not None:
                weights = jnp.where(mask, weights, 0.0)
            part = weights[:, :LANES]
            for lanes in range(LANES, wide, LANES):
                part = part + weights[:, lanes : lanes + LANES]
            numer = dot(weights.astype(BF16), latent)
            if first:
                totals[head] = part
                sums[head] = numer
            else:
                totals[head] += part
                sums[head] += numer

    row = lax.broadcasted_iota(jnp.int32, (QROWS, wide), 0)
    col = lax.broadcasted_iota(jnp.int32, (QROWS, wide), 1)
    query_pos = z * BLOCK + (row // ROWS) * (2 * ROWS) + p * ROWS + row % ROWS
    key_pos = (4 * pair + col // (2 * ROWS)) * BLOCK + x * (2 * ROWS) + col % (2 * ROWS)
    chunk(pair, key_pos <= query_pos, True)

    def body(index, carry):
        chunk(pair - 1 - index, None, False)
        return carry

    lax.fori_loop(0, pair, body, 0)
    value_copy.wait()
    ones = jnp.ones((HALO, LANES), F32)
    line = lax.broadcasted_iota(jnp.int32, (HALO, QROWS), 0)
    for chip in range(CHIPS):
        tail = jnp.zeros((HALO, QROWS), F32)
        for slot in range(2):
            head = 2 * chip + slot
            values = value_up[:, head * VALUE_DIM : (head + 1) * VALUE_DIM]
            numer = dot(sums[head].astype(BF16), values)
            out[chip, :QROWS, slot * LANES : (slot + 1) * LANES] = numer.astype(BF16)
            denom = dot(ones, totals[head], ((1,), (1,)), lax.Precision.HIGHEST)
            high = denom.astype(BF16).astype(F32)
            tail = jnp.where(line == 2 * slot, high, tail)
            tail = jnp.where(line == 2 * slot + 1, denom - high, tail)
        out[chip, QROWS:, :] = tail.astype(BF16)


def pool_kernel(pool_rows, halo, maps, scale, keep_out, give_out):
    z, x, p = place()
    lane = lax.broadcasted_iota(jnp.int32, (1, LANES), 1)
    early = lane < GROUP_DIM
    current = pool_rows[...].astype(F32)
    two = jnp.concatenate([halo[...].astype(F32), current], axis=0)
    two = two + pltpu.roll(two, 1, 0)
    four = two + pltpu.roll(two, 2, 0)
    eight = four + pltpu.roll(four, 4, 0)
    sixteen = eight + pltpu.roll(eight, 8, 0)
    short = jnp.where(early, two, four)
    long = jnp.where(early, eight, sixteen)
    total = jnp.where(p == 0, short, long)[HALO:]
    window = jnp.where(early, 2, 4) * jnp.where(p == 0, 1, 4)
    row = lax.broadcasted_iota(jnp.int32, (BLOCK, 1), 0)
    divisor = jnp.minimum((z * BLOCK + row).astype(F32) + 1.0, window.astype(F32))
    means = (total / divisor - current).astype(BF16)
    empty = jnp.zeros((GROUP_DIM, GROUP_DIM), F32)
    upper = jnp.concatenate([maps[4 * x + 2 * p].astype(F32), empty], axis=1)
    lower = jnp.concatenate([empty, maps[4 * x + 2 * p + 1].astype(F32)], axis=1)
    weights = jnp.concatenate([upper, lower], axis=0).astype(BF16)
    pooled = (dot(means, weights) * scale[...]).reshape(CHIPS, 2, ROWS, LANES)
    even = pooled[:, 0].reshape(QROWS, LANES)
    odd = pooled[:, 1].reshape(QROWS, LANES)
    keep_out[...] = jnp.where(p == 0, even, odd)
    give_out[...] = jnp.where(p == 0, odd, even)


def join_kernel(parts, pool_own, pool_other, attended_out, squares_out):
    tail = jnp.zeros((HALO, QROWS), F32)
    for chip in range(CHIPS):
        tail = tail + parts[chip, QROWS:, :].astype(F32)
    columns = jnp.transpose(tail)
    squares = jnp.zeros((QROWS, LANES), F32)
    for slot in range(2):
        numer = jnp.zeros((QROWS, LANES), F32)
        for chip in range(CHIPS):
            numer = numer + parts[chip, :QROWS, slot * LANES : (slot + 1) * LANES].astype(F32)
        denom = columns[:, 2 * slot : 2 * slot + 1] + columns[:, 2 * slot + 1 : 2 * slot + 2]
        attended = numer / denom
        attended_out[slot] = attended
        squares = squares + attended * attended
    ones = jnp.ones((8, LANES), F32)
    exact = lax.Precision.HIGHEST
    line = lax.broadcasted_iota(jnp.int32, (8, QROWS), 0)
    mine = dot(ones, squares, ((1,), (1,)), exact)
    pooled = pool_own[...] * pool_own[...] + pool_other[...] * pool_other[...]
    pools = dot(ones, pooled, ((1,), (1,)), exact)
    for chip in range(CHIPS):
        squares_out[chip] = jnp.where(line < 4, mine, pools)


def mix_kernel(
    attended,
    pool_own,
    pool_other,
    squares,
    gain_a,
    gain_p,
    own_attention,
    own_pool,
    other_out,
    partial_out,
):
    _, _, p = place()
    total = jnp.transpose(squares[0] + squares[1] + squares[2] + squares[3])
    attention_factor = lax.rsqrt(total[:, 0:1] * (1.0 / (HEADS * VALUE_DIM)) + EPS)
    pool_factor = lax.rsqrt(total[:, 4:5] * (1.0 / (HEADS * VALUE_DIM)) + EPS)
    sides = []
    rows = other_out[2 * LANES :, :LANES].astype(F32)
    far = rows[0:4] + rows[4:8] + rows[8:12]
    for first, second, pooled, slot in (
        (gain_a[...], gain_p[...], pool_own, p),
        (far[0:1, :], far[1:2, :], pool_other, 1 - p),
    ):
        sides.append((attended[slot] * attention_factor * first).astype(BF16))
        sides.append((pooled[...] * pool_factor * second).astype(BF16))
    mine = jnp.concatenate(sides[:2], axis=1)
    theirs = jnp.concatenate(sides[2:], axis=1)
    step = 512
    for at in range(0, D, step):
        weights = jnp.concatenate(
            [own_attention[:, at : at + step], own_pool[:, at : at + step]], axis=0
        )
        both = dot(mine, weights) + dot(theirs, other_out[: 2 * LANES, at : at + step])
        partial_out[:, :, at : at + step] = both.astype(BF16).reshape(CHIPS, ROWS, step)


def sum_kernel(parts, out):
    total = parts[0].astype(F32) + parts[1].astype(F32)
    total = total + parts[2].astype(F32) + parts[3].astype(F32)
    out[0] = total.astype(BF16)


def local(
    tokens,
    input_gain,
    query_weight,
    latent_down,
    rotary_down,
    pool_down,
    key_up,
    value_up,
    query_gain,
    key_gain,
    pool_weight,
    pool_scale,
    attention_gain,
    pool_gain,
    attention_out,
    pool_out,
):
    inside, starts, turned, begins = (jnp.asarray(t) for t in angle_tables())

    def chip():
        return lax.axis_index("tp") // 2

    def up_to(step):
        return jnp.minimum(step, lax.axis_index("sp") // 4)

    normed, latent_rows = whole(
        norm_kernel,
        (far((2 * CHIPS, ROWS, D), BF16), far((PACK, KV_LATENT), BF16)),
        tokens,
        input_gain[None],
        latent_down,
        rotary_down.T,
        room=56,
    )
    rows = among_all(normed)
    own_latents = lax.all_gather(latent_rows, "sp", axis=0, tiled=False)
    other_latents = to_partner(own_latents)

    queries, pool_rows, tail = whole(
        project_kernel,
        (
            far((2 * CHIPS, QROWS, LANES), BF16),
            shape((BLOCK, LANES), BF16),
            shape((HALO, LANES), BF16),
        ),
        rows,
        query_weight.T,
        pool_down,
        query_gain[None],
        inside,
        starts,
        room=ROOM_PROJECT,
    )
    queries = among_all(queries)
    halo = lax.ppermute(tail, "sp", [(i, i + 1) for i in range(BLOCKS - 1)])

    latent_spec = pl.BlockSpec((4, PACK, KV_LATENT), lambda i: (up_to(i), 0, 0))
    expand = pl.pallas_call(
        expand_kernel,
        grid=(BLOCKS // 4,),
        out_shape=(far((HEADS, QK_DIM, KEYS), BF16), far((KEYS, KV_LATENT), BF16)),
        in_specs=[
            latent_spec,
            latent_spec,
            pl.BlockSpec((KV_LATENT, HEADS * NOPE_DIM), lambda i: (0, 0)),
            pl.BlockSpec((1, QK_DIM), lambda i: (0, 0)),
            pl.BlockSpec((2, 1, ROPE_DIM // 2, LANES), lambda i: (0, chip(), 0, 0)),
            pl.BlockSpec((2, 4, ROPE_DIM // 2, LANES), lambda i: (0, up_to(i), 0, 0)),
        ],
        out_specs=[
            pl.BlockSpec((HEADS, QK_DIM, QUAD), lambda i: (0, 0, up_to(i))),
            pl.BlockSpec((QUAD, KV_LATENT), lambda i: (up_to(i), 0)),
        ],
        scratch_shapes=[pltpu.VMEM((HEADS * NOPE_DIM, KV_LATENT), BF16)],
        compiler_params=pltpu.CompilerParams(vmem_limit_bytes=56 * MIB),
        name="expand",
    )
    keys, latents = expand(own_latents, other_latents, key_up, key_gain[None], turned, begins)

    numer = whole(
        attend_kernel,
        far((CHIPS, QROWS + HALO, 2 * LANES), BF16),
        queries,
        keys,
        latents,
        value_up,
        specs=[VECTOR, AWAY, AWAY, AWAY],
        scratch=(
            pltpu.VMEM((HEADS, QK_DIM, KEYS), BF16),
            pltpu.VMEM((KEYS, KV_LATENT), BF16),
            pltpu.VMEM((KV_LATENT, HEADS * VALUE_DIM), BF16),
            pltpu.VMEM((HEADS, QROWS, KV_LATENT), F32),
            pltpu.VMEM((HEADS, QROWS, LANES), F32),
            pltpu.SemaphoreType.DMA((2, BLOCKS // 4 + 1)),
        ),
        room=56,
    )
    parts = among_chips(numer)

    pool_own, pool_give = whole(
        pool_kernel,
        (shape((QROWS, LANES), F32), shape((QROWS, LANES), F32)),
        pool_rows,
        halo,
        pool_weight,
        pool_scale[None],
    )
    pool_other = to_partner(pool_give)
    other_out = to_partner(
        whole(
            out_bundle_kernel,
            shape((2 * LANES + HALO, D), BF16),
            attention_out,
            pool_out,
            attention_gain[None],
            pool_gain[None],
        ),
    )
    attended, squares = whole(
        join_kernel,
        (shape((2, QROWS, LANES), F32), far((CHIPS, 8, QROWS), F32)),
        parts,
        pool_own,
        pool_other,
    )
    squares = among_chips(squares)
    partial = whole(
        mix_kernel,
        far((CHIPS, ROWS, D), BF16),
        attended,
        pool_own,
        pool_other,
        squares,
        attention_gain[None],
        pool_gain[None],
        attention_out,
        pool_out,
        other_out,
    )
    return whole(sum_kernel, shape((1, ROWS, D), BF16), among_chips(partial))


def solution(mesh):
    placed = (
        P("fs", ("sp", "tp"), None),
        P(),
        P(None, "tp"),
        P(),
        P(),
        P(None, "tp"),
        P(),
        P(),
        P(),
        P(),
        P(),
        P("tp"),
        P("tp"),
        P("tp"),
        P("tp", None),
        P("tp", None),
    )

    return jax.shard_map(
        local, mesh=mesh, in_specs=placed, out_specs=P("fs", ("sp", "tp"), None), check_vma=False
    )
```

time: 130 us -> 128 us (0.985)
  the two profiles are of different devices: /device:TPU:480 before, /device:TPU:408 now
where the time goes in v3:
time: 128 us; the launch traced here: 127 us
  blocking collectives  51.7 us (40%)
  Pallas kernels  29.1 us (23%)
  starting transfers between devices  25.3 us (20%)
  waiting for transfers between devices  15.1 us (12%)
  local copies, waits for them, and re-layouts  6.17 us (5%)
    all_gather x1, blocking collectives, local(): own_latents = lax.all_gather(latent_rows, 'sp', axis=0, tiled=False)  33.9 us
    pallas_call x8, Pallas kernels, whole(): pl.pallas_call(kernel, grid=() if specs is None else (1,), out_shape=out_...  22.3 us
    all_to_all x1, blocking collectives, among_chips(): lax.all_to_all(array, 'tp', 0, 0, axis_index_groups=SAME_CORE, tiled=True)  17.7 us
    all_to_all x2, starting transfers between devices, among_all(): return lax.all_to_all(array, 'tp', 0, 0, tiled=True)  8.91 us
    all_to_all x2, starting transfers between devices, among_chips(): lax.all_to_all(array, 'tp', 0, 0, axis_index_groups=SAME_CORE, tiled=True)  8.23 us
    pallas_call x1, Pallas kernels, local(): expand(own_latents, other_latents, key_up, key_gain[None], turned, begins)  6.78 us
    ppermute x3, starting transfers between devices, to_partner(): return lax.ppermute(array, 'tp', [(i, i ^ 1) for i in range(2 * CHIPS)])  6.22 us
    unnamed x38, local copies, waits for them, and re-layouts  6.17 us
  transfers between devices with their start and end apart: 8, of which 4 were waited for; matrix products, arithmetic and copies ran while one was open for 0% of the time, Pallas kernels for 17%

profile of v3, /device:TPU:408, one launch (start us, length us, event | category | flops | bytes accessed | tf_op | source)
XLA Modules:
  0.0 127.5 jit_solution(2293596235895220810)
XLA Ops:
  0.0 3.0 %shard_map.190 = (bf16[8,64,2048]{2,1,0:T(8,128)(2,1)}, bf16[72,256]{1,0:T(8,128)(2,1)}) custom-call(bf16[1,64,2048]{2,1,0:T(8,128)(2,1)} %tokens.1, f32[1,2048]{1,0:T(1,128)} %bitcast.17, bf16[2048,256]{1,0:T(8,128)(2,1)} %latent_down.1, bf16[32,2048]{1,0:T(8,128)(2,1)} %bitcast.16), custom_call_target="tpu_custom_call" | custom-call | tf_op jit(solution)/shard_map/pallas_call | solution.py:74
  3.0 4.4 %all-to-all-start = ((bf16[8,64,2048]{2,1,0:T(8,128)(2,1)}), bf16[8,64,2048]{2,1,0:T(8,128)(2,1)S(1)}, u32[]{:S(2)}, u32[]{:S(2)}) async-start(bf16[8,64,2048]{2,1,0:T(8,128)(2,1)} %get-tuple-element.16), calls=%async_computation | async-start | bytes 4194304 | tf_op jit(solution)/shard_map/all_to_all | solution.py:59
  8.8 1.1 shard_map.195
  9.9 2.4 %collective-permute-start.3 = (bf16[272,2048]{1,0:T(8,128)(2,1)}, bf16[272,2048]{1,0:T(8,128)(2,1)}, u32[]{:S(2)}, u32[]{:S(2)}) collective-permute-start(bf16[272,2048]{1,0:T(8,128)(2,1)} %shard_map.195), channel_id=1, source_target_pairs={{0,1},{1,0},{2,3},{3,2},{4,5},{5,4},{6,7},{7,6},{8,9},{9,8},{10,11... | collective-permute-start | bytes 3342344 | tf_op jit(solution)/shard_map/ppermute | solution.py:63
  12.4 33.9 %all-gather = bf16[1152,256]{1,0:T(8,128)(2,1)} all-gather(bf16[72,256]{1,0:T(8,128)(2,1)S(1)} %copy-done.18), channel_id=2, replica_groups=mesh['sp'=16,'fs'=4,'tp'=8] {'sp'}, dimensions={0}, use_global_device_ids=true | all-gather | bytes 626688 | tf_op jit(solution)/shard_map/all_gather | solution.py:426
  46.3 1.9 %collective-permute-start = (bf16[16,72,256]{2,1,0:T(8,128)(2,1)}, bf16[16,72,256]{2,1,0:T(8,128)(2,1)}, u32[]{:S(2)}, u32[]{:S(2)}) collective-permute-start(bf16[16,72,256]{2,1,0:T(8,128)(2,1)} %bitcast.4.own), channel_id=1, source_target_pairs={{0,1},{1,0},{2,3},{3,2},{4,5},{5,4},{6,7},{7,6},{8,9},{9,8},{10,11... | collective-permute-start | bytes 1769480 | tf_op jit(solution)/shard_map/ppermute | solution.py:63
  48.2 1.0 copy-done.2
  49.3 1.0 copy-done.3
  51.0 2.5 %shard_map.191 = (bf16[8,256,128]{2,1,0:T(8,128)(2,1)}, bf16[512,128]{1,0:T(8,128)(2,1)S(1)}, bf16[16,128]{1,0:T(8,128)(2,1)S(1)}) custom-call(bf16[8,64,2048]{2,1,0:T(8,128)(2,1)S(1)} %all-to-all-done.rows, bf16[96,2048]{1,0:T(8,128)(2,1)S(1)} %bitcast.9, bf16[2048,128]{1,0:T(8,128)(2,1)S(1)} %copy-done.2, f32[1,96]{1,0:T(1,128)S(1)} %bitcast.15, ...), custom_call_target="tpu_custom_call" | custom-call | tf_op jit(solution)/shard_map/pallas_call | solution.py:74
  54.8 4.5 %all-to-all-start.1 = ((bf16[8,256,128]{2,1,0:T(8,128)(2,1)}), bf16[8,256,128]{2,1,0:T(8,128)(2,1)S(1)}, u32[]{:S(2)}, u32[]{:S(2)}) async-start(bf16[8,256,128]{2,1,0:T(8,128)(2,1)} %get-tuple-element.17), calls=%async_computation.1 | async-start | bytes 1048576 | tf_op jit(solution)/shard_map/all_to_all | solution.py:59
  59.2 6.8 %expand.1 = (bf16[8,96,2048]{2,1,0:T(8,128)(2,1)}, bf16[2048,256]{1,0:T(8,128)(2,1)}) custom-call(bf16[16,72,256]{2,1,0:T(8,128)(2,1)} %bitcast.4.own, bf16[16,72,256]{2,1,0:T(8,128)(2,1)} %collective-permute-done.other, bf16[256,512]{1,0:T(8,128)(2,1)} %key_up.1, f32[1,96]{1,0:T(1,128)} %bitcast.18, f32[2,4,16,128]{3,2,1,0:T(8,128)} %constant.10.clone.inside, ...), custom_call_target="tpu_custom_call" | custom-call | tf_op jit(solution)/shard_map/expand/pallas_call | solution.py:468
  66.0 3.5 %all-to-all-done.1.queries = bf16[8,256,128]{2,1,0:T(8,128)(2,1)S(1)} async-done(((bf16[8,256,128]{2,1,0:T(8,128)(2,1)}), bf16[8,256,128]{2,1,0:T(8,128)(2,1)S(1)}, u32[]{:S(2)}, u32[]{:S(2)}) %all-to-all-start.1) | async-done | bytes 524320 | tf_op jit(solution)/shard_map/all_to_all | solution.py:59
  70.3 10.2 %shard_map.192 = bf16[4,272,256]{2,1,0:T(8,128)(2,1)} custom-call(bf16[8,256,128]{2,1,0:T(8,128)(2,1)} %copy-done.17, bf16[8,96,2048]{2,1,0:T(8,128)(2,1)} %get-tuple-element.19.keys_far, bf16[2048,256]{1,0:T(8,128)(2,1)} %get-tuple-element.20.latents_far, bf16[256,1024]{1,0:T(8,128)(2,1)} %value_far.1), custom_call_target="tpu_custom_call" | custom-call | tf_op jit(solution)/shard_map/pallas_call | solution.py:74
  80.5 3.5 %all-to-all-start.2 = ((bf16[4,272,256]{2,1,0:T(8,128)(2,1)}), bf16[4,272,256]{2,1,0:T(8,128)(2,1)S(1)}, u32[]{:S(2)}, u32[]{:S(2)}) async-start(bf16[4,272,256]{2,1,0:T(8,128)(2,1)} %shard_map.192), calls=%async_computation.2 | async-start | bytes 1114112 | tf_op jit(solution)/shard_map/all_to_all | solution.py:55
  84.0 1.9 %collective-permute-start.1 = (bf16[16,128]{1,0:T(8,128)(2,1)S(1)}, bf16[16,128]{1,0:T(8,128)(2,1)S(1)}, u32[]{:S(2)}, u32[]{:S(2)}) collective-permute-start(bf16[16,128]{1,0:T(8,128)(2,1)S(1)} %copy-done.16), channel_id=1, source_target_pairs={{0,32},{32,64},{64,96},{96,128},{128,160},{160,192},{192,224},{224... | collective-permute-start | bytes 12296 | tf_op jit(solution)/shard_map/ppermute | solution.py:445
  86.0 4.8 %collective-permute-done.1.halo = bf16[16,128]{1,0:T(8,128)(2,1)S(1)} collective-permute-done((bf16[16,128]{1,0:T(8,128)(2,1)S(1)}, bf16[16,128]{1,0:T(8,128)(2,1)S(1)}, u32[]{:S(2)}, u32[]{:S(2)}) %collective-permute-start.1) | collective-permute-done | bytes 4128 | tf_op jit(solution)/shard_map/ppermute | solution.py:445
  91.1 1.9 %collective-permute-start.2 = (f32[256,128]{1,0:T(8,128)S(1)}, f32[256,128]{1,0:T(8,128)S(1)}, u32[]{:S(2)}, u32[]{:S(2)}) collective-permute-start(f32[256,128]{1,0:T(8,128)S(1)} %get-tuple-element.24), channel_id=1, source_target_pairs={{0,1},{1,0},{2,3},{3,2},{4,5},{5,4},{6,7},{7,6},{8,9},{9,8},{10,11... | collective-permute-start | bytes 393224 | tf_op jit(solution)/shard_map/ppermute | solution.py:63
  93.0 1.3 %collective-permute-done.2.pool_other = f32[256,128]{1,0:T(8,128)S(1)} collective-permute-done((f32[256,128]{1,0:T(8,128)S(1)}, f32[256,128]{1,0:T(8,128)S(1)}, u32[]{:S(2)}, u32[]{:S(2)}) %collective-permute-start.2) | collective-permute-done | bytes 131104 | tf_op jit(solution)/shard_map/ppermute | solution.py:63
  94.3 1.2 shard_map.194
  95.6 4.7 %all-to-all-start.3 = ((f32[4,8,256]{2,1,0:T(8,128)}), f32[4,8,256]{2,1,0:T(8,128)S(1)}, u32[]{:S(2)}, u32[]{:S(2)}) async-start(f32[4,8,256]{2,1,0:T(8,128)} %get-tuple-element.26), calls=%async_computation.3 | async-start | bytes 65536 | tf_op jit(solution)/shard_map/all_to_all | solution.py:55
  100.3 5.4 %all-to-all-done.3.squares = f32[4,8,256]{2,1,0:T(8,128)S(1)} async-done(((f32[4,8,256]{2,1,0:T(8,128)}), f32[4,8,256]{2,1,0:T(8,128)S(1)}, u32[]{:S(2)}, u32[]{:S(2)}) %all-to-all-start.3) | async-done | bytes 32800 | tf_op jit(solution)/shard_map/all_to_all | solution.py:55
  105.8 3.1 %shard_map.196 = bf16[4,64,2048]{2,1,0:T(8,128)(2,1)} custom-call(f32[2,256,128]{2,1,0:T(8,128)S(1)} %get-tuple-element.25.attended, f32[256,128]{1,0:T(8,128)S(1)} %get-tuple-element.23.pool_own, f32[256,128]{1,0:T(8,128)S(1)} %collective-permute-done.2.pool_other, f32[4,8,256]{2,1,0:T(8,128)S(1)} %all-to-all-done.3.squares, f32[1,128]{1,0:T(1,128)S(1)} %bitcast.11, ...), custom_call_target="tpu_custom_call" | custom-call | tf_op jit(solution)/shard_map/pallas_call | solution.py:74
  108.9 17.7 %all_to_all.25.parts = bf16[4,64,2048]{2,1,0:T(8,128)(2,1)S(1)} all-to-all(bf16[4,64,2048]{2,1,0:T(8,128)(2,1)} %shard_map.196), channel_id=1, replica_groups={{0,2,4,6},{1,3,5,7},{8,10,12,14},{9,11,13,15},{16,18,20,22},{17,19,21,2..., dimensions={0} | all-to-all | bytes 2097152 | tf_op jit(solution)/shard_map/all_to_all | solution.py:55
  126.6 0.8 shard_map.197
  (41 shorter events, 4.4 us)
Async XLA Ops:
  3.0 4.5 %copy-start = (bf16[128,2048]{1,0:T(8,128)(2,1)S(1)}, bf16[128,2048]{1,0:T(8,128)(2,1)}, u32[]{:S(2)}) copy-start(bf16[128,2048]{1,0:T(8,128)(2,1)} %own_attention.1) | copy-start | bytes 1572868
  3.0 4.5 %copy-start.1 = (bf16[128,2048]{1,0:T(8,128)(2,1)S(1)}, bf16[128,2048]{1,0:T(8,128)(2,1)}, u32[]{:S(2)}) copy-start(bf16[128,2048]{1,0:T(8,128)(2,1)} %own_pool.1) | copy-start | bytes 1572868
  3.0 45.2 %all-to-all-start = ((bf16[8,64,2048]{2,1,0:T(8,128)(2,1)}), bf16[8,64,2048]{2,1,0:T(8,128)(2,1)S(1)}, u32[]{:S(2)}, u32[]{:S(2)}) async-start(bf16[8,64,2048]{2,1,0:T(8,128)(2,1)} %get-tuple-element.16), calls=%async_computation | async-start | bytes 4194304 | tf_op jit(solution)/shard_map/all_to_all | solution.py:59
  7.4 40.8 %copy-start.4 = (bf16[2048,96]{0,1:T(8,128)(2,1)S(1)}, bf16[2048,96]{0,1:T(8,128)(2,1)}, u32[]{:S(2)}) copy-start(bf16[2048,96]{0,1:T(8,128)(2,1)} %param.22) | copy-start | bytes 1179652
  7.4 40.8 %copy-start.8 = (f32[2,16,128]{2,1,0:T(8,128)S(1)}, f32[2,16,128]{2,1,0:T(8,128)}, u32[]{:S(2)}) copy-start(f32[2,16,128]{2,1,0:T(8,128)} %constant.9.clone.starts) | copy-start | bytes 49156
  7.5 0.7 copy-start.9
  8.2 0.7 copy-start.11
  8.8 3.5 %copy-start.18 = (bf16[72,256]{1,0:T(8,128)(2,1)S(1)}, bf16[72,256]{1,0:T(8,128)(2,1)}, u32[]{:S(2)}) copy-start(bf16[72,256]{1,0:T(8,128)(2,1)} %get-tuple-element.18) | copy-start | bytes 110596
  9.9 90.4 %collective-permute-start.3 = (bf16[272,2048]{1,0:T(8,128)(2,1)}, bf16[272,2048]{1,0:T(8,128)(2,1)}, u32[]{:S(2)}, u32[]{:S(2)}) collective-permute-start(bf16[272,2048]{1,0:T(8,128)(2,1)} %shard_map.195), channel_id=1, source_target_pairs={{0,1},{1,0},{2,3},{3,2},{4,5},{5,4},{6,7},{7,6},{8,9},{9,8},{10,11... | collective-permute-start | bytes 3342344 | tf_op jit(solution)/shard_map/ppermute | solution.py:63
  46.3 13.0 %collective-permute-start = (bf16[16,72,256]{2,1,0:T(8,128)(2,1)}, bf16[16,72,256]{2,1,0:T(8,128)(2,1)}, u32[]{:S(2)}, u32[]{:S(2)}) collective-permute-start(bf16[16,72,256]{2,1,0:T(8,128)(2,1)} %bitcast.4.own), channel_id=1, source_target_pairs={{0,1},{1,0},{2,3},{3,2},{4,5},{5,4},{6,7},{7,6},{8,9},{9,8},{10,11... | collective-permute-start | bytes 1769480 | tf_op jit(solution)/shard_map/ppermute | solution.py:63
  48.2 1.0 copy-start.2
  49.3 1.0 copy-start.3
  54.8 14.8 %all-to-all-start.1 = ((bf16[8,256,128]{2,1,0:T(8,128)(2,1)}), bf16[8,256,128]{2,1,0:T(8,128)(2,1)S(1)}, u32[]{:S(2)}, u32[]{:S(2)}) async-start(bf16[8,256,128]{2,1,0:T(8,128)(2,1)} %get-tuple-element.17), calls=%async_computation.1 | async-start | bytes 1048576 | tf_op jit(solution)/shard_map/all_to_all | solution.py:59
  69.5 0.8 copy-start.17
  70.3 13.7 %copy-start.16 = (bf16[16,128]{1,0:T(8,128)(2,1)S(1)}, bf16[16,128]{1,0:T(8,128)(2,1)}, u32[]{:S(2)}) copy-start(bf16[16,128]{1,0:T(8,128)(2,1)} %copy-done.15) | copy-start | bytes 12292
  70.3 20.4 %copy-start.5 = (bf16[16,64,64]{2,1,0:T(8,128)(2,1)S(1)}, bf16[16,64,64]{2,1,0:T(8,128)(2,1)}, u32[]{:S(2)}) copy-start(bf16[16,64,64]{2,1,0:T(8,128)(2,1)} %maps.1) | copy-start | bytes 393220
  70.3 20.4 %copy-start.7 = (bf16[512,128]{1,0:T(8,128)(2,1)S(1)}, bf16[512,128]{1,0:T(8,128)(2,1)}, u32[]{:S(2)}) copy-start(bf16[512,128]{1,0:T(8,128)(2,1)} %copy-done.6) | copy-start | bytes 393220
  70.3 20.4 %copy-start.13 = (f32[128]{0:T(128)S(1)}, f32[128]{0:T(128)}, u32[]{:S(2)}) copy-start(f32[128]{0:T(128)} %param.31) | copy-start | bytes 1540
  80.5 25.3 %copy-start.10 = (f32[128]{0:T(128)S(1)}, f32[128]{0:T(128)}, u32[]{:S(2)}) copy-start(f32[128]{0:T(128)} %param.32) | copy-start | bytes 1540
  80.5 25.3 %copy-start.12 = (f32[128]{0:T(128)S(1)}, f32[128]{0:T(128)}, u32[]{:S(2)}) copy-start(f32[128]{0:T(128)} %param.33) | copy-start | bytes 1540
  80.5 13.8 %all-to-all-start.2 = ((bf16[4,272,256]{2,1,0:T(8,128)(2,1)}), bf16[4,272,256]{2,1,0:T(8,128)(2,1)S(1)}, u32[]{:S(2)}, u32[]{:S(2)}) async-start(bf16[4,272,256]{2,1,0:T(8,128)(2,1)} %shard_map.192), calls=%async_computation.2 | async-start | bytes 1114112 | tf_op jit(solution)/shard_map/all_to_all | solution.py:55
  84.0 6.7 %collective-permute-start.1 = (bf16[16,128]{1,0:T(8,128)(2,1)S(1)}, bf16[16,128]{1,0:T(8,128)(2,1)S(1)}, u32[]{:S(2)}, u32[]{:S(2)}) collective-permute-start(bf16[16,128]{1,0:T(8,128)(2,1)S(1)} %copy-done.16), channel_id=1, source_target_pairs={{0,32},{32,64},{64,96},{96,128},{128,160},{160,192},{192,224},{224... | collective-permute-start | bytes 12296 | tf_op jit(solution)/shard_map/ppermute | solution.py:445
  91.1 3.2 %collective-permute-start.2 = (f32[256,128]{1,0:T(8,128)S(1)}, f32[256,128]{1,0:T(8,128)S(1)}, u32[]{:S(2)}, u32[]{:S(2)}) collective-permute-start(f32[256,128]{1,0:T(8,128)S(1)} %get-tuple-element.24), channel_id=1, source_target_pairs={{0,1},{1,0},{2,3},{3,2},{4,5},{5,4},{6,7},{7,6},{8,9},{9,8},{10,11... | collective-permute-start | bytes 393224 | tf_op jit(solution)/shard_map/ppermute | solution.py:63
  95.6 10.2 %all-to-all-start.3 = ((f32[4,8,256]{2,1,0:T(8,128)}), f32[4,8,256]{2,1,0:T(8,128)S(1)}, u32[]{:S(2)}, u32[]{:S(2)}) async-start(f32[4,8,256]{2,1,0:T(8,128)} %get-tuple-element.26), calls=%async_computation.3 | async-start | bytes 65536 | tf_op jit(solution)/shard_map/all_to_all | solution.py:55
  (3 other events, 1.9 us)

commit v4 on v3

--- a/solution.py
+++ b/solution.py
@@ -64,19 +64,19 @@
 
 
 MIB = 1024 * 1024
-ROOM_PROJECT = 14
+ROOM_PROJECT = 52
 VECTOR = pl.BlockSpec(memory_space=pltpu.VMEM)
 AWAY = pl.BlockSpec(memory_space=pltpu.HBM)
 
 
-def whole(kernel, out_shape, *args, specs=None, scratch=(), room=14):
+def whole(kernel, out_shape, *args, specs=None, outs=None, scratch=(), room=14):
     single = not isinstance(out_shape, (list, tuple))
     return pl.pallas_call(
         kernel,
         grid=() if specs is None else (1,),
         out_shape=out_shape,
         in_specs=[VECTOR] * len(args) if specs is None else specs,
-        out_specs=VECTOR if single else [VECTOR] * len(out_shape),
+        out_specs=outs or (VECTOR if single else [VECTOR] * len(out_shape)),
         scratch_shapes=list(scratch),
         compiler_params=pltpu.CompilerParams(vmem_limit_bytes=room * MIB),
     )(*args)
@@ -115,17 +115,21 @@
     return cosine, sine
 
 
-def norm_kernel(tokens, gain, latent_down, rotary_down, normed_out, latent_out):
+def norm_kernel(
+    tokens, gain, latent_down, rotary_down, query_gain, normed_out, latent_out, gain_out
+):
     source = tokens[0].astype(F32)
     scale = lax.rsqrt(jnp.mean(source * source, axis=-1, keepdims=True) + EPS)
     normed = (source * scale * gain[...]).astype(BF16)
     for member in range(2 * CHIPS):
         normed_out[member] = normed
-    latent = dot(normed, latent_down[...]).astype(BF16)
     rotary = dot(rotary_down[...], normed, ((1,), (1,)))
     packed = jnp.concatenate([rotary[at : at + 8] for at in range(0, ROPE_DIM, 8)], axis=1)
-    latent_out[:ROWS] = latent
     latent_out[ROWS:] = packed.astype(BF16)
+    wide = jnp.concatenate([query_gain[...], jnp.zeros((1, LANES - QK_DIM), F32)], axis=1)
+    wide = wide * (math.log2(math.e) / math.sqrt(QK_DIM))
+    gain_out[...] = jnp.broadcast_to(wide, (8, LANES))
+    latent_out[:ROWS] = dot(normed, latent_down[...]).astype(BF16)
 
 
 def out_bundle_kernel(attention_out, pool_out, gain_a, gain_p, both):
@@ -142,26 +146,50 @@
     both[2 * LANES :, :] = jnp.concatenate([rows] * (D // LANES), axis=1).astype(BF16)
 
 
-def project_kernel(rows, query_down, pool_down, gain, inside, starts, query_out, pool_out, tail_out):
+def project_kernel(
+    rows_far,
+    query_down,
+    pool_down,
+    gain,
+    inside,
+    starts,
+    query_out,
+    pool_out,
+    tail_out,
+    rows,
+    arrived,
+):
     z, _, _ = place()
-    piece = rows[...].reshape(BLOCK, D)
+    per = CHIPS
+    copies = []
+    for part in range(2):
+        span = pl.ds(part * per, per)
+        copies.append(
+            pltpu.make_async_copy(rows_far.at[span], rows.at[span], arrived.at[part])
+        )
+        copies[-1].start()
     start_cos = starts[0, pl.ds(z, 1), :]
     start_sin = starts[1, pl.ds(z, 1), :]
     cosine, sine = at_block(inside[0], inside[1], start_cos, start_sin)
     empty = jnp.zeros((LANES - QK_DIM, D), BF16)
-    wide_gain = jnp.concatenate([gain[...], jnp.zeros((1, LANES - QK_DIM), F32)], axis=1)
-    wide_gain = wide_gain * (math.log2(math.e) / math.sqrt(QK_DIM))
-    raw = dot(piece, jnp.concatenate([query_down[...], empty], axis=0), ((1,), (1,)))
-    square = jnp.sum(raw * raw, axis=-1, keepdims=True) * (1.0 / QK_DIM)
-    normal = raw * lax.rsqrt(square + EPS) * wide_gain
-    queries = turn(normal, cosine, sine).astype(BF16).reshape(CHIPS, 2, ROWS, LANES)
-    for side in range(2):
-        mine = queries[:, side].reshape(QROWS, LANES)
-        for chip in range(CHIPS):
-            query_out[2 * chip + side] = mine
-    result = dot(piece, pool_down[...]).astype(BF16)
-    pool_out[...] = result
-    tail_out[...] = result[BLOCK - HALO :]
+    query_wide = jnp.concatenate([query_down[...], empty], axis=0)
+    half = per * ROWS
+    for part in range(2):
+        copies[part].wait()
+        piece = rows[part * per : (part + 1) * per].reshape(half, D)
+        raw = dot(piece, query_wide, ((1,), (1,)))
+        square = jnp.sum(raw * raw, axis=-1, keepdims=True) * (1.0 / QK_DIM)
+        normal = raw * lax.rsqrt(square + EPS) * gain[0:1, :]
+        span = slice(part * half, (part + 1) * half)
+        queries = turn(normal, cosine[span], sine[span]).astype(BF16)
+        for member in range(per):
+            mine = queries[member * ROWS : (member + 1) * ROWS]
+            side, chip = member % 2, (part * per + member) // 2
+            for target in range(CHIPS):
+                query_out[2 * target + side, chip * ROWS : (chip + 1) * ROWS] = mine
+        result = dot(piece, pool_down[...]).astype(BF16)
+        pool_out[part * half : (part + 1) * half] = result
+    tail_out[...] = result[half - HALO :]
 
 
 def expand_kernel(own, other, key_up, gain, inside, starts, keys_out, latent_out, key_up_t):
@@ -214,7 +242,18 @@
 
 
 def attend_kernel(
-    queries, keys_far, latents_far, value_far, out, keys, latents, value_up, sums, totals, arrived
+    queries,
+    keys_far,
+    latents_far,
+    value_far,
+    out_far,
+    out,
+    keys,
+    latents,
+    value_up,
+    sums,
+    totals,
+    arrived,
 ):
     z, x, p = place()
     wide = QUAD
@@ -244,18 +283,18 @@
     value_copy = pltpu.make_async_copy(value_far, value_up, arrived.at[0, BLOCKS // 4])
     value_copy.start()
 
-    def chunk(index, mask, first):
+    def chunk(index, mask, first, width=QUAD):
         at = pl.multiple_of(index * wide, wide)
         for copy in copies(index):
             copy.wait()
-        latent = latents[pl.ds(at, wide), :]
+        latent = latents[pl.ds(at, width), :]
         for head in range(HEADS):
-            scores = dot(queries[head, :, :QK_DIM], keys[head, :, pl.ds(at, wide)])
+            scores = dot(queries[head, :, :QK_DIM], keys[head, :, pl.ds(at, width)])
             weights = jnp.exp2(scores)
             if mask is not None:
                 weights = jnp.where(mask, weights, 0.0)
             part = weights[:, :LANES]
-            for lanes in range(LANES, wide, LANES):
+            for lanes in range(LANES, width, LANES):
                 part = part + weights[:, lanes : lanes + LANES]
             numer = dot(weights.astype(BF16), latent)
             if first:
@@ -265,11 +304,20 @@
                 totals[head] += part
                 sums[head] += numer
 
-    row = lax.broadcasted_iota(jnp.int32, (QROWS, wide), 0)
-    col = lax.broadcasted_iota(jnp.int32, (QROWS, wide), 1)
-    query_pos = z * BLOCK + (row // ROWS) * (2 * ROWS) + p * ROWS + row % ROWS
-    key_pos = (4 * pair + col // (2 * ROWS)) * BLOCK + x * (2 * ROWS) + col % (2 * ROWS)
-    chunk(pair, key_pos <= query_pos, True)
+    def last(width):
+        row = lax.broadcasted_iota(jnp.int32, (QROWS, width), 0)
+        col = lax.broadcasted_iota(jnp.int32, (QROWS, width), 1)
+        query_pos = z * BLOCK + (row // ROWS) * (2 * ROWS) + p * ROWS + row % ROWS
+        key_pos = (4 * pair + col // (2 * ROWS)) * BLOCK + x * (2 * ROWS) + col % (2 * ROWS)
+        chunk(pair, key_pos <= query_pos, True, width)
+
+    @pl.when(z % 4 < 2)
+    def _():
+        last(QUAD // 2)
+
+    @pl.when(z % 4 >= 2)
+    def _():
+        last(QUAD)
 
     def body(index, carry):
         chunk(pair - 1 - index, None, False)
@@ -277,6 +325,7 @@
 
     lax.fori_loop(0, pair, body, 0)
     value_copy.wait()
+    sends = []
     ones = jnp.ones((HALO, LANES), F32)
     line = lax.broadcasted_iota(jnp.int32, (HALO, QROWS), 0)
     for chip in range(CHIPS):
@@ -291,6 +340,10 @@
             tail = jnp.where(line == 2 * slot, high, tail)
             tail = jnp.where(line == 2 * slot + 1, denom - high, tail)
         out[chip, QROWS:, :] = tail.astype(BF16)
+        sends.append(pltpu.make_async_copy(out.at[chip], out_far.at[chip], arrived.at[2, chip]))
+        sends[-1].start()
+    for send in sends:
+        send.wait()
 
 
 def pool_kernel(pool_rows, halo, maps, scale, keep_out, give_out):
@@ -413,13 +466,18 @@
     def up_to(step):
         return jnp.minimum(step, lax.axis_index("sp") // 4)
 
-    normed, latent_rows = whole(
+    normed, latent_rows, gain_row = whole(
         norm_kernel,
-        (far((2 * CHIPS, ROWS, D), BF16), far((PACK, KV_LATENT), BF16)),
+        (
+            far((2 * CHIPS, ROWS, D), BF16),
+            far((PACK, KV_LATENT), BF16),
+            shape((8, LANES), F32),
+        ),
         tokens,
         input_gain[None],
         latent_down,
         rotary_down.T,
+        query_gain[None],
         room=56,
     )
     rows = among_all(normed)
@@ -430,15 +488,20 @@
         project_kernel,
         (
             far((2 * CHIPS, QROWS, LANES), BF16),
-            shape((BLOCK, LANES), BF16),
-            shape((HALO, LANES), BF16),
+            far((BLOCK, LANES), BF16),
+            far((HALO, LANES), BF16),
         ),
         rows,
         query_weight.T,
         pool_down,
-        query_gain[None],
+        gain_row,
         inside,
         starts,
+        specs=[AWAY] + [VECTOR] * 5,
+        scratch=(
+            pltpu.VMEM((2 * CHIPS, ROWS, D), BF16),
+            pltpu.SemaphoreType.DMA((2,)),
+        ),
         room=ROOM_PROJECT,
     )
     queries = among_all(queries)
@@ -462,7 +525,7 @@
             pl.BlockSpec((QUAD, KV_LATENT), lambda i: (up_to(i), 0)),
         ],
         scratch_shapes=[pltpu.VMEM((HEADS * NOPE_DIM, KV_LATENT), BF16)],
-        compiler_params=pltpu.CompilerParams(vmem_limit_bytes=56 * MIB),
+        compiler_params=pltpu.CompilerParams(vmem_limit_bytes=52 * MIB),
         name="expand",
     )
     keys, latents = expand(own_latents, other_latents, key_up, key_gain[None], turned, begins)
@@ -475,15 +538,17 @@
         latents,
         value_up,
         specs=[VECTOR, AWAY, AWAY, AWAY],
+        outs=AWAY,
         scratch=(
+            pltpu.VMEM((CHIPS, QROWS + HALO, 2 * LANES), BF16),
             pltpu.VMEM((HEADS, QK_DIM, KEYS), BF16),
             pltpu.VMEM((KEYS, KV_LATENT), BF16),
             pltpu.VMEM((KV_LATENT, HEADS * VALUE_DIM), BF16),
             pltpu.VMEM((HEADS, QROWS, KV_LATENT), F32),
             pltpu.VMEM((HEADS, QROWS, LANES), F32),
-            pltpu.SemaphoreType.DMA((2, BLOCKS // 4 + 1)),
+            pltpu.SemaphoreType.DMA((3, BLOCKS // 4 + 1)),
         ),
-        room=56,
+        room=58,
     )
     parts = among_chips(numer)
 

time: 128 us -> 122 us (0.953)
  blocking collectives: 51.7 us -> 49.3 us
  Pallas kernels: 29.1 us -> 27 us
    all_gather x1, blocking collectives: 33.9 us -> 31.6 us  [local(): own_latents = lax.all_gather(latent_rows, 'sp', axis=0, tiled=False)]
    pallas_call x1, Pallas kernels: 6.78 us -> 5.23 us  [local(): expand(own_latents, other_latents, key_up, key_gain[None], turned, begins)]
    unnamed x38 -> x36, local copies, waits for them, and re-layouts: 6.17 us -> 5.02 us
where the time goes in v4:
time: 122 us
  blocking collectives  49.3 us (40%)
  Pallas kernels  27 us (22%)
  starting transfers between devices  25.2 us (21%)
  waiting for transfers between devices  14.8 us (12%)
  local copies, waits for them, and re-layouts  5.02 us (4%)
    all_gather x1, blocking collectives, local(): own_latents = lax.all_gather(latent_rows, 'sp', axis=0, tiled=False)  31.6 us
    pallas_call x8, Pallas kernels, whole(): pl.pallas_call(kernel, grid=() if specs is None else (1,), out_shape=out_...  21.7 us
    all_to_all x1, blocking collectives, among_chips(): lax.all_to_all(array, 'tp', 0, 0, axis_index_groups=SAME_CORE, tiled=True)  17.7 us
    all_to_all x2, starting transfers between devices, among_all(): return lax.all_to_all(array, 'tp', 0, 0, tiled=True)  8.85 us
    all_to_all x2, starting transfers between devices, among_chips(): lax.all_to_all(array, 'tp', 0, 0, axis_index_groups=SAME_CORE, tiled=True)  8.23 us
    ppermute x3, starting transfers between devices, to_partner(): return lax.ppermute(array, 'tp', [(i, i ^ 1) for i in range(2 * CHIPS)])  6.16 us
    all_to_all x2, waiting for transfers between devices, among_chips(): lax.all_to_all(array, 'tp', 0, 0, axis_index_groups=SAME_CORE, tiled=True)  5.45 us
    pallas_call x1, Pallas kernels, local(): expand(own_latents, other_latents, key_up, key_gain[None], turned, begins)  5.23 us
  transfers between devices with their start and end apart: 8, of which 4 were waited for; matrix products, arithmetic and copies ran while one was open for 0% of the time, Pallas kernels for 17%

profile of v4, /device:TPU:408, one launch (start us, length us, event | category | flops | bytes accessed | tf_op | source)
XLA Modules:
  0.0 121.5 jit_solution(154989671277590335)
XLA Ops:
  0.0 3.0 %shard_map.190 = (bf16[8,64,2048]{2,1,0:T(8,128)(2,1)}, bf16[72,256]{1,0:T(8,128)(2,1)}, f32[8,128]{1,0:T(8,128)}) custom-call(bf16[1,64,2048]{2,1,0:T(8,128)(2,1)} %tokens.1, f32[1,2048]{1,0:T(1,128)} %bitcast.19, bf16[2048,256]{1,0:T(8,128)(2,1)} %latent_down.1, bf16[32,2048]{1,0:T(8,128)(2,1)} %bitcast.18, f32[1,96]{1,0:T(1,128)} %bitcast.20), custom_call_target="tpu_custom_call" | custom-call | tf_op jit(solution)/shard_map/pallas_call | solution.py:74
  3.1 4.5 %all-to-all-start = ((bf16[8,64,2048]{2,1,0:T(8,128)(2,1)}), bf16[8,64,2048]{2,1,0:T(8,128)(2,1)}, u32[]{:S(2)}, u32[]{:S(2)}) async-start(bf16[8,64,2048]{2,1,0:T(8,128)(2,1)} %get-tuple-element.17), calls=%async_computation | async-start | bytes 4194304 | tf_op jit(solution)/shard_map/all_to_all | solution.py:59
  7.6 1.1 shard_map.195
  8.8 2.3 %collective-permute-start.3 = (bf16[272,2048]{1,0:T(8,128)(2,1)}, bf16[272,2048]{1,0:T(8,128)(2,1)S(1)}, u32[]{:S(2)}, u32[]{:S(2)}) collective-permute-start(bf16[272,2048]{1,0:T(8,128)(2,1)} %shard_map.195), channel_id=1, source_target_pairs={{0,1},{1,0},{2,3},{3,2},{4,5},{5,4},{6,7},{7,6},{8,9},{9,8},{10,11... | collective-permute-start | bytes 3342344 | tf_op jit(solution)/shard_map/ppermute | solution.py:63
  11.1 31.6 %all-gather = bf16[1152,256]{1,0:T(8,128)(2,1)S(1)} all-gather(bf16[72,256]{1,0:T(8,128)(2,1)S(1)} %copy-done.16), channel_id=2, replica_groups=mesh['sp'=16,'fs'=4,'tp'=8] {'sp'}, dimensions={0}, use_global_device_ids=true | all-gather | bytes 626688 | tf_op jit(solution)/shard_map/all_gather | solution.py:484
  42.7 1.9 %collective-permute-start = (bf16[16,72,256]{2,1,0:T(8,128)(2,1)S(1)}, bf16[16,72,256]{2,1,0:T(8,128)(2,1)S(1)}, u32[]{:S(2)}, u32[]{:S(2)}) collective-permute-start(bf16[16,72,256]{2,1,0:T(8,128)(2,1)S(1)} %bitcast.9), channel_id=1, source_target_pairs={{0,1},{1,0},{2,3},{3,2},{4,5},{5,4},{6,7},{7,6},{8,9},{9,8},{10,11... | collective-permute-start | bytes 1769480 | tf_op jit(solution)/shard_map/ppermute | solution.py:63
  44.6 1.0 copy-done.2
  45.7 1.0 copy-done.3
  46.7 1.0 copy-done.4
  47.7 3.8 %shard_map.191 = (bf16[8,256,128]{2,1,0:T(8,128)(2,1)}, bf16[512,128]{1,0:T(8,128)(2,1)}, bf16[16,128]{1,0:T(8,128)(2,1)}) custom-call(bf16[8,64,2048]{2,1,0:T(8,128)(2,1)} %all-to-all-done.rows_far, bf16[96,2048]{1,0:T(8,128)(2,1)S(1)} %bitcast.11, bf16[2048,128]{1,0:T(8,128)(2,1)S(1)} %copy-done.2, f32[8,128]{1,0:T(8,128)S(1)} %copy-done.11, ...), custom_call_target="tpu_custom_call" | custom-call | tf_op jit(solution)/shard_map/pallas_call | solution.py:74
  51.5 4.4 %all-to-all-start.1 = ((bf16[8,256,128]{2,1,0:T(8,128)(2,1)}), bf16[8,256,128]{2,1,0:T(8,128)(2,1)}, u32[]{:S(2)}, u32[]{:S(2)}) async-start(bf16[8,256,128]{2,1,0:T(8,128)(2,1)} %get-tuple-element.19), calls=%async_computation.1 | async-start | bytes 1048576 | tf_op jit(solution)/shard_map/all_to_all | solution.py:59
  57.8 5.2 %expand.1 = (bf16[8,96,2048]{2,1,0:T(8,128)(2,1)}, bf16[2048,256]{1,0:T(8,128)(2,1)}) custom-call(bf16[16,72,256]{2,1,0:T(8,128)(2,1)S(1)} %bitcast.10, bf16[16,72,256]{2,1,0:T(8,128)(2,1)S(1)} %collective-permute-done.other, bf16[256,512]{1,0:T(8,128)(2,1)S(1)} %copy-done.6, f32[1,96]{1,0:T(1,128)S(1)} %bitcast.17, f32[2,4,16,128]{3,2,1,0:T(8,128)S(1)} %copy-done.9, ...), custom_call_target="tpu_custom_call" | custom-call | tf_op jit(solution)/shard_map/expand/pallas_call | solution.py:531
  63.1 3.3 %all-to-all-done.1.queries = bf16[8,256,128]{2,1,0:T(8,128)(2,1)} async-done(((bf16[8,256,128]{2,1,0:T(8,128)(2,1)}), bf16[8,256,128]{2,1,0:T(8,128)(2,1)}, u32[]{:S(2)}, u32[]{:S(2)}) %all-to-all-start.1) | async-done | bytes 524320 | tf_op jit(solution)/shard_map/all_to_all | solution.py:59
  66.3 9.5 %shard_map.192 = bf16[4,272,256]{2,1,0:T(8,128)(2,1)} custom-call(bf16[8,256,128]{2,1,0:T(8,128)(2,1)} %all-to-all-done.1.queries, bf16[8,96,2048]{2,1,0:T(8,128)(2,1)} %get-tuple-element.21.keys_far, bf16[2048,256]{1,0:T(8,128)(2,1)} %get-tuple-element.22.latents_far, bf16[256,1024]{1,0:T(8,128)(2,1)} %value_far.1), custom_call_target="tpu_custom_call" | custom-call | tf_op jit(solution)/shard_map/pallas_call | solution.py:74
  75.9 3.5 %all-to-all-start.2 = ((bf16[4,272,256]{2,1,0:T(8,128)(2,1)}), bf16[4,272,256]{2,1,0:T(8,128)(2,1)S(1)}, u32[]{:S(2)}, u32[]{:S(2)}) async-start(bf16[4,272,256]{2,1,0:T(8,128)(2,1)} %shard_map.192), calls=%async_computation.2 | async-start | bytes 1114112 | tf_op jit(solution)/shard_map/all_to_all | solution.py:55
  79.4 1.9 %collective-permute-start.1 = (bf16[16,128]{1,0:T(8,128)(2,1)S(1)}, bf16[16,128]{1,0:T(8,128)(2,1)S(1)}, u32[]{:S(2)}, u32[]{:S(2)}) collective-permute-start(bf16[16,128]{1,0:T(8,128)(2,1)S(1)} %copy-done.17), channel_id=1, source_target_pairs={{0,32},{32,64},{64,96},{96,128},{128,160},{160,192},{192,224},{224... | collective-permute-start | bytes 12296 | tf_op jit(solution)/shard_map/ppermute | solution.py:508
  81.3 4.8 %collective-permute-done.1.halo = bf16[16,128]{1,0:T(8,128)(2,1)S(1)} collective-permute-done((bf16[16,128]{1,0:T(8,128)(2,1)S(1)}, bf16[16,128]{1,0:T(8,128)(2,1)S(1)}, u32[]{:S(2)}, u32[]{:S(2)}) %collective-permute-start.1) | collective-permute-done | bytes 4128 | tf_op jit(solution)/shard_map/ppermute | solution.py:508
  86.4 1.9 %collective-permute-start.2 = (f32[256,128]{1,0:T(8,128)S(1)}, f32[256,128]{1,0:T(8,128)S(1)}, u32[]{:S(2)}, u32[]{:S(2)}) collective-permute-start(f32[256,128]{1,0:T(8,128)S(1)} %get-tuple-element.26), channel_id=1, source_target_pairs={{0,1},{1,0},{2,3},{3,2},{4,5},{5,4},{6,7},{7,6},{8,9},{9,8},{10,11... | collective-permute-start | bytes 393224 | tf_op jit(solution)/shard_map/ppermute | solution.py:63
  88.3 1.3 %collective-permute-done.2.pool_other = f32[256,128]{1,0:T(8,128)S(1)} collective-permute-done((f32[256,128]{1,0:T(8,128)S(1)}, f32[256,128]{1,0:T(8,128)S(1)}, u32[]{:S(2)}, u32[]{:S(2)}) %collective-permute-start.2) | collective-permute-done | bytes 131104 | tf_op jit(solution)/shard_map/ppermute | solution.py:63
  89.7 1.2 %shard_map.194 = (f32[2,256,128]{2,1,0:T(8,128)S(1)}, f32[4,8,256]{2,1,0:T(8,128)}) custom-call(bf16[4,272,256]{2,1,0:T(8,128)(2,1)S(1)} %all-to-all-done.2.parts, f32[256,128]{1,0:T(8,128)S(1)} %get-tuple-element.25.pool_own, f32[256,128]{1,0:T(8,128)S(1)} %collective-permute-done.2.pool_other), custom_call_target="tpu_custom_call" | custom-call | tf_op jit(solution)/shard_map/pallas_call | solution.py:74
  90.9 4.7 %all-to-all-start.3 = ((f32[4,8,256]{2,1,0:T(8,128)}), f32[4,8,256]{2,1,0:T(8,128)S(1)}, u32[]{:S(2)}, u32[]{:S(2)}) async-start(f32[4,8,256]{2,1,0:T(8,128)} %get-tuple-element.28), calls=%async_computation.3 | async-start | bytes 65536 | tf_op jit(solution)/shard_map/all_to_all | solution.py:55
  95.6 5.4 %all-to-all-done.3.squares = f32[4,8,256]{2,1,0:T(8,128)S(1)} async-done(((f32[4,8,256]{2,1,0:T(8,128)}), f32[4,8,256]{2,1,0:T(8,128)S(1)}, u32[]{:S(2)}, u32[]{:S(2)}) %all-to-all-start.3) | async-done | bytes 32800 | tf_op jit(solution)/shard_map/all_to_all | solution.py:55
  101.1 1.9 %shard_map.196 = bf16[4,64,2048]{2,1,0:T(8,128)(2,1)} custom-call(f32[2,256,128]{2,1,0:T(8,128)S(1)} %get-tuple-element.27.attended, f32[256,128]{1,0:T(8,128)S(1)} %get-tuple-element.25.pool_own, f32[256,128]{1,0:T(8,128)S(1)} %collective-permute-done.2.pool_other, f32[4,8,256]{2,1,0:T(8,128)S(1)} %all-to-all-done.3.squares, f32[1,128]{1,0:T(1,128)S(1)} %bitcast.13, ...), custom_call_target="tpu_custom_call" | custom-call | tf_op jit(solution)/shard_map/pallas_call | solution.py:74
  103.0 17.7 %all_to_all.25.parts = bf16[4,64,2048]{2,1,0:T(8,128)(2,1)S(1)} all-to-all(bf16[4,64,2048]{2,1,0:T(8,128)(2,1)} %shard_map.196), channel_id=1, replica_groups={{0,2,4,6},{1,3,5,7},{8,10,12,14},{9,11,13,15},{16,18,20,22},{17,19,21,2..., dimensions={0} | all-to-all | bytes 2097152 | tf_op jit(solution)/shard_map/all_to_all | solution.py:55
  (39 shorter events, 3.1 us)
Async XLA Ops:
  3.0 4.6 %copy-start = (bf16[128,2048]{1,0:T(8,128)(2,1)S(1)}, bf16[128,2048]{1,0:T(8,128)(2,1)}, u32[]{:S(2)}) copy-start(bf16[128,2048]{1,0:T(8,128)(2,1)} %own_attention.1) | copy-start | bytes 1572868
  3.0 4.6 %copy-start.1 = (bf16[128,2048]{1,0:T(8,128)(2,1)S(1)}, bf16[128,2048]{1,0:T(8,128)(2,1)}, u32[]{:S(2)}) copy-start(bf16[128,2048]{1,0:T(8,128)(2,1)} %own_pool.1) | copy-start | bytes 1572868
  3.0 4.6 %copy-start.12 = (f32[128]{0:T(128)S(1)}, f32[128]{0:T(128)}, u32[]{:S(2)}) copy-start(f32[128]{0:T(128)} %param.32) | copy-start | bytes 1540
  3.1 4.6 %copy-start.13 = (f32[128]{0:T(128)S(1)}, f32[128]{0:T(128)}, u32[]{:S(2)}) copy-start(f32[128]{0:T(128)} %param.33) | copy-start | bytes 1540
  3.1 41.5 %all-to-all-start = ((bf16[8,64,2048]{2,1,0:T(8,128)(2,1)}), bf16[8,64,2048]{2,1,0:T(8,128)(2,1)}, u32[]{:S(2)}, u32[]{:S(2)}) async-start(bf16[8,64,2048]{2,1,0:T(8,128)(2,1)} %get-tuple-element.17), calls=%async_computation | async-start | bytes 4194304 | tf_op jit(solution)/shard_map/all_to_all | solution.py:59
  7.6 3.5 %copy-start.16 = (bf16[72,256]{1,0:T(8,128)(2,1)S(1)}, bf16[72,256]{1,0:T(8,128)(2,1)}, u32[]{:S(2)}) copy-start(bf16[72,256]{1,0:T(8,128)(2,1)} %get-tuple-element.20) | copy-start | bytes 110596
  7.6 37.1 %copy-start.10 = (f32[2,16,128]{2,1,0:T(8,128)S(1)}, f32[2,16,128]{2,1,0:T(8,128)}, u32[]{:S(2)}) copy-start(f32[2,16,128]{2,1,0:T(8,128)} %constant.9.clone.starts) | copy-start | bytes 49156
  7.6 37.1 %copy-start.11 = (f32[8,128]{1,0:T(8,128)S(1)}, f32[8,128]{1,0:T(8,128)}, u32[]{:S(2)}) copy-start(f32[8,128]{1,0:T(8,128)} %get-tuple-element.18.gain) | copy-start | bytes 12292
  8.8 86.9 %collective-permute-start.3 = (bf16[272,2048]{1,0:T(8,128)(2,1)}, bf16[272,2048]{1,0:T(8,128)(2,1)S(1)}, u32[]{:S(2)}, u32[]{:S(2)}) collective-permute-start(bf16[272,2048]{1,0:T(8,128)(2,1)} %shard_map.195), channel_id=1, source_target_pairs={{0,1},{1,0},{2,3},{3,2},{4,5},{5,4},{6,7},{7,6},{8,9},{9,8},{10,11... | collective-permute-start | bytes 3342344 | tf_op jit(solution)/shard_map/ppermute | solution.py:63
  42.7 13.2 %collective-permute-start = (bf16[16,72,256]{2,1,0:T(8,128)(2,1)S(1)}, bf16[16,72,256]{2,1,0:T(8,128)(2,1)S(1)}, u32[]{:S(2)}, u32[]{:S(2)}) collective-permute-start(bf16[16,72,256]{2,1,0:T(8,128)(2,1)S(1)} %bitcast.9), channel_id=1, source_target_pairs={{0,1},{1,0},{2,3},{3,2},{4,5},{5,4},{6,7},{7,6},{8,9},{9,8},{10,11... | collective-permute-start | bytes 1769480 | tf_op jit(solution)/shard_map/ppermute | solution.py:63
  44.6 1.0 copy-start.2
  45.7 1.0 copy-start.3
  46.7 1.0 copy-start.4
  47.7 8.2 %copy-start.9 = (f32[2,4,16,128]{3,2,1,0:T(8,128)S(1)}, f32[2,4,16,128]{3,2,1,0:T(8,128)}, u32[]{:S(2)}) copy-start(f32[2,4,16,128]{3,2,1,0:T(8,128)} %constant.10.clone.inside) | copy-start | bytes 196612
  47.7 8.2 %copy-start.15 = (f32[96]{0:T(128)S(1)}, f32[96]{0:T(128)}, u32[]{:S(2)}) copy-start(f32[96]{0:T(128)} %param.29) | copy-start | bytes 1156
  51.5 14.8 %all-to-all-start.1 = ((bf16[8,256,128]{2,1,0:T(8,128)(2,1)}), bf16[8,256,128]{2,1,0:T(8,128)(2,1)}, u32[]{:S(2)}, u32[]{:S(2)}) async-start(bf16[8,256,128]{2,1,0:T(8,128)(2,1)} %get-tuple-element.19), calls=%async_computation.1 | async-start | bytes 1048576 | tf_op jit(solution)/shard_map/all_to_all | solution.py:59
  66.3 13.0 %copy-start.17 = (bf16[16,128]{1,0:T(8,128)(2,1)S(1)}, bf16[16,128]{1,0:T(8,128)(2,1)}, u32[]{:S(2)}) copy-start(bf16[16,128]{1,0:T(8,128)(2,1)} %get-tuple-element.24) | copy-start | bytes 12292
  66.3 19.7 %copy-start.5 = (bf16[16,64,64]{2,1,0:T(8,128)(2,1)S(1)}, bf16[16,64,64]{2,1,0:T(8,128)(2,1)}, u32[]{:S(2)}) copy-start(bf16[16,64,64]{2,1,0:T(8,128)(2,1)} %maps.1) | copy-start | bytes 393220
  66.3 19.7 %copy-start.8 = (bf16[512,128]{1,0:T(8,128)(2,1)S(1)}, bf16[512,128]{1,0:T(8,128)(2,1)}, u32[]{:S(2)}) copy-start(bf16[512,128]{1,0:T(8,128)(2,1)} %get-tuple-element.23.pool_rows) | copy-start | bytes 393220
  66.3 19.7 %copy-start.14 = (f32[128]{0:T(128)S(1)}, f32[128]{0:T(128)}, u32[]{:S(2)}) copy-start(f32[128]{0:T(128)} %param.31) | copy-start | bytes 1540
  75.9 13.8 %all-to-all-start.2 = ((bf16[4,272,256]{2,1,0:T(8,128)(2,1)}), bf16[4,272,256]{2,1,0:T(8,128)(2,1)S(1)}, u32[]{:S(2)}, u32[]{:S(2)}) async-start(bf16[4,272,256]{2,1,0:T(8,128)(2,1)} %shard_map.192), calls=%async_computation.2 | async-start | bytes 1114112 | tf_op jit(solution)/shard_map/all_to_all | solution.py:55
  79.4 6.7 %collective-permute-start.1 = (bf16[16,128]{1,0:T(8,128)(2,1)S(1)}, bf16[16,128]{1,0:T(8,128)(2,1)S(1)}, u32[]{:S(2)}, u32[]{:S(2)}) collective-permute-start(bf16[16,128]{1,0:T(8,128)(2,1)S(1)} %copy-done.17), channel_id=1, source_target_pairs={{0,32},{32,64},{64,96},{96,128},{128,160},{160,192},{192,224},{224... | collective-permute-start | bytes 12296 | tf_op jit(solution)/shard_map/ppermute | solution.py:508
  86.4 3.2 %collective-permute-start.2 = (f32[256,128]{1,0:T(8,128)S(1)}, f32[256,128]{1,0:T(8,128)S(1)}, u32[]{:S(2)}, u32[]{:S(2)}) collective-permute-start(f32[256,128]{1,0:T(8,128)S(1)} %get-tuple-element.26), channel_id=1, source_target_pairs={{0,1},{1,0},{2,3},{3,2},{4,5},{5,4},{6,7},{7,6},{8,9},{9,8},{10,11... | collective-permute-start | bytes 393224 | tf_op jit(solution)/shard_map/ppermute | solution.py:63
  90.9 10.2 %all-to-all-start.3 = ((f32[4,8,256]{2,1,0:T(8,128)}), f32[4,8,256]{2,1,0:T(8,128)S(1)}, u32[]{:S(2)}, u32[]{:S(2)}) async-start(f32[4,8,256]{2,1,0:T(8,128)} %get-tuple-element.28), calls=%async_computation.3 | async-start | bytes 65536 | tf_op jit(solution)/shard_map/all_to_all | solution.py:55
  (2 other events, 1.9 us)

commit v5 on v4

--- a/solution.py
+++ b/solution.py
@@ -95,10 +95,14 @@
     return pltpu.HBM(dims, dtype)
 
 
-def dot(a, b, dims=((1,), (0,)), precision=None):
-    return lax.dot_general(
-        a, b, (dims, ((), ())), preferred_element_type=F32, precision=precision
-    )
+def dot(a, b, dims=((1,), (0,))):
+    return lax.dot_general(a, b, (dims, ((), ())), preferred_element_type=F32)
+
+
+def lane_totals(ones, values):
+    high = values.astype(BF16)
+    low = (values - high.astype(F32)).astype(BF16)
+    return dot(ones, high, ((1,), (1,))) + dot(ones, low, ((1,), (1,)))
 
 
 def turn(vectors, cosine, sine):
@@ -326,7 +330,7 @@
     lax.fori_loop(0, pair, body, 0)
     value_copy.wait()
     sends = []
-    ones = jnp.ones((HALO, LANES), F32)
+    ones = jnp.ones((HALO, LANES), BF16)
     line = lax.broadcasted_iota(jnp.int32, (HALO, QROWS), 0)
     for chip in range(CHIPS):
         tail = jnp.zeros((HALO, QROWS), F32)
@@ -335,7 +339,7 @@
             values = value_up[:, head * VALUE_DIM : (head + 1) * VALUE_DIM]
             numer = dot(sums[head].astype(BF16), values)
             out[chip, :QROWS, slot * LANES : (slot + 1) * LANES] = numer.astype(BF16)
-            denom = dot(ones, totals[head], ((1,), (1,)), lax.Precision.HIGHEST)
+            denom = lane_totals(ones, totals[head])
             high = denom.astype(BF16).astype(F32)
             tail = jnp.where(line == 2 * slot, high, tail)
             tail = jnp.where(line == 2 * slot + 1, denom - high, tail)
@@ -388,12 +392,11 @@
         attended = numer / denom
         attended_out[slot] = attended
         squares = squares + attended * attended
-    ones = jnp.ones((8, LANES), F32)
-    exact = lax.Precision.HIGHEST
+    ones = jnp.ones((HALO, LANES), BF16)
     line = lax.broadcasted_iota(jnp.int32, (8, QROWS), 0)
-    mine = dot(ones, squares, ((1,), (1,)), exact)
+    mine = lane_totals(ones, squares)[:8]
     pooled = pool_own[...] * pool_own[...] + pool_other[...] * pool_other[...]
-    pools = dot(ones, pooled, ((1,), (1,)), exact)
+    pools = lane_totals(ones, pooled)[:8]
     for chip in range(CHIPS):
         squares_out[chip] = jnp.where(line < 4, mine, pools)
 
@@ -548,7 +551,7 @@
             pltpu.VMEM((HEADS, QROWS, LANES), F32),
             pltpu.SemaphoreType.DMA((3, BLOCKS // 4 + 1)),
         ),
-        room=58,
+        room=53,
     )
     parts = among_chips(numer)
 

time: 122 us -> 121 us (level)
  the two profiles are of different devices: /device:TPU:408 before, /device:TPU:384 now
where the time goes in v5:
time: 121 us; the launch traced here: 120 us
  blocking collectives  49.3 us (41%)
  Pallas kernels  26.1 us (22%)
  starting transfers between devices  25.2 us (21%)
  waiting for transfers between devices  13.2 us (11%)
  local copies, waits for them, and re-layouts  6.12 us (5%)
    all_gather x1, blocking collectives, local(): own_latents = lax.all_gather(latent_rows, 'sp', axis=0, tiled=False)  31.6 us
    pallas_call x8, Pallas kernels, whole(): pl.pallas_call(kernel, grid=() if specs is None else (1,), out_shape=out_...  19.9 us
    all_to_all x1, blocking collectives, among_chips(): lax.all_to_all(array, 'tp', 0, 0, axis_index_groups=SAME_CORE, tiled=True)  17.7 us
    all_to_all x2, starting transfers between devices, among_all(): return lax.all_to_all(array, 'tp', 0, 0, tiled=True)  8.86 us
    all_to_all x2, starting transfers between devices, among_chips(): lax.all_to_all(array, 'tp', 0, 0, axis_index_groups=SAME_CORE, tiled=True)  8.23 us
    pallas_call x1, Pallas kernels, local(): expand(own_latents, other_latents, key_up, key_gain[None], turned, begins)  6.19 us
    ppermute x3, starting transfers between devices, to_partner(): return lax.ppermute(array, 'tp', [(i, i ^ 1) for i in range(2 * CHIPS)])  6.16 us
    unnamed x40, local copies, waits for them, and re-layouts  6.12 us
  transfers between devices with their start and end apart: 8, of which 4 were waited for; matrix products, arithmetic and copies ran while one was open for 0% of the time, Pallas kernels for 17%

profile of v5, /device:TPU:384, one launch (start us, length us, event | category | flops | bytes accessed | tf_op | source)
XLA Modules:
  0.0 120.1 jit_solution(15985721725943808786)
XLA Ops:
  0.0 3.0 %shard_map.190 = (bf16[8,64,2048]{2,1,0:T(8,128)(2,1)}, bf16[72,256]{1,0:T(8,128)(2,1)}, f32[8,128]{1,0:T(8,128)}) custom-call(bf16[1,64,2048]{2,1,0:T(8,128)(2,1)} %tokens.1, f32[1,2048]{1,0:T(1,128)} %bitcast.19, bf16[2048,256]{1,0:T(8,128)(2,1)} %latent_down.1, bf16[32,2048]{1,0:T(8,128)(2,1)} %bitcast.18, f32[1,96]{1,0:T(1,128)} %bitcast.20), custom_call_target="tpu_custom_call" | custom-call | tf_op jit(solution)/shard_map/pallas_call | solution.py:74
  3.1 4.5 %all-to-all-start = ((bf16[8,64,2048]{2,1,0:T(8,128)(2,1)}), bf16[8,64,2048]{2,1,0:T(8,128)(2,1)}, u32[]{:S(2)}, u32[]{:S(2)}) async-start(bf16[8,64,2048]{2,1,0:T(8,128)(2,1)} %get-tuple-element.17), calls=%async_computation | async-start | bytes 4194304 | tf_op jit(solution)/shard_map/all_to_all | solution.py:59
  7.6 1.1 shard_map.195
  8.7 2.3 %collective-permute-start.3 = (bf16[272,2048]{1,0:T(8,128)(2,1)}, bf16[272,2048]{1,0:T(8,128)(2,1)S(1)}, u32[]{:S(2)}, u32[]{:S(2)}) collective-permute-start(bf16[272,2048]{1,0:T(8,128)(2,1)} %shard_map.195), channel_id=1, source_target_pairs={{0,1},{1,0},{2,3},{3,2},{4,5},{5,4},{6,7},{7,6},{8,9},{9,8},{10,11... | collective-permute-start | bytes 3342344 | tf_op jit(solution)/shard_map/ppermute | solution.py:63
  11.1 31.6 %all-gather = bf16[1152,256]{1,0:T(8,128)(2,1)S(1)} all-gather(bf16[72,256]{1,0:T(8,128)(2,1)S(1)} %copy-done.18), channel_id=2, replica_groups=mesh['sp'=16,'fs'=4,'tp'=8] {'sp'}, dimensions={0}, use_global_device_ids=true | all-gather | bytes 626688 | tf_op jit(solution)/shard_map/all_gather | solution.py:487
  42.7 1.9 %collective-permute-start = (bf16[16,72,256]{2,1,0:T(8,128)(2,1)S(1)}, bf16[16,72,256]{2,1,0:T(8,128)(2,1)}, u32[]{:S(2)}, u32[]{:S(2)}) collective-permute-start(bf16[16,72,256]{2,1,0:T(8,128)(2,1)S(1)} %bitcast.9), channel_id=1, source_target_pairs={{0,1},{1,0},{2,3},{3,2},{4,5},{5,4},{6,7},{7,6},{8,9},{9,8},{10,11... | collective-permute-start | bytes 1769480 | tf_op jit(solution)/shard_map/ppermute | solution.py:63
  44.6 1.0 copy-done.3
  45.7 1.0 copy-done.4
  47.3 3.8 %shard_map.191 = (bf16[8,256,128]{2,1,0:T(8,128)(2,1)}, bf16[512,128]{1,0:T(8,128)(2,1)}, bf16[16,128]{1,0:T(8,128)(2,1)}) custom-call(bf16[8,64,2048]{2,1,0:T(8,128)(2,1)} %all-to-all-done.rows_far, bf16[96,2048]{1,0:T(8,128)(2,1)S(1)} %bitcast.11, bf16[2048,128]{1,0:T(8,128)(2,1)S(1)} %copy-done.2, f32[8,128]{1,0:T(8,128)S(1)} %copy-done.11, ...), custom_call_target="tpu_custom_call" | custom-call | tf_op jit(solution)/shard_map/pallas_call | solution.py:74
  51.2 4.4 %all-to-all-start.1 = ((bf16[8,256,128]{2,1,0:T(8,128)(2,1)}), bf16[8,256,128]{2,1,0:T(8,128)(2,1)S(1)}, u32[]{:S(2)}, u32[]{:S(2)}) async-start(bf16[8,256,128]{2,1,0:T(8,128)(2,1)} %get-tuple-element.19), calls=%async_computation.1 | async-start | bytes 1048576 | tf_op jit(solution)/shard_map/all_to_all | solution.py:59
  55.6 0.9 copy-done.7
  58.0 6.2 %expand.1 = (bf16[8,96,2048]{2,1,0:T(8,128)(2,1)}, bf16[2048,256]{1,0:T(8,128)(2,1)}) custom-call(bf16[16,72,256]{2,1,0:T(8,128)(2,1)S(1)} %bitcast.10, bf16[16,72,256]{2,1,0:T(8,128)(2,1)} %collective-permute-done.other, bf16[256,512]{1,0:T(8,128)(2,1)S(1)} %copy-done.6, f32[1,96]{1,0:T(1,128)S(1)} %bitcast.17, f32[2,4,16,128]{3,2,1,0:T(8,128)S(1)} %copy-done.9, ...), custom_call_target="tpu_custom_call" | custom-call | tf_op jit(solution)/shard_map/expand/pallas_call | solution.py:534
  64.2 1.7 %all-to-all-done.1.queries = bf16[8,256,128]{2,1,0:T(8,128)(2,1)S(1)} async-done(((bf16[8,256,128]{2,1,0:T(8,128)(2,1)}), bf16[8,256,128]{2,1,0:T(8,128)(2,1)S(1)}, u32[]{:S(2)}, u32[]{:S(2)}) %all-to-all-start.1) | async-done | bytes 524320 | tf_op jit(solution)/shard_map/all_to_all | solution.py:59
  65.9 7.8 %shard_map.192 = bf16[4,272,256]{2,1,0:T(8,128)(2,1)} custom-call(bf16[8,256,128]{2,1,0:T(8,128)(2,1)S(1)} %all-to-all-done.1.queries, bf16[8,96,2048]{2,1,0:T(8,128)(2,1)} %get-tuple-element.21.keys_far, bf16[2048,256]{1,0:T(8,128)(2,1)} %get-tuple-element.22.latents_far, bf16[256,1024]{1,0:T(8,128)(2,1)} %value_far.1), custom_call_target="tpu_custom_call" | custom-call | tf_op jit(solution)/shard_map/pallas_call | solution.py:74
  73.7 3.5 %all-to-all-start.2 = ((bf16[4,272,256]{2,1,0:T(8,128)(2,1)}), bf16[4,272,256]{2,1,0:T(8,128)(2,1)S(1)}, u32[]{:S(2)}, u32[]{:S(2)}) async-start(bf16[4,272,256]{2,1,0:T(8,128)(2,1)} %shard_map.192), calls=%async_computation.2 | async-start | bytes 1114112 | tf_op jit(solution)/shard_map/all_to_all | solution.py:55
  77.2 1.9 %collective-permute-start.1 = (bf16[16,128]{1,0:T(8,128)(2,1)S(1)}, bf16[16,128]{1,0:T(8,128)(2,1)S(1)}, u32[]{:S(2)}, u32[]{:S(2)}) collective-permute-start(bf16[16,128]{1,0:T(8,128)(2,1)S(1)} %copy-done.19), channel_id=1, source_target_pairs={{0,32},{32,64},{64,96},{96,128},{128,160},{160,192},{192,224},{224... | collective-permute-start | bytes 12296 | tf_op jit(solution)/shard_map/ppermute | solution.py:511
  79.2 4.8 %collective-permute-done.1.halo = bf16[16,128]{1,0:T(8,128)(2,1)S(1)} collective-permute-done((bf16[16,128]{1,0:T(8,128)(2,1)S(1)}, bf16[16,128]{1,0:T(8,128)(2,1)S(1)}, u32[]{:S(2)}, u32[]{:S(2)}) %collective-permute-start.1) | collective-permute-done | bytes 4128 | tf_op jit(solution)/shard_map/ppermute | solution.py:511
  85.2 1.9 %collective-permute-start.2 = (f32[256,128]{1,0:T(8,128)S(1)}, f32[256,128]{1,0:T(8,128)S(1)}, u32[]{:S(2)}, u32[]{:S(2)}) collective-permute-start(f32[256,128]{1,0:T(8,128)S(1)} %get-tuple-element.26), channel_id=1, source_target_pairs={{0,1},{1,0},{2,3},{3,2},{4,5},{5,4},{6,7},{7,6},{8,9},{9,8},{10,11... | collective-permute-start | bytes 393224 | tf_op jit(solution)/shard_map/ppermute | solution.py:63
  87.1 1.3 %collective-permute-done.2.pool_other = f32[256,128]{1,0:T(8,128)S(1)} collective-permute-done((f32[256,128]{1,0:T(8,128)S(1)}, f32[256,128]{1,0:T(8,128)S(1)}, u32[]{:S(2)}, u32[]{:S(2)}) %collective-permute-start.2) | collective-permute-done | bytes 131104 | tf_op jit(solution)/shard_map/ppermute | solution.py:63
  88.5 1.1 shard_map.194
  89.5 4.7 %all-to-all-start.3 = ((f32[4,8,256]{2,1,0:T(8,128)}), f32[4,8,256]{2,1,0:T(8,128)S(1)}, u32[]{:S(2)}, u32[]{:S(2)}) async-start(f32[4,8,256]{2,1,0:T(8,128)} %get-tuple-element.28), calls=%async_computation.3 | async-start | bytes 65536 | tf_op jit(solution)/shard_map/all_to_all | solution.py:55
  94.3 5.4 %all-to-all-done.3.squares = f32[4,8,256]{2,1,0:T(8,128)S(1)} async-done(((f32[4,8,256]{2,1,0:T(8,128)}), f32[4,8,256]{2,1,0:T(8,128)S(1)}, u32[]{:S(2)}, u32[]{:S(2)}) %all-to-all-start.3) | async-done | bytes 32800 | tf_op jit(solution)/shard_map/all_to_all | solution.py:55
  99.7 1.8 %shard_map.196 = bf16[4,64,2048]{2,1,0:T(8,128)(2,1)} custom-call(f32[2,256,128]{2,1,0:T(8,128)S(1)} %get-tuple-element.27.attended, f32[256,128]{1,0:T(8,128)S(1)} %get-tuple-element.25.pool_own, f32[256,128]{1,0:T(8,128)S(1)} %collective-permute-done.2.pool_other, f32[4,8,256]{2,1,0:T(8,128)S(1)} %all-to-all-done.3.squares, f32[1,128]{1,0:T(1,128)S(1)} %bitcast.13, ...), custom_call_target="tpu_custom_call" | custom-call | tf_op jit(solution)/shard_map/pallas_call | solution.py:74
  101.6 17.7 %all_to_all.25.parts = bf16[4,64,2048]{2,1,0:T(8,128)(2,1)S(1)} all-to-all(bf16[4,64,2048]{2,1,0:T(8,128)(2,1)} %shard_map.196), channel_id=1, replica_groups={{0,2,4,6},{1,3,5,7},{8,10,12,14},{9,11,13,15},{16,18,20,22},{17,19,21,2..., dimensions={0} | all-to-all | bytes 2097152 | tf_op jit(solution)/shard_map/all_to_all | solution.py:55
  (43 shorter events, 4.3 us)
Async XLA Ops:
  3.0 4.6 %copy-start = (bf16[128,2048]{1,0:T(8,128)(2,1)S(1)}, bf16[128,2048]{1,0:T(8,128)(2,1)}, u32[]{:S(2)}) copy-start(bf16[128,2048]{1,0:T(8,128)(2,1)} %own_attention.1) | copy-start | bytes 1572868
  3.0 4.6 %copy-start.1 = (bf16[128,2048]{1,0:T(8,128)(2,1)S(1)}, bf16[128,2048]{1,0:T(8,128)(2,1)}, u32[]{:S(2)}) copy-start(bf16[128,2048]{1,0:T(8,128)(2,1)} %own_pool.1) | copy-start | bytes 1572868
  3.0 4.6 %copy-start.12 = (f32[128]{0:T(128)S(1)}, f32[128]{0:T(128)}, u32[]{:S(2)}) copy-start(f32[128]{0:T(128)} %param.32) | copy-start | bytes 1540
  3.0 4.6 %copy-start.14 = (f32[128]{0:T(128)S(1)}, f32[128]{0:T(128)}, u32[]{:S(2)}) copy-start(f32[128]{0:T(128)} %param.33) | copy-start | bytes 1540
  3.1 41.5 %all-to-all-start = ((bf16[8,64,2048]{2,1,0:T(8,128)(2,1)}), bf16[8,64,2048]{2,1,0:T(8,128)(2,1)}, u32[]{:S(2)}, u32[]{:S(2)}) async-start(bf16[8,64,2048]{2,1,0:T(8,128)(2,1)} %get-tuple-element.17), calls=%async_computation | async-start | bytes 4194304 | tf_op jit(solution)/shard_map/all_to_all | solution.py:59
  7.5 3.5 %copy-start.18 = (bf16[72,256]{1,0:T(8,128)(2,1)S(1)}, bf16[72,256]{1,0:T(8,128)(2,1)}, u32[]{:S(2)}) copy-start(bf16[72,256]{1,0:T(8,128)(2,1)} %get-tuple-element.20) | copy-start | bytes 110596
  7.6 37.0 %copy-start.2 = (bf16[2048,128]{1,0:T(8,128)(2,1)S(1)}, bf16[2048,128]{1,0:T(8,128)(2,1)}, u32[]{:S(2)}) copy-start(bf16[2048,128]{1,0:T(8,128)(2,1)} %pool_down.1) | copy-start | bytes 1572868
  7.6 37.0 %copy-start.10 = (f32[2,16,128]{2,1,0:T(8,128)S(1)}, f32[2,16,128]{2,1,0:T(8,128)}, u32[]{:S(2)}) copy-start(f32[2,16,128]{2,1,0:T(8,128)} %constant.9.clone.starts) | copy-start | bytes 49156
  8.7 85.5 %collective-permute-start.3 = (bf16[272,2048]{1,0:T(8,128)(2,1)}, bf16[272,2048]{1,0:T(8,128)(2,1)S(1)}, u32[]{:S(2)}, u32[]{:S(2)}) collective-permute-start(bf16[272,2048]{1,0:T(8,128)(2,1)} %shard_map.195), channel_id=1, source_target_pairs={{0,1},{1,0},{2,3},{3,2},{4,5},{5,4},{6,7},{7,6},{8,9},{9,8},{10,11... | collective-permute-start | bytes 3342344 | tf_op jit(solution)/shard_map/ppermute | solution.py:63
  42.7 12.9 %collective-permute-start = (bf16[16,72,256]{2,1,0:T(8,128)(2,1)S(1)}, bf16[16,72,256]{2,1,0:T(8,128)(2,1)}, u32[]{:S(2)}, u32[]{:S(2)}) collective-permute-start(bf16[16,72,256]{2,1,0:T(8,128)(2,1)S(1)} %bitcast.9), channel_id=1, source_target_pairs={{0,1},{1,0},{2,3},{3,2},{4,5},{5,4},{6,7},{7,6},{8,9},{9,8},{10,11... | collective-permute-start | bytes 1769480 | tf_op jit(solution)/shard_map/ppermute | solution.py:63
  44.6 1.0 copy-start.3
  45.7 1.0 copy-start.4
  47.3 8.2 %copy-start.6 = (bf16[256,512]{1,0:T(8,128)(2,1)S(1)}, bf16[256,512]{1,0:T(8,128)(2,1)}, u32[]{:S(2)}) copy-start(bf16[256,512]{1,0:T(8,128)(2,1)} %key_up.1) | copy-start | bytes 786436
  51.2 14.7 %all-to-all-start.1 = ((bf16[8,256,128]{2,1,0:T(8,128)(2,1)}), bf16[8,256,128]{2,1,0:T(8,128)(2,1)S(1)}, u32[]{:S(2)}, u32[]{:S(2)}) async-start(bf16[8,256,128]{2,1,0:T(8,128)(2,1)} %get-tuple-element.19), calls=%async_computation.1 | async-start | bytes 1048576 | tf_op jit(solution)/shard_map/all_to_all | solution.py:59
  55.6 1.0 copy-start.7
  65.9 11.4 %copy-start.19 = (bf16[16,128]{1,0:T(8,128)(2,1)S(1)}, bf16[16,128]{1,0:T(8,128)(2,1)}, u32[]{:S(2)}) copy-start(bf16[16,128]{1,0:T(8,128)(2,1)} %get-tuple-element.24) | copy-start | bytes 12292
  65.9 18.1 %copy-start.5 = (bf16[16,64,64]{2,1,0:T(8,128)(2,1)S(1)}, bf16[16,64,64]{2,1,0:T(8,128)(2,1)}, u32[]{:S(2)}) copy-start(bf16[16,64,64]{2,1,0:T(8,128)(2,1)} %maps.1) | copy-start | bytes 393220
  65.9 18.1 %copy-start.16 = (f32[128]{0:T(128)S(1)}, f32[128]{0:T(128)}, u32[]{:S(2)}) copy-start(f32[128]{0:T(128)} %param.31) | copy-start | bytes 1540
  73.7 26.0 %copy-start.13 = (f32[128]{0:T(128)S(1)}, f32[128]{0:T(128)}, u32[]{:S(2)}) copy-start(f32[128]{0:T(128)} %param.32) | copy-start | bytes 1540
  73.7 26.0 %copy-start.15 = (f32[128]{0:T(128)S(1)}, f32[128]{0:T(128)}, u32[]{:S(2)}) copy-start(f32[128]{0:T(128)} %param.33) | copy-start | bytes 1540
  73.7 14.7 %all-to-all-start.2 = ((bf16[4,272,256]{2,1,0:T(8,128)(2,1)}), bf16[4,272,256]{2,1,0:T(8,128)(2,1)S(1)}, u32[]{:S(2)}, u32[]{:S(2)}) async-start(bf16[4,272,256]{2,1,0:T(8,128)(2,1)} %shard_map.192), calls=%async_computation.2 | async-start | bytes 1114112 | tf_op jit(solution)/shard_map/all_to_all | solution.py:55
  77.2 6.7 %collective-permute-start.1 = (bf16[16,128]{1,0:T(8,128)(2,1)S(1)}, bf16[16,128]{1,0:T(8,128)(2,1)S(1)}, u32[]{:S(2)}, u32[]{:S(2)}) collective-permute-start(bf16[16,128]{1,0:T(8,128)(2,1)S(1)} %copy-done.19), channel_id=1, source_target_pairs={{0,32},{32,64},{64,96},{96,128},{128,160},{160,192},{192,224},{224... | collective-permute-start | bytes 12296 | tf_op jit(solution)/shard_map/ppermute | solution.py:511
  85.2 3.2 %collective-permute-start.2 = (f32[256,128]{1,0:T(8,128)S(1)}, f32[256,128]{1,0:T(8,128)S(1)}, u32[]{:S(2)}, u32[]{:S(2)}) collective-permute-start(f32[256,128]{1,0:T(8,128)S(1)} %get-tuple-element.26), channel_id=1, source_target_pairs={{0,1},{1,0},{2,3},{3,2},{4,5},{5,4},{6,7},{7,6},{8,9},{9,8},{10,11... | collective-permute-start | bytes 393224 | tf_op jit(solution)/shard_map/ppermute | solution.py:63
  89.5 10.2 %all-to-all-start.3 = ((f32[4,8,256]{2,1,0:T(8,128)}), f32[4,8,256]{2,1,0:T(8,128)S(1)}, u32[]{:S(2)}, u32[]{:S(2)}) async-start(f32[4,8,256]{2,1,0:T(8,128)} %get-tuple-element.28), calls=%async_computation.3 | async-start | bytes 65536 | tf_op jit(solution)/shard_map/all_to_all | solution.py:55
  (4 other events, 3.1 us)

commit v6 on v5

--- a/solution.py
+++ b/solution.py
@@ -315,7 +315,11 @@
         key_pos = (4 * pair + col // (2 * ROWS)) * BLOCK + x * (2 * ROWS) + col % (2 * ROWS)
         chunk(pair, key_pos <= query_pos, True, width)
 
-    @pl.when(z % 4 < 2)
+    @pl.when(z % 4 == 0)
+    def _():
+        last(QUAD // 4)
+
+    @pl.when(z % 4 == 1)
     def _():
         last(QUAD // 2)
 

time: 121 us -> 121 us (level)
  no operation moved by 1% of the time
where the time goes in v6:
time: 121 us; the launch traced here: 120 us
  blocking collectives  49.3 us (41%)
  Pallas kernels  26.3 us (22%)
  starting transfers between devices  25.2 us (21%)
  waiting for transfers between devices  13.2 us (11%)
  local copies, waits for them, and re-layouts  6.12 us (5%)
    all_gather x1, blocking collectives, local(): own_latents = lax.all_gather(latent_rows, 'sp', axis=0, tiled=False)  31.6 us
    pallas_call x8, Pallas kernels, whole(): pl.pallas_call(kernel, grid=() if specs is None else (1,), out_shape=out_...  20.1 us
    all_to_all x1, blocking collectives, among_chips(): lax.all_to_all(array, 'tp', 0, 0, axis_index_groups=SAME_CORE, tiled=True)  17.7 us
    all_to_all x2, starting transfers between devices, among_all(): return lax.all_to_all(array, 'tp', 0, 0, tiled=True)  8.86 us
    all_to_all x2, starting transfers between devices, among_chips(): lax.all_to_all(array, 'tp', 0, 0, axis_index_groups=SAME_CORE, tiled=True)  8.23 us
    pallas_call x1, Pallas kernels, local(): expand(own_latents, other_latents, key_up, key_gain[None], turned, begins)  6.19 us
    ppermute x3, starting transfers between devices, to_partner(): return lax.ppermute(array, 'tp', [(i, i ^ 1) for i in range(2 * CHIPS)])  6.16 us
    unnamed x40, local copies, waits for them, and re-layouts  6.12 us
  transfers between devices with their start and end apart: 8, of which 4 were waited for; matrix products, arithmetic and copies ran while one was open for 0% of the time, Pallas kernels for 17%

profile of v6, /device:TPU:384, one launch (start us, length us, event | category | flops | bytes accessed | tf_op | source)
XLA Modules:
  0.0 120.3 jit_solution(13581347556612646992)
XLA Ops:
  0.0 3.0 %shard_map.190 = (bf16[8,64,2048]{2,1,0:T(8,128)(2,1)}, bf16[72,256]{1,0:T(8,128)(2,1)}, f32[8,128]{1,0:T(8,128)}) custom-call(bf16[1,64,2048]{2,1,0:T(8,128)(2,1)} %tokens.1, f32[1,2048]{1,0:T(1,128)} %bitcast.19, bf16[2048,256]{1,0:T(8,128)(2,1)} %latent_down.1, bf16[32,2048]{1,0:T(8,128)(2,1)} %bitcast.18, f32[1,96]{1,0:T(1,128)} %bitcast.20), custom_call_target="tpu_custom_call" | custom-call | tf_op jit(solution)/shard_map/pallas_call | solution.py:74
  3.1 4.5 %all-to-all-start = ((bf16[8,64,2048]{2,1,0:T(8,128)(2,1)}), bf16[8,64,2048]{2,1,0:T(8,128)(2,1)}, u32[]{:S(2)}, u32[]{:S(2)}) async-start(bf16[8,64,2048]{2,1,0:T(8,128)(2,1)} %get-tuple-element.17), calls=%async_computation | async-start | bytes 4194304 | tf_op jit(solution)/shard_map/all_to_all | solution.py:59
  7.6 1.1 shard_map.195
  8.7 2.3 %collective-permute-start.3 = (bf16[272,2048]{1,0:T(8,128)(2,1)}, bf16[272,2048]{1,0:T(8,128)(2,1)S(1)}, u32[]{:S(2)}, u32[]{:S(2)}) collective-permute-start(bf16[272,2048]{1,0:T(8,128)(2,1)} %shard_map.195), channel_id=1, source_target_pairs={{0,1},{1,0},{2,3},{3,2},{4,5},{5,4},{6,7},{7,6},{8,9},{9,8},{10,11... | collective-permute-start | bytes 3342344 | tf_op jit(solution)/shard_map/ppermute | solution.py:63
  11.1 31.6 %all-gather = bf16[1152,256]{1,0:T(8,128)(2,1)S(1)} all-gather(bf16[72,256]{1,0:T(8,128)(2,1)S(1)} %copy-done.18), channel_id=2, replica_groups=mesh['sp'=16,'fs'=4,'tp'=8] {'sp'}, dimensions={0}, use_global_device_ids=true | all-gather | bytes 626688 | tf_op jit(solution)/shard_map/all_gather | solution.py:491
  42.7 1.9 %collective-permute-start = (bf16[16,72,256]{2,1,0:T(8,128)(2,1)S(1)}, bf16[16,72,256]{2,1,0:T(8,128)(2,1)}, u32[]{:S(2)}, u32[]{:S(2)}) collective-permute-start(bf16[16,72,256]{2,1,0:T(8,128)(2,1)S(1)} %bitcast.9), channel_id=1, source_target_pairs={{0,1},{1,0},{2,3},{3,2},{4,5},{5,4},{6,7},{7,6},{8,9},{9,8},{10,11... | collective-permute-start | bytes 1769480 | tf_op jit(solution)/shard_map/ppermute | solution.py:63
  44.6 1.0 copy-done.3
  45.7 1.0 copy-done.4
  47.3 3.8 %shard_map.191 = (bf16[8,256,128]{2,1,0:T(8,128)(2,1)}, bf16[512,128]{1,0:T(8,128)(2,1)}, bf16[16,128]{1,0:T(8,128)(2,1)}) custom-call(bf16[8,64,2048]{2,1,0:T(8,128)(2,1)} %all-to-all-done.rows_far, bf16[96,2048]{1,0:T(8,128)(2,1)S(1)} %bitcast.11, bf16[2048,128]{1,0:T(8,128)(2,1)S(1)} %copy-done.2, f32[8,128]{1,0:T(8,128)S(1)} %copy-done.11, ...), custom_call_target="tpu_custom_call" | custom-call | tf_op jit(solution)/shard_map/pallas_call | solution.py:74
  51.2 4.4 %all-to-all-start.1 = ((bf16[8,256,128]{2,1,0:T(8,128)(2,1)}), bf16[8,256,128]{2,1,0:T(8,128)(2,1)S(1)}, u32[]{:S(2)}, u32[]{:S(2)}) async-start(bf16[8,256,128]{2,1,0:T(8,128)(2,1)} %get-tuple-element.19), calls=%async_computation.1 | async-start | bytes 1048576 | tf_op jit(solution)/shard_map/all_to_all | solution.py:59
  55.6 0.9 copy-done.7
  58.0 6.2 %expand.1 = (bf16[8,96,2048]{2,1,0:T(8,128)(2,1)}, bf16[2048,256]{1,0:T(8,128)(2,1)}) custom-call(bf16[16,72,256]{2,1,0:T(8,128)(2,1)S(1)} %bitcast.10, bf16[16,72,256]{2,1,0:T(8,128)(2,1)} %collective-permute-done.other, bf16[256,512]{1,0:T(8,128)(2,1)S(1)} %copy-done.6, f32[1,96]{1,0:T(1,128)S(1)} %bitcast.17, f32[2,4,16,128]{3,2,1,0:T(8,128)S(1)} %copy-done.9, ...), custom_call_target="tpu_custom_call" | custom-call | tf_op jit(solution)/shard_map/expand/pallas_call | solution.py:538
  64.2 1.7 %all-to-all-done.1.queries = bf16[8,256,128]{2,1,0:T(8,128)(2,1)S(1)} async-done(((bf16[8,256,128]{2,1,0:T(8,128)(2,1)}), bf16[8,256,128]{2,1,0:T(8,128)(2,1)S(1)}, u32[]{:S(2)}, u32[]{:S(2)}) %all-to-all-start.1) | async-done | bytes 524320 | tf_op jit(solution)/shard_map/all_to_all | solution.py:59
  65.9 8.0 %shard_map.192 = bf16[4,272,256]{2,1,0:T(8,128)(2,1)} custom-call(bf16[8,256,128]{2,1,0:T(8,128)(2,1)S(1)} %all-to-all-done.1.queries, bf16[8,96,2048]{2,1,0:T(8,128)(2,1)} %get-tuple-element.21.keys_far, bf16[2048,256]{1,0:T(8,128)(2,1)} %get-tuple-element.22.latents_far, bf16[256,1024]{1,0:T(8,128)(2,1)} %value_far.1), custom_call_target="tpu_custom_call" | custom-call | tf_op jit(solution)/shard_map/pallas_call | solution.py:74
  73.9 3.5 %all-to-all-start.2 = ((bf16[4,272,256]{2,1,0:T(8,128)(2,1)}), bf16[4,272,256]{2,1,0:T(8,128)(2,1)S(1)}, u32[]{:S(2)}, u32[]{:S(2)}) async-start(bf16[4,272,256]{2,1,0:T(8,128)(2,1)} %shard_map.192), calls=%async_computation.2 | async-start | bytes 1114112 | tf_op jit(solution)/shard_map/all_to_all | solution.py:55
  77.4 1.9 %collective-permute-start.1 = (bf16[16,128]{1,0:T(8,128)(2,1)S(1)}, bf16[16,128]{1,0:T(8,128)(2,1)S(1)}, u32[]{:S(2)}, u32[]{:S(2)}) collective-permute-start(bf16[16,128]{1,0:T(8,128)(2,1)S(1)} %copy-done.19), channel_id=1, source_target_pairs={{0,32},{32,64},{64,96},{96,128},{128,160},{160,192},{192,224},{224... | collective-permute-start | bytes 12296 | tf_op jit(solution)/shard_map/ppermute | solution.py:515
  79.4 4.8 %collective-permute-done.1.halo = bf16[16,128]{1,0:T(8,128)(2,1)S(1)} collective-permute-done((bf16[16,128]{1,0:T(8,128)(2,1)S(1)}, bf16[16,128]{1,0:T(8,128)(2,1)S(1)}, u32[]{:S(2)}, u32[]{:S(2)}) %collective-permute-start.1) | collective-permute-done | bytes 4128 | tf_op jit(solution)/shard_map/ppermute | solution.py:515
  85.4 1.9 %collective-permute-start.2 = (f32[256,128]{1,0:T(8,128)S(1)}, f32[256,128]{1,0:T(8,128)S(1)}, u32[]{:S(2)}, u32[]{:S(2)}) collective-permute-start(f32[256,128]{1,0:T(8,128)S(1)} %get-tuple-element.26), channel_id=1, source_target_pairs={{0,1},{1,0},{2,3},{3,2},{4,5},{5,4},{6,7},{7,6},{8,9},{9,8},{10,11... | collective-permute-start | bytes 393224 | tf_op jit(solution)/shard_map/ppermute | solution.py:63
  87.3 1.3 %collective-permute-done.2.pool_other = f32[256,128]{1,0:T(8,128)S(1)} collective-permute-done((f32[256,128]{1,0:T(8,128)S(1)}, f32[256,128]{1,0:T(8,128)S(1)}, u32[]{:S(2)}, u32[]{:S(2)}) %collective-permute-start.2) | collective-permute-done | bytes 131104 | tf_op jit(solution)/shard_map/ppermute | solution.py:63
  88.6 1.1 shard_map.194
  89.7 4.7 %all-to-all-start.3 = ((f32[4,8,256]{2,1,0:T(8,128)}), f32[4,8,256]{2,1,0:T(8,128)S(1)}, u32[]{:S(2)}, u32[]{:S(2)}) async-start(f32[4,8,256]{2,1,0:T(8,128)} %get-tuple-element.28), calls=%async_computation.3 | async-start | bytes 65536 | tf_op jit(solution)/shard_map/all_to_all | solution.py:55
  94.5 5.4 %all-to-all-done.3.squares = f32[4,8,256]{2,1,0:T(8,128)S(1)} async-done(((f32[4,8,256]{2,1,0:T(8,128)}), f32[4,8,256]{2,1,0:T(8,128)S(1)}, u32[]{:S(2)}, u32[]{:S(2)}) %all-to-all-start.3) | async-done | bytes 32800 | tf_op jit(solution)/shard_map/all_to_all | solution.py:55
  99.9 1.8 %shard_map.196 = bf16[4,64,2048]{2,1,0:T(8,128)(2,1)} custom-call(f32[2,256,128]{2,1,0:T(8,128)S(1)} %get-tuple-element.27.attended, f32[256,128]{1,0:T(8,128)S(1)} %get-tuple-element.25.pool_own, f32[256,128]{1,0:T(8,128)S(1)} %collective-permute-done.2.pool_other, f32[4,8,256]{2,1,0:T(8,128)S(1)} %all-to-all-done.3.squares, f32[1,128]{1,0:T(1,128)S(1)} %bitcast.13, ...), custom_call_target="tpu_custom_call" | custom-call | tf_op jit(solution)/shard_map/pallas_call | solution.py:74
  101.8 17.7 %all_to_all.25.parts = bf16[4,64,2048]{2,1,0:T(8,128)(2,1)S(1)} all-to-all(bf16[4,64,2048]{2,1,0:T(8,128)(2,1)} %shard_map.196), channel_id=1, replica_groups={{0,2,4,6},{1,3,5,7},{8,10,12,14},{9,11,13,15},{16,18,20,22},{17,19,21,2..., dimensions={0} | all-to-all | bytes 2097152 | tf_op jit(solution)/shard_map/all_to_all | solution.py:55
  (43 shorter events, 4.3 us)
Async XLA Ops:
  3.0 4.6 %copy-start = (bf16[128,2048]{1,0:T(8,128)(2,1)S(1)}, bf16[128,2048]{1,0:T(8,128)(2,1)}, u32[]{:S(2)}) copy-start(bf16[128,2048]{1,0:T(8,128)(2,1)} %own_attention.1) | copy-start | bytes 1572868
  3.0 4.6 %copy-start.1 = (bf16[128,2048]{1,0:T(8,128)(2,1)S(1)}, bf16[128,2048]{1,0:T(8,128)(2,1)}, u32[]{:S(2)}) copy-start(bf16[128,2048]{1,0:T(8,128)(2,1)} %own_pool.1) | copy-start | bytes 1572868
  3.0 4.6 %copy-start.12 = (f32[128]{0:T(128)S(1)}, f32[128]{0:T(128)}, u32[]{:S(2)}) copy-start(f32[128]{0:T(128)} %param.32) | copy-start | bytes 1540
  3.0 4.6 %copy-start.14 = (f32[128]{0:T(128)S(1)}, f32[128]{0:T(128)}, u32[]{:S(2)}) copy-start(f32[128]{0:T(128)} %param.33) | copy-start | bytes 1540
  3.1 41.5 %all-to-all-start = ((bf16[8,64,2048]{2,1,0:T(8,128)(2,1)}), bf16[8,64,2048]{2,1,0:T(8,128)(2,1)}, u32[]{:S(2)}, u32[]{:S(2)}) async-start(bf16[8,64,2048]{2,1,0:T(8,128)(2,1)} %get-tuple-element.17), calls=%async_computation | async-start | bytes 4194304 | tf_op jit(solution)/shard_map/all_to_all | solution.py:59
  7.5 3.5 %copy-start.18 = (bf16[72,256]{1,0:T(8,128)(2,1)S(1)}, bf16[72,256]{1,0:T(8,128)(2,1)}, u32[]{:S(2)}) copy-start(bf16[72,256]{1,0:T(8,128)(2,1)} %get-tuple-element.20) | copy-start | bytes 110596
  7.6 37.0 %copy-start.2 = (bf16[2048,128]{1,0:T(8,128)(2,1)S(1)}, bf16[2048,128]{1,0:T(8,128)(2,1)}, u32[]{:S(2)}) copy-start(bf16[2048,128]{1,0:T(8,128)(2,1)} %pool_down.1) | copy-start | bytes 1572868
  7.6 37.0 %copy-start.10 = (f32[2,16,128]{2,1,0:T(8,128)S(1)}, f32[2,16,128]{2,1,0:T(8,128)}, u32[]{:S(2)}) copy-start(f32[2,16,128]{2,1,0:T(8,128)} %constant.9.clone.starts) | copy-start | bytes 49156
  8.7 85.7 %collective-permute-start.3 = (bf16[272,2048]{1,0:T(8,128)(2,1)}, bf16[272,2048]{1,0:T(8,128)(2,1)S(1)}, u32[]{:S(2)}, u32[]{:S(2)}) collective-permute-start(bf16[272,2048]{1,0:T(8,128)(2,1)} %shard_map.195), channel_id=1, source_target_pairs={{0,1},{1,0},{2,3},{3,2},{4,5},{5,4},{6,7},{7,6},{8,9},{9,8},{10,11... | collective-permute-start | bytes 3342344 | tf_op jit(solution)/shard_map/ppermute | solution.py:63
  42.7 12.9 %collective-permute-start = (bf16[16,72,256]{2,1,0:T(8,128)(2,1)S(1)}, bf16[16,72,256]{2,1,0:T(8,128)(2,1)}, u32[]{:S(2)}, u32[]{:S(2)}) collective-permute-start(bf16[16,72,256]{2,1,0:T(8,128)(2,1)S(1)} %bitcast.9), channel_id=1, source_target_pairs={{0,1},{1,0},{2,3},{3,2},{4,5},{5,4},{6,7},{7,6},{8,9},{9,8},{10,11... | collective-permute-start | bytes 1769480 | tf_op jit(solution)/shard_map/ppermute | solution.py:63
  44.6 1.0 copy-start.3
  45.7 1.0 copy-start.4
  47.3 8.2 %copy-start.6 = (bf16[256,512]{1,0:T(8,128)(2,1)S(1)}, bf16[256,512]{1,0:T(8,128)(2,1)}, u32[]{:S(2)}) copy-start(bf16[256,512]{1,0:T(8,128)(2,1)} %key_up.1) | copy-start | bytes 786436
  51.2 14.7 %all-to-all-start.1 = ((bf16[8,256,128]{2,1,0:T(8,128)(2,1)}), bf16[8,256,128]{2,1,0:T(8,128)(2,1)S(1)}, u32[]{:S(2)}, u32[]{:S(2)}) async-start(bf16[8,256,128]{2,1,0:T(8,128)(2,1)} %get-tuple-element.19), calls=%async_computation.1 | async-start | bytes 1048576 | tf_op jit(solution)/shard_map/all_to_all | solution.py:59
  55.6 1.0 copy-start.7
  65.9 11.6 %copy-start.19 = (bf16[16,128]{1,0:T(8,128)(2,1)S(1)}, bf16[16,128]{1,0:T(8,128)(2,1)}, u32[]{:S(2)}) copy-start(bf16[16,128]{1,0:T(8,128)(2,1)} %get-tuple-element.24) | copy-start | bytes 12292
  65.9 18.3 %copy-start.5 = (bf16[16,64,64]{2,1,0:T(8,128)(2,1)S(1)}, bf16[16,64,64]{2,1,0:T(8,128)(2,1)}, u32[]{:S(2)}) copy-start(bf16[16,64,64]{2,1,0:T(8,128)(2,1)} %maps.1) | copy-start | bytes 393220
  65.9 18.3 %copy-start.16 = (f32[128]{0:T(128)S(1)}, f32[128]{0:T(128)}, u32[]{:S(2)}) copy-start(f32[128]{0:T(128)} %param.31) | copy-start | bytes 1540
  73.9 26.0 %copy-start.13 = (f32[128]{0:T(128)S(1)}, f32[128]{0:T(128)}, u32[]{:S(2)}) copy-start(f32[128]{0:T(128)} %param.32) | copy-start | bytes 1540
  73.9 26.0 %copy-start.15 = (f32[128]{0:T(128)S(1)}, f32[128]{0:T(128)}, u32[]{:S(2)}) copy-start(f32[128]{0:T(128)} %param.33) | copy-start | bytes 1540
  73.9 14.7 %all-to-all-start.2 = ((bf16[4,272,256]{2,1,0:T(8,128)(2,1)}), bf16[4,272,256]{2,1,0:T(8,128)(2,1)S(1)}, u32[]{:S(2)}, u32[]{:S(2)}) async-start(bf16[4,272,256]{2,1,0:T(8,128)(2,1)} %shard_map.192), calls=%async_computation.2 | async-start | bytes 1114112 | tf_op jit(solution)/shard_map/all_to_all | solution.py:55
  77.4 6.7 %collective-permute-start.1 = (bf16[16,128]{1,0:T(8,128)(2,1)S(1)}, bf16[16,128]{1,0:T(8,128)(2,1)S(1)}, u32[]{:S(2)}, u32[]{:S(2)}) collective-permute-start(bf16[16,128]{1,0:T(8,128)(2,1)S(1)} %copy-done.19), channel_id=1, source_target_pairs={{0,32},{32,64},{64,96},{96,128},{128,160},{160,192},{192,224},{224... | collective-permute-start | bytes 12296 | tf_op jit(solution)/shard_map/ppermute | solution.py:515
  85.4 3.2 %collective-permute-start.2 = (f32[256,128]{1,0:T(8,128)S(1)}, f32[256,128]{1,0:T(8,128)S(1)}, u32[]{:S(2)}, u32[]{:S(2)}) collective-permute-start(f32[256,128]{1,0:T(8,128)S(1)} %get-tuple-element.26), channel_id=1, source_target_pairs={{0,1},{1,0},{2,3},{3,2},{4,5},{5,4},{6,7},{7,6},{8,9},{9,8},{10,11... | collective-permute-start | bytes 393224 | tf_op jit(solution)/shard_map/ppermute | solution.py:63
  89.7 10.2 %all-to-all-start.3 = ((f32[4,8,256]{2,1,0:T(8,128)}), f32[4,8,256]{2,1,0:T(8,128)S(1)}, u32[]{:S(2)}, u32[]{:S(2)}) async-start(f32[4,8,256]{2,1,0:T(8,128)} %get-tuple-element.28), calls=%async_computation.3 | async-start | bytes 65536 | tf_op jit(solution)/shard_map/all_to_all | solution.py:55
  (4 other events, 3.1 us)
